TPU v7x, 32 devices: a whole 2x2x4 slice. The times are simulated.
32 devices in a mesh: sp: 8 (over z, y), tp: 4 (over x, core).
Axes of the slice: x: 2, y: 2, z: 4, core: 2. Of those that a mesh axis runs over, the one named last changes fastest.
Arguments:
- tokens: bfloat16 [8192, 2048], P('sp', 'tp'), may hold values from -16 to 16
- mix_gain: float32 [2048], replicated, may hold values from 0.1 to 1.9
- query_weight: bfloat16 [2048, 1024], P(None, 'tp'), may hold values from -0.125 to 0.125
- key_weight: bfloat16 [2048, 1024], P(None, 'tp'), may hold values from -0.125 to 0.125
- value_weight: bfloat16 [2048, 1024], P(None, 'tp'), may hold values from -0.125 to 0.125
- outer_gate_weight: bfloat16 [2048, 1024], P(None, 'tp'), may hold values from -0.125 to 0.125
- inner_gate_weight: bfloat16 [2048, 1024], P(None, 'tp'), may hold values from -0.125 to 0.125
- conv_input_weight: bfloat16 [2048, 1024], P(None, 'tp'), may hold values from -0.125 to 0.125
- query_gain: float32 [64], replicated, may hold values from 0.6 to 10
- key_gain: float32 [64], replicated, may hold values from 0.6 to 10
- gate_totals: float32 [8192, 16], P('sp', 'tp'), may hold values from -2048 to 0, as said below
- conv_taps: float32 [3, 1024], P(None, 'tp'), may hold values from -3 to 3
- attn_out_gain: float32 [1024], P('tp'), may hold values from 0.1 to 1.9
- conv_out_gain: float32 [1024], P('tp'), may hold values from 0.1 to 1.9
- attn_out_weight: bfloat16 [1024, 2048], P('tp'), may hold values from -0.125 to 0.125
- conv_out_weight: bfloat16 [1024, 2048], P('tp'), may hold values from -0.125 to 0.125
Outputs:
- mixed: bfloat16 [8192, 2048], P(('sp', 'tp'))
Inputs may be any that keep to these rules, and one draw needn't show every extreme that they name: `gate_totals`: in every head the values never rise from one position to the next.
All inputs are finite; a program needn't handle non-finite values.
Results may differ from a plain program's by a relative error of at most 0.015.
The roundings to bfloat16 on the way count: a program that leaves them out, or rounds other values in their place, can miss the bound.
Values may be sent and summed in bfloat16 or wider, within the bound.
No kernel may reach another device: no remote copies, remote signals or barrier semaphores. Data moves between devices by JAX's collectives and lax.ppermute only.
A program may use at most 64 MiB of HBM per device.

v0:
```python
import jax
import jax.numpy as jnp
from jax import lax
from jax.sharding import PartitionSpec as P

NORM_EPSILON = 1e-06


def shifted(shard, axis, by):
    devices = lax.axis_size(axis)
    pairs = [(i, i + by) for i in range(devices) if 0 <= i + by < devices]
    return lax.ppermute(shard, axis, pairs)


def head_norm(values, head_dim, gain):
    row_count = values.shape[0]
    grouped = values.reshape(row_count, -1, head_dim)
    normed = grouped * lax.rsqrt(jnp.mean(grouped * grouped, axis=2, keepdims=True) + NORM_EPSILON)
    return (normed * gain.reshape(-1, head_dim)).reshape(row_count, -1)


def per_device(
    tokens,
    mix_gain,
    query_weight,
    key_weight,
    value_weight,
    outer_gate_weight,
    inner_gate_weight,
    conv_input_weight,
    query_gain,
    key_gain,
    gate_totals,
    conv_taps,
    attn_out_gain,
    conv_out_gain,
    attn_out_weight,
    conv_out_weight,
):
    row_count = tokens.shape[0]
    head_dim = query_gain.shape[0]
    attn_width = query_weight.shape[1]
    conv_width = outer_gate_weight.shape[1]
    head_count = attn_width // head_dim
    stacked = jnp.concatenate(
        [
            query_weight,
            key_weight,
            value_weight,
            outer_gate_weight,
            inner_gate_weight,
            conv_input_weight,
        ],
        axis=1,
    )
    widened = tokens.astype(jnp.float32)
    squares = lax.psum(jnp.sum(widened * widened, axis=1), "tp")
    scaled = (
        lax.all_gather(tokens, "tp", axis=1, tiled=True).astype(jnp.float32) * mix_gain
    ).astype(jnp.bfloat16)
    product = jnp.dot(scaled, stacked, preferred_element_type=jnp.float32)
    row_scale = lax.rsqrt(squares / mix_gain.shape[0] + NORM_EPSILON)[:, None]
    projected = product * row_scale
    queries = head_norm(projected[:, 0:attn_width], head_dim, query_gain).astype(jnp.bfloat16)
    key_rows = head_norm(projected[:, attn_width : 2 * attn_width], head_dim, key_gain).astype(
        jnp.bfloat16
    )
    value_rows = projected[:, 2 * attn_width : 3 * attn_width].astype(jnp.bfloat16)
    conv_base = 3 * attn_width
    proj_outer = projected[:, conv_base : conv_base + conv_width]
    proj_inner = projected[:, conv_base + conv_width : conv_base + 2 * conv_width]
    proj_input = projected[:, conv_base + 2 * conv_width : conv_base + 3 * conv_width]
    all_gates = lax.all_gather(gate_totals, "sp", axis=0, tiled=True)
    query_start = lax.axis_index("sp") * row_count
    sp_count = lax.axis_size("sp")
    sequence_length = sp_count * row_count
    key_positions = jnp.arange(row_count, dtype=jnp.int32)
    score_scale = head_dim ** (-0.5)
    groups = [(queries, gate_totals, query_start + key_positions)]
    groups = [
        (
            group_rows.reshape(group_rows.shape[0], head_count, head_dim),
            group_gates.T,
            group_positions,
        )
        for group_rows, group_gates, group_positions in groups
    ]

    def fold_block(carried, block_keys, block_values, key_start):
        keys_heads = block_keys.reshape(row_count, head_count, head_dim)
        values_heads = block_values.reshape(row_count, head_count, head_dim)
        results = []
        for group, current_state in zip(groups, carried):
            group_queries, group_gates, group_positions = group

            def compute(
                current,
                group_queries=group_queries,
                group_gates=group_gates,
                group_positions=group_positions,
            ):
                running_max, accum = current
                scores = (
                    jnp.einsum(
                        "qhd,khd->hqk",
                        group_queries,
                        keys_heads,
                        preferred_element_type=jnp.float32,
                    )
                    * score_scale
                )
                block_gates = lax.dynamic_slice_in_dim(all_gates, key_start, row_count, 0).T
                scores = scores + group_gates[:, :, None] - block_gates[:, None, :]
                allowed = (key_start + key_positions)[None, :] <= group_positions[:, None]
                new_max = jnp.maximum(
                    running_max, jnp.max(jnp.where(allowed[None], scores, -jnp.inf), axis=2)
                )
                weights = jnp.where(
                    allowed[None], jnp.exp(scores - new_max[:, :, None]), 0.0
                ).astype(jnp.bfloat16)
                factor = jnp.exp(running_max - new_max)
                added = jnp.einsum(
                    "hqk,khd->qhd", weights, values_heads, preferred_element_type=jnp.float32
                )
                return (new_max, accum * factor.T[:, :, None] + added)

            live = (key_start >= 0) & (key_start <= group_positions[-1])
            results.append(lax.cond(live, compute, lambda current: current, current_state))
        return tuple(results)

    initial = tuple(
        (
            (
                jnp.full((head_count, group[0].shape[0]), -1e30, jnp.float32),
                jnp.zeros((group[0].shape[0], head_count, head_dim), jnp.float32),
            )
            for group in groups
        )
    )
    start_at = jnp.int32(0)
    piece_keys = lax.all_gather(key_rows, "sp", axis=0, tiled=True)
    piece_values = lax.all_gather(value_rows, "sp", axis=0, tiled=True)

    def fold_one(block_number, current):
        offset = block_number * row_count
        block_keys = lax.dynamic_slice_in_dim(piece_keys, offset, row_count, 0)
        block_values = lax.dynamic_slice_in_dim(piece_values, offset, row_count, 0)
        key_start = jnp.mod(start_at + offset, sequence_length)
        return fold_block(current, block_keys, block_values, key_start)

    folded = lax.fori_loop(0, piece_keys.shape[0] // row_count, fold_one, initial)
    normed_groups = [
        head_norm(state[1].reshape(state[1].shape[0], attn_width), head_dim, attn_out_gain).astype(
            jnp.bfloat16
        )
        for state in folded
    ]
    attn_mixed = normed_groups[0]
    tap_count = conv_taps.shape[0]
    gated = (proj_inner * proj_input).astype(jnp.bfloat16)
    prior_rows = shifted(gated[row_count - tap_count + 1 :], "sp", 1)
    padded = jnp.concatenate([prior_rows, gated], axis=0).astype(jnp.float32)
    convolved = conv_taps[0] * padded[0:row_count]
    for tap_index in range(1, tap_count):
        convolved = convolved + conv_taps[tap_index] * padded[tap_index : tap_index + row_count]
    conv_mixed = head_norm(proj_outer * convolved, head_dim, conv_out_gain).astype(jnp.bfloat16)
    joined = jnp.concatenate([attn_mixed, conv_mixed], axis=1)
    out_weight = jnp.concatenate([attn_out_weight, conv_out_weight], axis=0)
    return lax.psum_scatter(
        jnp.dot(joined, out_weight, preferred_element_type=jnp.float32).astype(jnp.bfloat16),
        "tp",
        scatter_dimension=0,
        tiled=True,
    )


def solution(mesh):
    placed = (
        P("sp", "tp"),
        P(),
        P(None, "tp"),
        P(None, "tp"),
        P(None, "tp"),
        P(None, "tp"),
        P(None, "tp"),
        P(None, "tp"),
        P(),
        P(),
        P("sp", "tp"),
        P(None, "tp"),
        P("tp"),
        P("tp"),
        P("tp", None),
        P("tp", None),
    )
    return jax.shard_map(
        per_device, mesh=mesh, in_specs=placed, out_specs=P(("sp", "tp"), None), check_vma=False
    )
```

profile of v0, /device:TPU:0, one launch (start us, length us, event | category | flops | bytes accessed | tf_op | source)
XLA Modules:
  0.0 378.3 jit_solution(2975799271338801407)
XLA Ops:
  6.5 0.7 all-gather.4.cloned.1.call-update
  7.3 0.8 mul.204
  8.1 0.1 mul.205
  8.2 0.7 mul.213
  8.9 0.1 mul.214
  9.0 1.5 multiply_reduce_fusion
  10.5 8.4 %psum.7 = f32[1024]{0:T(1024)S(1)} all-reduce(f32[1024]{0:T(1024)S(1)} %multiply_reduce_fusion), channel_id=1, replica_groups=mesh['sp'=8,'tp'=4] {'tp'}, use_global_device_ids=true, to_apply=%region_1.0 | all-reduce | flops 1024 | bytes 8192 | tf_op jit(solution)/shard_map/psum | solution.py:57
  18.9 2.6 constant_dynamic-update-slice_fusion.5
  21.4 2.3 constant_dynamic-update-slice_fusion.4
  23.8 1.1 constant_dynamic-update-slice_fusion.3
  24.9 1.2 constant_dynamic-update-slice_fusion.2
  26.0 1.1 constant_dynamic-update-slice_fusion.1
  27.2 1.1 constant_dynamic-update-slice_fusion
  28.3 17.8 %all-gather.4.cloned.1.call-done = bf16[1024,2048]{1,0:T(8,128)(2,1)} async-done(((bf16[1024,512]{1,0:T(8,128)(2,1)}), bf16[1024,2048]{1,0:T(8,128)(2,1)}) %all-gather.4.cloned.1.call-update) | async-done | bytes 4194320 | tf_op jit(solution)/shard_map/all_gather | solution.py:59
  46.1 10.0 %convolution_multiply_fusion = f32[1024,1536]{1,0:T(8,128)S(1)} fusion(bf16[2048,1536]{1,0:T(8,128)(2,1)} %constant_dynamic-update-slice_fusion, bf16[1024,2048]{1,0:T(8,128)(2,1)} %all-gather.4.cloned.1.call-done, f32[2048]{0:T(1024)S(1)} %copy-done.10, f32[1024]{0:T(1024)S(1)} %add_rsqrt_fusion.4), kind=kOutput, calls=%fused_computation.21 | convolution fusion | flops 6450315264 | bytes 16789504 | tf_op jit(solution)/shard_map/dot_general | solution.py:61
  56.2 2.6 copy-done
  58.8 0.2 slice_multiply_fusion.4
  59.0 0.3 copy.26
  59.3 0.1 bitcast_reduce_fusion.2
  59.4 0.1 mul.201
  59.5 0.3 copy.27
  59.9 0.3 copy.28
  60.2 0.1 bitcast_reduce_fusion.1
  60.3 0.1 mul.210
  60.5 0.3 copy.29
  60.8 3.5 multiply_convert_fusion.4
  64.3 0.0 all-gather.8.cloned.1.call-start
  64.3 2.1 slice.97
  66.6 3.4 collective-permute-start
  70.0 31.5 %all_gather.14 = f32[8192,4]{0,1:T(4,128)S(1)} all-gather(f32[1024,4]{0,1:T(4,128)S(1)} %copy-done.6), channel_id=1, replica_groups=mesh['sp'=8,'tp'=4] {'sp'}, dimensions={0}, use_global_device_ids=true | all-gather | bytes 147456 | tf_op jit(solution)/shard_map/all_gather | solution.py:73
  101.5 0.1 mul.220
  101.6 1.0 copy.30
  102.6 0.1 maximum_convert_fusion
  102.7 1.6 fusion.29
  104.3 0.3 copy.33
  104.7 0.1 bitcast_reduce_fusion
  104.8 0.1 mul.236
  104.9 0.3 copy.34
  105.3 0.2 multiply_convert_fusion.2
  105.4 32.7 %all-gather.6.cloned.1.call-done = bf16[8192,256]{1,0:T(8,128)(2,1)} async-done(((bf16[1024,256]{1,0:T(8,128)(2,1)}), bf16[8192,256]{1,0:T(8,128)(2,1)}) %all-gather.6.cloned.1.call-update) | async-done | bytes 4194320 | tf_op jit(solution)/shard_map/all_gather | solution.py:141
  138.1 6.3 %copy.31 = bf16[8192,256]{0,1:T(8,128)(2,1)} copy(bf16[8192,256]{1,0:T(8,128)(2,1)} %all-gather.6.cloned.1.call-done) | data formatting | bytes 8388608
  144.5 67.1 %all-gather.8.cloned.1.call-done = bf16[8192,256]{1,0:T(8,128)(2,1)} async-done(((bf16[1024,256]{1,0:T(8,128)(2,1)}), bf16[8192,256]{1,0:T(8,128)(2,1)}) %all-gather.8.cloned.1.call-update) | async-done | bytes 4194320 | tf_op jit(solution)/shard_map/all_gather | solution.py:142
  211.6 6.4 %copy.32 = bf16[8192,256]{0,1:T(8,128)(2,1)} copy(bf16[8192,256]{1,0:T(8,128)(2,1)} %all-gather.8.cloned.1.call-done) | data formatting | bytes 8388608
  218.0 0.1 broadcast_in_dim.46
  218.2 23.0 %while.18 = (s32[]{:T(128)}, f32[4,1024]{1,0:T(4,128)S(1)}, f32[1024,4,64]{0,2,1:T(8,128)S(1)}, s32[1024]{0:T(1024)S(1)}, bf16[8192,256]{0,1:T(8,128)(2,1)}, /*i...) while((s32[]{:T(128)}, f32[4,1024]{1,0:T(4,128)S(1)}, ...), condition=%wide.region_8.9_spmd.clone, body=%wide.region_4.8_spmd.clone.sunk | while | flops 1121457152 | bytes 42701296 | solution.py:151
  218.2 0.7 slice.106
  219.6 11.6 %conditional.3 = ((f32[4,1024]{1,0:T(4,128)S(1)}, f32[1024,4,64]{0,2,1:T(8,128)S(1)})) conditional(s32[]{:T(128)} %convert_element_type.80, (f32[4,1024]{1,0:T(4,128)S(1)}, f32[1024,4,64]{0,2,1:T(8,128)S(1)}) %tuple.67, (s32[]{:T(128)}, s32[1024]{0:T(1024)S(1)}, s32[1024]{0:T(1024)S(1)}, s32[]{:T(128)}, bf16[8192,256]{0,1:T(8,128)(2,1)}, ...), branch_computations={%region_5.5_spmd, %region_6.7_spmd} | conditional | flops 1121457152 | bytes 42696808 | solution.py:128
  219.6 0.1 dynamic-slice_bitcast_fusion
  219.7 1.3 constant_dynamic-slice_fusion
  221.0 0.7 broadcast_compare_fusion
  221.6 4.6 %fusion.2 = (f32[4,1024]{1,0:T(4,128)S(1)}, f32[4,1024,1024]{2,1,0:T(8,128)S(1)}) fusion(f32[4,1024]{1,0:T(4,128)S(1)} %dynamic-slice_bitcast_fusion, f32[4,1024]{1,0:T(4,128)S(1)} %get-tuple-element.341, pred[1024,1024]{0,1:T(8,128)(4,1)S(1)} %broadcast_compare_fusion, bf16[1024,4,64]{0,2,1:T(8,128)(2,1)S(1)} %bitcast.49, ...), kind=kOutput, calls=%fused_computation.3 | convolution fusion | flops 557838336 | bytes 18923520 | tf_op jit(solution)/shard_map/while/body/eval_jaxpr/cond/branch_1_fun/qhd,khd->hqk/dot_general | solution.py:104
  226.2 4.9 %fusion.12 = f32[1024,4,64]{0,2,1:T(8,128)S(1)} fusion(bf16[1024,4,64]{0,2,1:T(8,128)(2,1)S(1)} %bitcast.48, f32[4,1024,1024]{2,1,0:T(8,128)S(1)} %get-tuple-element.423, f32[4,1024]{1,0:T(4,128)S(1)} %get-tuple-element.495, f32[4,1024]{1,0:T(4,128)S(1)} %dynamic-slice_bitcast_fusion, f32[4,1024]{1,0:T(4,128)S(1)} %get-tuple-element.341, ...), kind=kOutput, calls=%fused_computation.12 | convolution fusion | flops 562561024 | bytes 20512768 | tf_op jit(solution)/shard_map/while/body/eval_jaxpr/cond/branch_1_fun/hqk,khd->qhd/dot_general | solution.py:122
  231.2 0.7 slice.106
  232.6 0.7 slice.106
  234.1 0.7 slice.106
  235.5 0.7 slice.106
  236.9 0.7 slice.106
  238.3 0.7 slice.106
  239.8 0.7 slice.106
  241.1 0.1 multiply_reduce_fusion.1
  241.3 0.1 multiply_convert_fusion.3
  241.4 0.2 copy.35
  241.6 5.8 %convolution_convert_fusion = bf16[1024,2048]{1,0:T(8,128)(2,1)} fusion(bf16[256,2048]{1,0:T(8,128)(2,1)} %param.35, bf16[256,2048]{1,0:T(8,128)(2,1)} %param.34, bf16[1024,256]{1,0:T(8,128)(2,1)S(1)} %multiply_convert_fusion.2, bf16[1024,256]{1,0:T(8,128)(2,1)S(1)} %copy.35), kind=kOutput, calls=%fused_computation.23 | convolution fusion | flops 2155872256 | bytes 7340032 | tf_op jit(solution)/shard_map/dot_general | solution.py:170
  247.5 124.3 %reduce-scatter.2.cloned.1.call-done = bf16[256,2048]{1,0:T(8,128)(2,1)} async-done(((bf16[1024,2048]{1,0:T(8,128)(2,1)}), bf16[256,2048]{1,0:T(8,128)(2,1)}) %reduce-scatter.2.cloned.1.call-update) | async-done | bytes 1048592 | tf_op jit(solution)/shard_map/reduce_scatter | solution.py:169
  (54 shorter events, 0.4 us)
Async XLA Ops:
  6.5 17.2 %copy-start.1 = (bf16[2048,256]{1,0:T(8,128)(2,1)S(1)}, bf16[2048,256]{1,0:T(8,128)(2,1)}, u32[]{:S(2)}) copy-start(bf16[2048,256]{1,0:T(8,128)(2,1)} %param.24) | copy-start | bytes 3145732
  6.5 18.4 %copy-start.2 = (bf16[2048,256]{1,0:T(8,128)(2,1)S(1)}, bf16[2048,256]{1,0:T(8,128)(2,1)}, u32[]{:S(2)}) copy-start(bf16[2048,256]{1,0:T(8,128)(2,1)} %param.25) | copy-start | bytes 3145732
  6.5 19.5 %copy-start.3 = (bf16[2048,256]{1,0:T(8,128)(2,1)S(1)}, bf16[2048,256]{1,0:T(8,128)(2,1)}, u32[]{:S(2)}) copy-start(bf16[2048,256]{1,0:T(8,128)(2,1)} %param.26) | copy-start | bytes 3145732
  6.5 39.6 %all-gather.4.cloned.1.call-start = ((), (), s32[]{:S(2)}) async-start(), calls=%async_computation.1 | async-start | bytes 5242880 | tf_op jit(solution)/shard_map/all_gather | solution.py:59
  7.3 130.9 %all-gather.6.cloned.1.call-start = ((), (), s32[]{:S(2)}) async-start(), calls=%async_computation.2 | async-start | bytes 4718592 | tf_op jit(solution)/shard_map/all_gather | solution.py:141
  18.8 8.3 %copy-start.4 = (bf16[2048,256]{1,0:T(8,128)(2,1)S(1)}, bf16[2048,256]{1,0:T(8,128)(2,1)}, u32[]{:S(2)}) copy-start(bf16[2048,256]{1,0:T(8,128)(2,1)} %param.27) | copy-start | bytes 3145732
  18.9 27.3 %copy-start.10 = (f32[2048]{0:T(1024)S(1)}, f32[2048]{0:T(1024)}, u32[]{:S(2)}) copy-start(f32[2048]{0:T(1024)} %param.21) | copy-start | bytes 24580
  56.1 2.7 copy-start
  60.4 6.1 %copy-start.7 = (f32[3,256]{1,0:T(4,128)S(1)}, f32[3,256]{1,0:T(4,128)}, u32[]{:S(2)}) copy-start(f32[3,256]{1,0:T(4,128)} %param.31) | copy-start | bytes 9220
  60.5 9.5 %copy-start.6 = (f32[1024,4]{0,1:T(4,128)S(1)}, f32[1024,4]{0,1:T(4,128)}, u32[]{:S(2)}) copy-start(f32[1024,4]{0,1:T(4,128)} %param.30) | copy-start | bytes 49156
  60.5 41.0 %copy-start.9 = (f32[256]{0:T(256)S(1)}, f32[256]{0:T(256)}, u32[]{:S(2)}) copy-start(f32[256]{0:T(256)} %param.32) | copy-start | bytes 3076
  64.3 147.3 %all-gather.8.cloned.1.call-start = ((), (), s32[]{:S(2)}) async-start(), calls=%async_computation.3 | async-start | bytes 4718592 | tf_op jit(solution)/shard_map/all_gather | solution.py:142
  66.5 305.3 %reduce-scatter.2.cloned.1.call-start = ((), (), s32[]{:S(2)}) async-start(), calls=%async_computation.4 | async-start | bytes 5242880 | tf_op jit(solution)/shard_map/reduce_scatter | solution.py:169
  66.6 36.0 %collective-permute-start = (bf16[2,256]{1,0:T(2,128)(2,1)S(1)}, bf16[2,256]{1,0:T(2,128)(2,1)S(1)}, u32[]{:S(2)}, u32[]{:S(2)}) collective-permute-start(bf16[2,256]{1,0:T(2,128)(2,1)S(1)} %slice.70), channel_id=1, source_target_pairs={{0,4},{4,8},{8,12},{12,16},{16,20},{20,24},{24,28},{1,5},{5,9},{9,... | collective-permute-start | bytes 3080 | tf_op jit(solution)/shard_map/ppermute | solution.py:12
  102.7 2.6 copy-start.8
  144.5 73.7 %copy-start.5 = (bf16[1024,256]{0,1:T(8,128)(2,1)S(1)}, bf16[1024,256]{0,1:T(8,128)(2,1)}, u32[]{:S(2)}) copy-start(bf16[1024,256]{0,1:T(8,128)(2,1)} %copy.30) | copy-start | bytes 1572868
Sparse Core Ops, SparseCore 0:
  8.9 37.1 all-gather.3
  64.4 73.6 all-gather.5
  140.3 71.3 all-gather.7
  247.6 124.1 reduce-scatter.1
where the time goes:
time: 379 us; the launch traced here: 378 us
  waiting for transfers between devices  243 us (64%)
  blocking collectives  39.9 us (11%)
  local copies, waits for them, and re-layouts  39 us (10%)
  matrix products  25.4 us (7%)
  between operations  13.4 us (4%)
  other arithmetic  8.24 us (2%)
  loops' own time  6.15 us (2%)
    reduce_scatter x1, waiting for transfers between devices, per_device(): lax.psum_scatter(jnp.dot(joined, out_weight, preferred_element_type=jnp.f...  124 us
    all_gather x1, waiting for transfers between devices, per_device(): piece_values = lax.all_gather(value_rows, 'sp', axis=0, tiled=True)  67.1 us
    all_gather x1, waiting for transfers between devices, per_device(): piece_keys = lax.all_gather(key_rows, 'sp', axis=0, tiled=True)  32.7 us
    all_gather x1, blocking collectives, per_device(): all_gates = lax.all_gather(gate_totals, 'sp', axis=0, tiled=True)  31.5 us
    unnamed x29, local copies, waits for them, and re-layouts  23.8 us
    all_gather x1, waiting for transfers between devices, per_device(): lax.all_gather(tokens, 'tp', axis=1, tiled=True).astype(jnp.float32)  17.8 us
    dot_general x1, matrix products, per_device(): product = jnp.dot(scaled, stacked, preferred_element_type=jnp.float32)  10 us
    psum x1, blocking collectives, per_device(): squares = lax.psum(jnp.sum(widened * widened, axis=1), 'tp')  8.38 us
  transfers between devices with their start and end apart: 5, of which 4 were waited for; matrix products, arithmetic and copies ran while one was open for 7% of the time, Pallas kernels for 0%

commit v1 on v0

v1 whole, which is shorter than its diff:
```python
import jax
import jax.numpy as jnp
from jax import lax
from jax.experimental import pallas as pl
from jax.experimental.pallas import tpu as pltpu
from jax.sharding import PartitionSpec as P

NORM_EPSILON = 1e-06
LOG2_E = 1.4426950408889634
ROW_CHUNKS = 2
QUERY_TILE = 512
F32 = jnp.float32
BF16 = jnp.bfloat16


def swapped(shard, axis, offset):
    devices = lax.axis_size(axis)
    return lax.ppermute(shard, axis, [(i, i ^ offset) for i in range(devices)])


def xor_offsets(count):
    offsets = [0]
    bit = count >> 1
    while bit:
        offsets = offsets + [o ^ bit for o in offsets]
        bit >>= 1
    return offsets


def spread(shard, axis):
    pieces = [shard]
    bit = lax.axis_size(axis) >> 1
    while bit:
        pieces = pieces + [swapped(piece, axis, bit) for piece in pieces]
        bit >>= 1
    return pieces


def vmem_call(body, out_shape, operands, scalars=0, scratch=(), flops=0, limit=16):
    specs = [pl.BlockSpec(memory_space=pltpu.SMEM)] * scalars
    specs += [pl.BlockSpec(memory_space=pltpu.VMEM)] * (len(operands) - scalars)
    many = isinstance(out_shape, (list, tuple))
    out_specs = [pl.BlockSpec(memory_space=pltpu.VMEM)] * len(out_shape) if many else pl.BlockSpec(memory_space=pltpu.VMEM)
    return pl.pallas_call(
        body,
        out_shape=out_shape,
        in_specs=specs,
        out_specs=out_specs,
        scratch_shapes=list(scratch),
        compiler_params=pltpu.CompilerParams(vmem_limit_bytes=limit * 1024 * 1024),
        cost_estimate=pl.CostEstimate(flops=flops, transcendentals=0, bytes_accessed=1 << 20),
    )(*operands)


def dot_tn(left, right):
    return lax.dot_general(left, right, (((0,), (0,)), ((), ())), preferred_element_type=F32)


def dot_nn(left, right):
    return lax.dot_general(left, right, (((1,), (0,)), ((), ())), preferred_element_type=F32)


def column_norm(values):
    return values * lax.rsqrt(jnp.mean(values * values, axis=0, keepdims=True) + NORM_EPSILON)


def exchanged(shard, axis, groups):
    return lax.all_to_all(shard, axis, 0, 0, axis_index_groups=groups)


def project(ids, pieces, squares, weights, finish, out_shape, extra):
    rows, features = pieces[0].shape
    width = weights[0].shape[0]
    count = len(pieces)

    def body(ids_ref, *refs):
        piece_refs = refs[:count]
        squares_ref = refs[count]
        weight_refs = refs[count + 1 : count + 4]
        extra_refs = refs[count + 4 : count + 4 + len(extra)]
        outs, held = refs[count + 4 + len(extra) : -1], refs[-1]
        for offset, piece_ref in zip(xor_offsets(count), piece_refs):
            start = pl.multiple_of((ids_ref[1] ^ offset) * features, features)
            held[:, pl.ds(start, features)] = piece_ref[...]
        row_scale = lax.rsqrt(squares_ref[...] / width + NORM_EPSILON)
        kept = None
        for index, weight_ref in enumerate(weight_refs):
            product = dot_nn(held[...], weight_ref[...]).T * row_scale
            kept = finish(index, product, extra_refs, outs, kept)

    return vmem_call(
        body,
        out_shape,
        [ids, *pieces, squares, *weights, *extra],
        scalars=1,
        scratch=[pltpu.VMEM((rows, width), BF16)],
        flops=2 * sum(w.shape[1] for w in weights) * rows * width,
        limit=20,
    )


def project_heads(ids, pieces, squares, weights, gains, earlier, head_dim):
    rows = pieces[0].shape[0]
    head_count = weights[0].shape[1] // head_dim
    before = 0 if earlier is None else earlier.shape[2]

    def finish(index, product, extra_refs, outs, kept):
        query_out, pair_out = outs
        if index == 0 and before:
            query_out[:, :, :before] = extra_refs[2][...]
        for head in range(head_count):
            part = product[head * head_dim : (head + 1) * head_dim]
            if index == 0:
                query_out[head, :, before:] = (column_norm(part) * extra_refs[0][...]).astype(BF16)
            elif index == 1:
                pair_out[head, 0:head_dim, :] = (column_norm(part) * extra_refs[1][...]).astype(BF16)
            else:
                pair_out[head, head_dim : 2 * head_dim, :] = part.astype(BF16)

    out_shape = [
        jax.ShapeDtypeStruct((head_count, head_dim, before + rows), BF16),
        jax.ShapeDtypeStruct((head_count, 2 * head_dim, rows), BF16),
    ]
    extra = [*gains] + ([earlier] if before else [])
    return project(ids, pieces, squares, weights, finish, out_shape, extra)


def project_conv(ids, pieces, squares, weights):
    rows = pieces[0].shape[0]
    channels = weights[0].shape[1]

    def finish(index, product, extra_refs, outs, kept):
        if index == 0:
            outs[0][...] = product
        elif index == 1:
            return product
        else:
            outs[1][...] = (kept * product).astype(BF16)

    out_shape = [jax.ShapeDtypeStruct((channels, rows), F32), jax.ShapeDtypeStruct((channels, rows), BF16)]
    return project(ids, pieces, squares, weights, finish, out_shape, [])


def finish_conv(outers, gateds, prior, taps, gain, group, tile_count):
    channels, chunk_rows = gateds[0].shape
    count = len(gateds)
    rows = chunk_rows * count
    tail = prior.shape[1]
    tap_count = taps.shape[1]
    tile_rows = rows // tile_count

    def body(*refs):
        outer_refs, gated_refs = refs[:count], refs[count : 2 * count]
        prior_ref, taps_ref, gain_ref, out = refs[2 * count :]
        lane = lax.broadcasted_iota(jnp.int32, (group, tail), 1)
        for index in range(channels // group):
            span = slice(index * group, (index + 1) * group)
            values = jnp.concatenate([ref[span, :].astype(F32) for ref in gated_refs], axis=1)
            outer = jnp.concatenate([ref[span, :] for ref in outer_refs], axis=1)
            before = prior_ref[span, :].astype(F32)
            weights = taps_ref[span, :]
            total = weights[:, tap_count - 1 : tap_count] * values
            for back in range(1, tap_count):
                moved = pltpu.roll(values, back, 1)
                head = jnp.where(lane < back, pltpu.roll(before, back, 1), moved[:, :tail])
                moved = jnp.concatenate([head, moved[:, tail:]], axis=1)
                total = total + weights[:, tap_count - 1 - back : tap_count - back] * moved
            mixed = (column_norm(outer * total) * gain_ref[span, :]).astype(BF16)
            for tile in range(tile_count):
                out[tile, span, :] = mixed[:, tile * tile_rows : (tile + 1) * tile_rows]

    return vmem_call(
        body,
        jax.ShapeDtypeStruct((tile_count, channels, tile_rows), BF16),
        [*outers, *gateds, prior, taps, gain],
        flops=1 << 20,
    )


def attend(ids, queries, pairs, gates, gain, lane_count, tile_count):
    chunk_count = len(pairs[0])
    slot_count, head_dim, rows = queries.shape
    chunk_rows = rows // chunk_count
    tile_rows = rows // tile_count
    q_tile = min(QUERY_TILE, chunk_rows)
    k_tile = q_tile
    q_tiles = rows // q_tile
    per_chunk = chunk_rows // k_tile
    block_count = slot_count * lane_count
    wide = 2 * head_dim
    inverse_scale = float(head_dim) ** 0.5
    exponent_scale = LOG2_E / inverse_scale
    subtiles = q_tile // tile_rows

    def body(ids_ref, *refs):
        query_ref = refs[0]
        pair_refs = [refs[1 + chunk_count * l : 1 + chunk_count * (l + 1)] for l in range(lane_count)]
        cursor = 1 + chunk_count * lane_count
        gate_refs = refs[cursor : cursor + lane_count]
        gain_ref, out, key_store, value_store, query_store, score_store = refs[cursor + lane_count :]
        own = ids_ref[0]
        own_slot = own // lane_count
        own_lane = own % lane_count
        query_lane = jnp.where(own_slot % 2 == 0, own_lane, lane_count - 1 - own_lane)

        row8 = lax.broadcasted_iota(jnp.int32, (8, k_tile), 0)
        filler = jnp.zeros((head_dim - 8, k_tile), F32)
        for lane in range(lane_count):
            for slot in range(slot_count):
                block = slot * lane_count + (own_lane ^ lane)
                for chunk in range(chunk_count):
                    for part in range(per_chunk):
                        span = slice(part * k_tile, (part + 1) * k_tile)
                        at = chunk * chunk_rows + part * k_tile
                        index = block * q_tiles + chunk * per_chunk + part
                        ref = pair_refs[lane][chunk]
                        gate = gate_refs[lane][pl.ds(own_slot ^ slot, 1), at : at + k_tile] * (-inverse_scale)
                        first = gate.astype(BF16).astype(F32)
                        rest = gate - first
                        second = rest.astype(BF16).astype(F32)
                        third = rest - second
                        gate_rows = jnp.where(row8 == 0, first, jnp.where(row8 == 1, second, jnp.where(row8 == 2, third, 0.0)))
                        stacked = jnp.concatenate([ref[slot, 0:head_dim, span].astype(F32), gate_rows, filler], axis=0)
                        key_store[index] = stacked.T.astype(BF16)
                        value_store[index] = ref[slot, head_dim : 2 * head_dim, span]
        ones = (lax.broadcasted_iota(jnp.int32, (head_dim, q_tile), 0) < 3).astype(F32).astype(BF16)
        for slot in range(slot_count):
            for part in range(q_tiles):
                index = slot * q_tiles + part
                query_store[index, 0:head_dim, :] = query_ref[slot, :, part * q_tile : (part + 1) * q_tile]
                query_store[index, head_dim : 2 * head_dim, :] = ones

        key_at = lax.broadcasted_iota(jnp.int32, (k_tile, q_tile), 0)
        query_at = lax.broadcasted_iota(jnp.int32, (k_tile, q_tile), 1)
        head_gain = gain_ref[own_slot]

        def one_tile(step, _):
            slot = step // q_tiles
            block = slot * lane_count + jnp.where(slot % 2 == 0, query_lane, lane_count - 1 - query_lane)
            index = block * q_tiles + step % q_tiles
            query = query_store[step]

            def score(tile, place, top, masked=False):
                scores = dot_nn(key_store[tile], query)
                if masked:
                    scores = jnp.where(key_at <= query_at, scores, -1e30)
                score_store[place] = scores
                return jnp.maximum(top, jnp.max(scores, axis=0, keepdims=True))

            def absorb(tile, place, old_top, top, total):
                weights = jnp.exp2((score_store[place] - top) * exponent_scale).astype(BF16)
                factor = jnp.exp2((old_top - top) * exponent_scale)
                return total * factor + dot_nn(value_store[tile], weights)

            first = jnp.full((1, q_tile), -1e30, F32)
            total = jnp.zeros((head_dim, q_tile), F32)
            top = score(index, 0, first, True)

            def two_tiles(pair, carry):
                older, old, total = carry
                tile = 2 * pair
                before = jnp.where(pair == 0, index, tile - 1)
                middle = score(tile, 1, old)
                total = absorb(before, 0, older, old, total)
                latest = score(tile + 1, 0, middle)
                total = absorb(tile, 1, old, middle, total)
                return middle, latest, total

            older, old, total = lax.fori_loop(0, index // 2, two_tiles, (first, top, total))
            before = jnp.where(index < 2, index, index // 2 * 2 - 1)

            def odd_end():
                latest = score(index - 1, 1, old)
                return absorb(index - 1, 1, old, latest, absorb(before, 0, older, old, total))

            total = lax.cond(index % 2 == 1, odd_end, lambda: absorb(before, 0, older, old, total))
            mixed = (column_norm(total) * head_gain).astype(BF16)
            for sub in range(subtiles):
                out[step * subtiles + sub] = mixed[:, sub * tile_rows : (sub + 1) * tile_rows]
            return 0

        lax.fori_loop(0, slot_count * q_tiles, one_tile, 0)

    return vmem_call(
        body,
        jax.ShapeDtypeStruct((slot_count * tile_count, head_dim, tile_rows), BF16),
        [ids, queries, *[kv for lane in pairs for kv in lane], *gates, gain],
        scalars=1,
        scratch=[
            pltpu.VMEM((block_count * q_tiles, k_tile, wide), BF16),
            pltpu.VMEM((block_count * q_tiles, head_dim, k_tile), BF16),
            pltpu.VMEM((slot_count * q_tiles, wide, q_tile), BF16),
            pltpu.VMEM((2, k_tile, q_tile), F32),
        ],
        flops=4 * head_dim * slot_count * rows * block_count * rows,
        limit=20,
    )


def output_rows(ids, pieces, weights, base, out_dtype):
    source_count = len(weights)
    piece_count, piece_height, rows = pieces.shape
    slot_count = piece_count // source_count
    height = slot_count * piece_height
    width = weights[0].shape[1]
    offsets = xor_offsets(source_count)
    has_base = base is not None

    def body(ids_ref, piece_ref, *refs):
        weight_refs = refs[:source_count]
        held, out_ref = refs[-1], refs[-2]
        for place, offset in enumerate(offsets):
            source = ids_ref[1] ^ offset
            for slot in range(slot_count):
                start = place * height + slot * piece_height
                held[start : start + piece_height, :] = piece_ref[slot * source_count + source]
        total = refs[source_count][...] if has_base else None
        for place in range(source_count):
            part = dot_tn(held[place * height : (place + 1) * height, :], weight_refs[place][...])
            total = part if total is None else total + part
        out_ref[...] = total.astype(out_dtype)

    return vmem_call(
        body,
        jax.ShapeDtypeStruct((rows, width), out_dtype),
        [ids, pieces, *weights] + ([base] if has_base else []),
        scalars=1,
        scratch=[pltpu.VMEM((source_count * height, rows), BF16)],
        flops=2 * source_count * height * rows * width,
    )


def per_device(
    tokens,
    mix_gain,
    query_weight,
    key_weight,
    value_weight,
    outer_gate_weight,
    inner_gate_weight,
    conv_input_weight,
    query_gain,
    key_gain,
    gate_totals,
    conv_taps,
    attn_out_gain,
    conv_out_gain,
    attn_out_weight,
    conv_out_weight,
):
    rows, features = tokens.shape
    head_dim = query_gain.shape[0]
    head_count = query_weight.shape[1] // head_dim
    sp_count = lax.axis_size("sp")
    tp_count = lax.axis_size("tp")
    lane_count = sp_count // head_count
    sp_index = lax.axis_index("sp")
    tp_index = lax.axis_index("tp")
    ids = jnp.stack([sp_index, tp_index]).astype(jnp.int32)
    chunk_rows = rows // ROW_CHUNKS
    straight = [[slot * lane_count + lane for slot in range(head_count)] for lane in range(lane_count)]
    snaked = [
        [slot * lane_count + (lane_count - 1 - lane if slot % 2 else lane) for slot in range(head_count)]
        for lane in range(lane_count)
    ]
    snaked_wide = [[p * tp_count + t for p in group for t in range(tp_count)] for group in snaked]

    own_gain = lax.dynamic_slice_in_dim(mix_gain, tp_index * features, features, 0)
    scaled = [
        (tokens[c * chunk_rows : (c + 1) * chunk_rows].astype(F32) * own_gain).astype(BF16) for c in range(ROW_CHUNKS)
    ]
    far = []
    for c in range(ROW_CHUNKS):
        far.append(swapped(scaled[c], "tp", tp_count >> 1))
    tokens, gate_totals = lax.optimization_barrier((tokens, gate_totals, *scaled))[:2]
    widened = tokens.astype(F32)
    squares = jnp.sum(widened * widened, axis=1).reshape(1, rows)
    bit = tp_count >> 1
    while bit:
        squares = squares + swapped(squares, "tp", bit)
        bit >>= 1
    gains = (query_gain.reshape(-1, 1), key_gain.reshape(-1, 1))
    far[0], squares, ids, gains = lax.optimization_barrier((far[0], squares, ids, gains))
    chunks = []
    for c in range(ROW_CHUNKS):
        pieces = [scaled[c], far[c]]
        bit = tp_count >> 2
        while bit:
            pieces = pieces + [swapped(piece, "tp", bit) for piece in pieces]
            bit >>= 1
        chunks.append(pieces)

    attn_weight = (query_weight, key_weight, value_weight)
    conv_weight = (outer_gate_weight, inner_gate_weight, conv_input_weight)
    queries, outers, gateds = None, [], []
    pairs = [[] for _ in range(lane_count)]
    for c in range(ROW_CHUNKS):
        chunk_squares = squares[:, c * chunk_rows : (c + 1) * chunk_rows]
        queries, chunk_pairs = project_heads(ids, chunks[c], chunk_squares, attn_weight, gains, queries, head_dim)
        moved = exchanged(chunk_pairs, "sp", straight)
        pairs[0].append(moved)
        for lane in range(1, lane_count):
            pairs[lane].append(swapped(moved, "sp", lane))
    for c in range(ROW_CHUNKS):
        chunk_squares = squares[:, c * chunk_rows : (c + 1) * chunk_rows]
        outer, gated = project_conv(ids, chunks[c], chunk_squares, conv_weight)
        outers.append(outer)
        gateds.append(gated)
    tail = min(128, chunk_rows)
    prior = lax.ppermute(gateds[-1][:, chunk_rows - tail :], "sp", [(i, i + 1) for i in range(sp_count - 1)])
    queries = exchanged(queries, "sp", snaked)

    own_gates = gate_totals.T
    own_slot = sp_index // lane_count
    slot_gates = []
    for offset in range(head_count):
        wanted = lax.dynamic_slice_in_dim(own_gates, own_slot ^ offset, 1, 0)
        slot_gates.append(swapped(wanted, "sp", offset * lane_count) if offset else wanted)
    slot_gates = jnp.concatenate(slot_gates, axis=0)
    gates = [slot_gates]
    for lane in range(1, lane_count):
        gates.append(swapped(slot_gates, "sp", lane))

    attn_out_weight, conv_out_weight = lax.optimization_barrier((attn_out_weight, conv_out_weight, far[-1]))[:2]
    attn_rows = spread(attn_out_weight, "tp")
    conv_rows = spread(conv_out_weight, "tp")

    conv_mixed = finish_conv(
        outers, gateds, prior, conv_taps.T, conv_out_gain.reshape(-1, 1), head_dim, tp_count
    )
    conv_pieces = lax.all_to_all(conv_mixed, "tp", 0, 0)
    base = output_rows(ids, conv_pieces, conv_rows, None, F32)

    attended = attend(ids, queries, pairs, gates, attn_out_gain.reshape(head_count, head_dim, 1), lane_count, tp_count)
    attn_pieces = lax.all_to_all(attended, ("sp", "tp"), 0, 0, axis_index_groups=snaked_wide)
    return output_rows(ids, attn_pieces, attn_rows, base, BF16)


def solution(mesh):
    placed = (
        P("sp", "tp"),
        P(),
        P(None, "tp"),
        P(None, "tp"),
        P(None, "tp"),
        P(None, "tp"),
        P(None, "tp"),
        P(None, "tp"),
        P(),
        P(),
        P("sp", "tp"),
        P(None, "tp"),
        P("tp"),
        P("tp"),
        P("tp", None),
        P("tp", None),
    )
    return jax.shard_map(per_device, mesh=mesh, in_specs=placed, out_specs=P(("sp", "tp"), None), check_vma=False)
```

time: 379 us -> 174 us (0.46)
  waiting for transfers between devices: 243 us -> 47.2 us
  Pallas kernels: 0 us -> 50.8 us
  starting transfers between devices: 3.5 us -> 47.9 us
  blocking collectives: 39.9 us -> 0 us
  matrix products: 25.4 us -> 0 us
  local copies, waits for them, and re-layouts: 39 us -> 23.6 us
  between operations: 13.4 us -> 0.39 us
  loops' own time: 6.15 us -> 0 us
  other arithmetic: 8.24 us -> 2.44 us
    reduce_scatter x1 -> x0, waiting for transfers between devices: 124 us -> none  [per_device(): lax.psum_scatter(jnp.dot(joined, out_weight, preferred_element_type=jnp.f...]
    all_gather x3 -> x0, waiting for transfers between devices: 118 us -> none  [the longest x1 67.1 us: per_device(): piece_values = lax.all_gather(value_rows, 'sp', axis=0, tiled=True)]
    pallas_call x0 -> x8, Pallas kernels: none -> 50.8 us  [vmem_call(): pl.pallas_call(body, out_shape=out_shape, in_specs=specs, out_specs=out_s...]
    all_gather x1 -> x0, blocking collectives: 31.5 us -> none  [per_device(): all_gates = lax.all_gather(gate_totals, 'sp', axis=0, tiled=True)]
    dot_general x4 -> x0, matrix products: 25.4 us -> none  [the longest x1 10 us: per_device(): product = jnp.dot(scaled, stacked, preferred_element_type=jnp.float32)]
    all_to_all x0 -> x5, waiting for transfers between devices: none -> 23.8 us  [the longest x3 13.9 us: exchanged(): return lax.all_to_all(shard, axis, 0, 0, axis_index_groups=groups)]
    ppermute x1 -> x21, waiting for transfers between devices: 0.01 us -> 23.4 us  [the longest x20 22.2 us: swapped(): return lax.ppermute(shard, axis, [(i, i ^ offset) for i in range(devices)])]
    all_to_all x0 -> x5, starting transfers between devices: none -> 22.8 us  [the longest x3 13.3 us: exchanged(): return lax.all_to_all(shard, axis, 0, 0, axis_index_groups=groups)]
  transfers between devices with their start and end apart: 5 -> 26, of which waited for: 4 -> 11; matrix products, arithmetic and copies ran while one was open for 7% -> 2% of each run, Pallas kernels for 0% -> 27%
where the time goes in v1:
time: 174 us; the launch traced here: 172 us
  Pallas kernels  50.8 us (29%)
  starting transfers between devices  47.9 us (28%)
  waiting for transfers between devices  47.2 us (27%)
  local copies, waits for them, and re-layouts  23.6 us (14%)
  other arithmetic  2.44 us (1%)
    pallas_call x8, Pallas kernels, vmem_call(): pl.pallas_call(body, out_shape=out_shape, in_specs=specs, out_specs=out_s...  50.8 us
    ppermute x20, waiting for transfers between devices, swapped(): return lax.ppermute(shard, axis, [(i, i ^ offset) for i in range(devices)])  22.2 us
    ppermute x20, starting transfers between devices, swapped(): return lax.ppermute(shard, axis, [(i, i ^ offset) for i in range(devices)])  21.9 us
    unnamed x81, local copies, waits for them, and re-layouts  20.9 us
    all_to_all x3, waiting for transfers between devices, exchanged(): return lax.all_to_all(shard, axis, 0, 0, axis_index_groups=groups)  13.9 us
    all_to_all x3, starting transfers between devices, exchanged(): return lax.all_to_all(shard, axis, 0, 0, axis_index_groups=groups)  13.3 us
    all_to_all x1, waiting for transfers between devices, per_device(): lax.all_to_all(attended, ('sp', 'tp'), 0, 0, axis_index_groups=snaked_wide)  9.83 us
    all_to_all x1, starting transfers between devices, per_device(): lax.all_to_all(attended, ('sp', 'tp'), 0, 0, axis_index_groups=snaked_wide)  5.74 us
  transfers between devices with their start and end apart: 26, of which 11 were waited for; matrix products, arithmetic and copies ran while one was open for 2% of the time, Pallas kernels for 27%

profile of v1, /device:TPU:0, one launch (start us, length us, event | category | flops | bytes accessed | tf_op | source)
XLA Modules:
  0.0 172.3 jit_solution(685204482577763921)
XLA Ops:
  0.0 0.9 dynamic_slice.15
  0.9 1.4 multiply_convert_fusion
  2.3 3.1 %collective-permute-start = (bf16[512,512]{1,0:T(8,128)(2,1)S(1)}, bf16[512,512]{1,0:T(8,128)(2,1)S(1)}, u32[]{:S(2)}, u32[]{:S(2)}) collective-permute-start(bf16[512,512]{1,0:T(8,128)(2,1)S(1)} %get-tuple-element.40.refs_0_), channel_id=1, source_target_pairs={{0,2},{1,3},{2,0},{3,1},{4,6},{5,7},{6,4},{7,5},{8,10},{9,11},{10,... | collective-permute-start | bytes 1572872 | tf_op jit(solution)/shard_map/ppermute | solution.py:18
  5.8 11.6 %collective-permute-done.1 = f32[1,1024]{1,0:T(1,128)S(1)} collective-permute-done((f32[1,1024]{1,0:T(1,128)S(1)}, f32[1,1024]{1,0:T(1,128)S(1)}, u32[]{:S(2)}, u32[]{:S(2)}) %collective-permute-start.1) | collective-permute-done | bytes 4128 | tf_op jit(solution)/shard_map/ppermute | solution.py:18
  17.5 1.1 collective-permute-done.2
  18.8 1.7 %collective-permute-start.3 = (bf16[512,512]{1,0:T(8,128)(2,1)S(1)}, bf16[512,512]{1,0:T(8,128)(2,1)}, u32[]{:S(2)}, u32[]{:S(2)}) collective-permute-start(bf16[512,512]{1,0:T(8,128)(2,1)S(1)} %get-tuple-element.39.refs_0_), channel_id=1, source_target_pairs={{0,2},{1,3},{2,0},{3,1},{4,6},{5,7},{6,4},{7,5},{8,10},{9,11},{10,... | collective-permute-start | bytes 1572872 | tf_op jit(solution)/shard_map/ppermute | solution.py:18
  20.8 1.2 copy-done.16
  22.0 1.2 copy-done.18
  23.2 4.2 %shard_map.154 = (bf16[4,64,512]{2,1,0:T(8,128)(2,1)S(1)}, bf16[4,128,512]{2,1,0:T(8,128)(2,1)}) custom-call(s32[2]{0:T(128)S(1)} %pad_add_fusion.ids_ref, bf16[512,512]{1,0:T(8,128)(2,1)S(1)} %get-tuple-element.40.refs_0_, bf16[512,512]{1,0:T(8,128)(2,1)S(1)} %collective-permute-done.refs_1_, bf16[512,512]{1,0:T(8,128)(2,1)} %collective-permute-done.6.refs_2_, ...), custom_call_target="tpu_custom_call" | custom-call | flops 1610612736 | bytes 1048576 | tf_op jit(solution)/shard_map/pallas_call | solution.py:44
  27.4 5.0 %all-to-all-start.1 = ((bf16[4,128,512]{2,1,0:T(8,128)(2,1)}), bf16[4,128,512]{2,1,0:T(8,128)(2,1)S(1)}, u32[]{:S(2)}, u32[]{:S(2)}) async-start(bf16[4,128,512]{2,1,0:T(8,128)(2,1)} %get-tuple-element.30), calls=%async_computation.1 | async-start | bytes 1048576 | tf_op jit(solution)/shard_map/all_to_all | solution.py:68
  32.5 0.6 collective-permute-done.3.refs_1_
  33.1 1.3 collective-permute-done.4.refs_2_
  34.4 0.8 collective-permute-done.5.refs_3_
  35.2 1.2 copy-done.15
  36.4 1.2 copy-done.17
  37.7 1.2 copy-done.19
  38.9 4.1 %shard_map.155 = (bf16[4,64,1024]{2,1,0:T(8,128)(2,1)S(1)}, bf16[4,128,512]{2,1,0:T(8,128)(2,1)}) custom-call(s32[2]{0:T(128)S(1)} %pad_add_fusion.ids_ref, bf16[512,512]{1,0:T(8,128)(2,1)S(1)} %get-tuple-element.39.refs_0_, bf16[512,512]{1,0:T(8,128)(2,1)} %collective-permute-done.3.refs_1_, bf16[512,512]{1,0:T(8,128)(2,1)S(1)} %collective-permute-done.4.refs_2_, ...), custom_call_target="tpu_custom_call" | custom-call | flops 1610612736 | bytes 1048576 | tf_op jit(solution)/shard_map/pallas_call | solution.py:44
  43.0 0.8 copy-done.6
  43.8 0.8 copy-done.25
  44.6 0.8 copy-done.27
  45.4 1.9 %all-to-all-done.1.refs_1_ = bf16[4,128,512]{2,1,0:T(8,128)(2,1)S(1)} async-done(((bf16[4,128,512]{2,1,0:T(8,128)(2,1)}), bf16[4,128,512]{2,1,0:T(8,128)(2,1)S(1)}, u32[]{:S(2)}, u32[]{:S(2)}) %all-to-all-start.1) | async-done | bytes 524320 | tf_op jit(solution)/shard_map/all_to_all | solution.py:68
  47.3 4.1 %all-to-all-start.2 = ((bf16[4,128,512]{2,1,0:T(8,128)(2,1)}), bf16[4,128,512]{2,1,0:T(8,128)(2,1)}, u32[]{:S(2)}, u32[]{:S(2)}) async-start(bf16[4,128,512]{2,1,0:T(8,128)(2,1)} %get-tuple-element.31), calls=%async_computation.2 | async-start | bytes 1048576 | tf_op jit(solution)/shard_map/all_to_all | solution.py:68
  51.4 1.6 collective-permute-start.14
  53.0 0.5 collective-permute-start.18
  53.5 12.1 %all-to-all-done.2.refs_2_ = bf16[4,128,512]{2,1,0:T(8,128)(2,1)} async-done(((bf16[4,128,512]{2,1,0:T(8,128)(2,1)}), bf16[4,128,512]{2,1,0:T(8,128)(2,1)}, u32[]{:S(2)}, u32[]{:S(2)}) %all-to-all-start.2) | async-done | bytes 524320 | tf_op jit(solution)/shard_map/all_to_all | solution.py:68
  65.6 4.1 %all-to-all-start = ((bf16[4,64,1024]{2,1,0:T(8,128)(2,1)}), bf16[4,64,1024]{2,1,0:T(8,128)(2,1)}, u32[]{:S(2)}, u32[]{:S(2)}) async-start(bf16[4,64,1024]{2,1,0:T(8,128)(2,1)} %copy-done.6), calls=%async_computation | async-start | bytes 1048576 | tf_op jit(solution)/shard_map/all_to_all | solution.py:68
  69.8 1.6 collective-permute-start.8
  71.4 0.5 collective-permute-start.9
  71.9 0.6 dynamic-slice_bitcast_fusion.3
  72.5 4.6 %collective-permute-start.12 = (f32[1,1024]{1,0:T(1,128)S(1)}, f32[1,1024]{1,0:T(1,128)S(1)}, u32[]{:S(2)}, u32[]{:S(2)}) collective-permute-start(f32[1,1024]{1,0:T(1,128)S(1)} %get-tuple-element.42), channel_id=1, source_target_pairs={{0,24},{4,28},{8,16},{12,20},{16,8},{20,12},{24,0},{28,4},{1,25},{... | collective-permute-start | bytes 12296 | tf_op jit(solution)/shard_map/ppermute | solution.py:18
  77.1 5.8 %collective-permute-done.12 = f32[1,1024]{1,0:T(1,128)S(1)} collective-permute-done((f32[1,1024]{1,0:T(1,128)S(1)}, f32[1,1024]{1,0:T(1,128)S(1)}, u32[]{:S(2)}, u32[]{:S(2)}) %collective-permute-start.12) | collective-permute-done | bytes 4128 | tf_op jit(solution)/shard_map/ppermute | solution.py:18
  82.9 0.6 copy-done.35
  83.5 2.5 %collective-permute-start.11 = (f32[1,1024]{1,0:T(1,128)S(1)}, f32[1,1024]{1,0:T(1,128)}, u32[]{:S(2)}, u32[]{:S(2)}) collective-permute-start(f32[1,1024]{1,0:T(1,128)S(1)} %get-tuple-element.43), channel_id=1, source_target_pairs={{0,16},{4,20},{8,24},{12,28},{16,0},{20,4},{24,8},{28,12},{1,17},{... | collective-permute-start | bytes 12296 | tf_op jit(solution)/shard_map/ppermute | solution.py:18
  86.4 0.8 copy.28.refs_6_
  87.2 0.9 collective-permute-done.11
  88.1 1.8 %collective-permute-start.10 = (f32[1,1024]{1,0:T(1,128)S(1)}, f32[1,1024]{1,0:T(1,128)S(1)}, u32[]{:S(2)}, u32[]{:S(2)}) collective-permute-start(f32[1,1024]{1,0:T(1,128)S(1)} %get-tuple-element.44), channel_id=1, source_target_pairs={{0,8},{4,12},{8,0},{12,4},{16,24},{20,28},{24,16},{28,20},{1,9},{5... | collective-permute-start | bytes 12296 | tf_op jit(solution)/shard_map/ppermute | solution.py:18
  90.0 1.2 copy-done.20
  91.2 1.2 copy-done.21
  92.4 1.2 copy-done.22
  93.7 1.0 copy-done.26
  94.7 1.0 copy-done.28
  95.7 3.3 %shard_map.158 = (f32[256,512]{1,0:T(8,128)S(1)}, bf16[256,512]{1,0:T(8,128)(2,1)S(1)}) custom-call(s32[2]{0:T(128)S(1)} %pad_add_fusion.ids_ref, bf16[512,512]{1,0:T(8,128)(2,1)S(1)} %get-tuple-element.39.refs_0_, bf16[512,512]{1,0:T(8,128)(2,1)} %collective-permute-done.3.refs_1_, bf16[512,512]{1,0:T(8,128)(2,1)S(1)} %copy-done.26, ...), custom_call_target="tpu_custom_call" | custom-call | flops 1610612736 | bytes 1048576 | tf_op jit(solution)/shard_map/pallas_call | solution.py:44
  99.1 3.1 %collective-permute-start.17 = (bf16[256,128]{1,0:T(8,128)(2,1)S(1)}, bf16[256,128]{1,0:T(8,128)(2,1)S(1)}, u32[]{:S(2)}, u32[]{:S(2)}) collective-permute-start(bf16[256,128]{1,0:T(8,128)(2,1)S(1)} %slice.21), channel_id=1, source_target_pairs={{0,4},{4,8},{8,12},{12,16},{16,20},{20,24},{24,28},{1,5},{5,9},{9,... | collective-permute-start | bytes 196616 | tf_op jit(solution)/shard_map/ppermute | solution.py:410
  102.2 0.7 pad_maximum_fusion.refs_5_
  102.9 1.2 collective-permute-done.17.refs_4_
  104.1 2.5 %collective-permute-start.13 = (f32[4,1024]{1,0:T(4,128)S(1)}, f32[4,1024]{1,0:T(4,128)S(1)}, u32[]{:S(2)}, u32[]{:S(2)}) collective-permute-start(f32[4,1024]{1,0:T(4,128)S(1)} %pad_maximum_fusion.refs_5_), channel_id=1, source_target_pairs={{0,4},{4,0},{8,12},{12,8},{16,20},{20,16},{24,28},{28,24},{1,5},{5... | collective-permute-start | bytes 49160 | tf_op jit(solution)/shard_map/ppermute | solution.py:18
  106.6 0.6 copy-done.9
  107.2 3.4 %shard_map.157 = (f32[256,512]{1,0:T(8,128)S(1)}, bf16[256,512]{1,0:T(8,128)(2,1)S(1)}) custom-call(s32[2]{0:T(128)S(1)} %copy-done.9, bf16[512,512]{1,0:T(8,128)(2,1)S(1)} %get-tuple-element.40.refs_0_, bf16[512,512]{1,0:T(8,128)(2,1)S(1)} %copy-done.24, bf16[512,512]{1,0:T(8,128)(2,1)} %collective-permute-done.6.refs_2_, ...), custom_call_target="tpu_custom_call" | custom-call | flops 1610612736 | bytes 1048576 | tf_op jit(solution)/shard_map/pallas_call | solution.py:44
  110.6 1.7 %shard_map.159 = bf16[4,256,256]{2,1,0:T(8,128)(2,1)} custom-call(f32[256,512]{1,0:T(8,128)S(1)} %get-tuple-element.34.refs_0_, f32[256,512]{1,0:T(8,128)S(1)} %get-tuple-element.35.refs_1_, bf16[256,512]{1,0:T(8,128)(2,1)S(1)} %get-tuple-element.36.refs_2_, bf16[256,512]{1,0:T(8,128)(2,1)S(1)} %get-tuple-element.37.refs_3_, ...), custom_call_target="tpu_custom_call" | custom-call | flops 1048576 | bytes 1048576 | tf_op jit(solution)/shard_map/pallas_call | solution.py:44
  112.4 0.6 copy-done.29
  113.0 0.5 collective-permute-start.19
  113.5 3.8 %all-to-all-start.4 = ((bf16[4,256,256]{2,1,0:T(8,128)(2,1)}), bf16[4,256,256]{2,1,0:T(8,128)(2,1)S(1)}, u32[]{:S(2)}, u32[]{:S(2)}) async-start(bf16[4,256,256]{2,1,0:T(8,128)(2,1)} %shard_map.159), calls=%async_computation.4 | async-start | bytes 1048576 | tf_op jit(solution)/shard_map/all_to_all | solution.py:431
  117.3 0.3 collective-permute-start.16
  117.6 0.3 collective-permute-start.20
  117.9 0.6 copy-done.10
  118.5 0.7 copy-done.30
  119.2 26.9 %shard_map.156 = bf16[16,64,256]{2,1,0:T(8,128)(2,1)S(1)} custom-call(s32[2]{0:T(128)S(1)} %copy-done.10, bf16[4,64,1024]{2,1,0:T(8,128)(2,1)} %all-to-all-done.refs_0_, bf16[4,128,512]{2,1,0:T(8,128)(2,1)S(1)} %copy-done.5, bf16[4,128,512]{2,1,0:T(8,128)(2,1)} %all-to-all-done.2.refs_2_, bf16[4,128,512]{2,1,0:T(8,128)(2,1)} %collective-permute-done.8.refs_3_, ...), custom_call_target="tpu_custom_call" | custom-call | flops 8589934592 | bytes 1048576 | tf_op jit(solution)/shard_map/pallas_call | solution.py:44
  146.2 0.8 copy-done.7
  147.0 5.7 %all-to-all-start.3 = ((bf16[16,64,256]{2,1,0:T(8,128)(2,1)}), bf16[16,64,256]{2,1,0:T(8,128)(2,1)S(1)}, u32[]{:S(2)}, u32[]{:S(2)}) async-start(bf16[16,64,256]{2,1,0:T(8,128)(2,1)} %copy-done.7), calls=%async_computation.3 | async-start | bytes 1048576 | tf_op jit(solution)/shard_map/all_to_all | solution.py:435
  152.8 1.2 copy-done.1
  154.0 1.2 copy-done.3
  155.2 2.8 %shard_map.160.refs_4_ = f32[256,2048]{1,0:T(8,128)S(1)} custom-call(s32[2]{0:T(128)S(1)} %copy-done.11, bf16[4,256,256]{2,1,0:T(8,128)(2,1)S(1)} %all-to-all-done.4.piece_ref, bf16[256,2048]{1,0:T(8,128)(2,1)S(1)} %copy-done.1, bf16[256,2048]{1,0:T(8,128)(2,1)S(1)} %copy-done.3, bf16[256,2048]{1,0:T(8,128)(2,1)} %collective-permute-done.19.refs_2_, ...), custom_call_target="tpu_custom_call" | custom-call | flops 1073741824 | bytes 1048576 | tf_op jit(solution)/shard_map/pallas_call | solution.py:44
  158.1 9.8 %all-to-all-done.3.piece_ref = bf16[16,64,256]{2,1,0:T(8,128)(2,1)S(1)} async-done(((bf16[16,64,256]{2,1,0:T(8,128)(2,1)}), bf16[16,64,256]{2,1,0:T(8,128)(2,1)S(1)}, u32[]{:S(2)}, u32[]{:S(2)}) %all-to-all-start.3) | async-done | bytes 524320 | tf_op jit(solution)/shard_map/all_to_all | solution.py:435
  167.9 4.4 %shard_map.161 = bf16[256,2048]{1,0:T(8,128)(2,1)} custom-call(s32[2]{0:T(128)S(1)} %copy-done.11, bf16[16,64,256]{2,1,0:T(8,128)(2,1)S(1)} %all-to-all-done.3.piece_ref, bf16[256,2048]{1,0:T(8,128)(2,1)} %refs_0_.1, bf16[256,2048]{1,0:T(8,128)(2,1)} %collective-permute-done.14.refs_1_, bf16[256,2048]{1,0:T(8,128)(2,1)} %collective-permute-done.15.refs_2_, ...), custom_call_target="tpu_custom_call" | custom-call | flops 1073741824 | bytes 1048576 | tf_op jit(solution)/shard_map/pallas_call | solution.py:44
  (91 shorter events, 1.4 us)
Async XLA Ops:
  0.0 20.7 %copy-start.39 = (f32[64]{0:T(128)S(1)}, f32[64]{0:T(128)}, u32[]{:S(2)}) copy-start(f32[64]{0:T(128)} %param.25) | copy-start | bytes 772
  0.0 20.6 %copy-start.38 = (f32[64]{0:T(128)S(1)}, f32[64]{0:T(128)}, u32[]{:S(2)}) copy-start(f32[64]{0:T(128)} %param.24) | copy-start | bytes 772
  0.0 20.8 %copy-start.14 = (bf16[2048,256]{1,0:T(8,128)(2,1)S(1)}, bf16[2048,256]{1,0:T(8,128)(2,1)}, u32[]{:S(2)}) copy-start(bf16[2048,256]{1,0:T(8,128)(2,1)} %refs_5_.5) | copy-start | bytes 3145732
  0.0 5.4 %copy-start.31 = (bf16[1024,512]{1,0:T(8,128)(2,1)S(1)}, bf16[1024,512]{1,0:T(8,128)(2,1)}, u32[]{:S(2)}) copy-start(bf16[1024,512]{1,0:T(8,128)(2,1)} %param.16) | copy-start | bytes 3145732
  2.3 16.2 %collective-permute-start = (bf16[512,512]{1,0:T(8,128)(2,1)S(1)}, bf16[512,512]{1,0:T(8,128)(2,1)S(1)}, u32[]{:S(2)}, u32[]{:S(2)}) collective-permute-start(bf16[512,512]{1,0:T(8,128)(2,1)S(1)} %get-tuple-element.40.refs_0_), channel_id=1, source_target_pairs={{0,2},{1,3},{2,0},{3,1},{4,6},{5,7},{6,4},{7,5},{8,10},{9,11},{10,... | collective-permute-start | bytes 1572872 | tf_op jit(solution)/shard_map/ppermute | solution.py:18
  5.6 11.7 %collective-permute-start.1 = (f32[1,1024]{1,0:T(1,128)S(1)}, f32[1,1024]{1,0:T(1,128)S(1)}, u32[]{:S(2)}, u32[]{:S(2)}) collective-permute-start(f32[1,1024]{1,0:T(1,128)S(1)} %bitcast.16), channel_id=1, source_target_pairs={{0,2},{1,3},{2,0},{3,1},{4,6},{5,7},{6,4},{7,5},{8,10},{9,11},{10,... | collective-permute-start | bytes 12296 | tf_op jit(solution)/shard_map/ppermute | solution.py:18
  5.7 15.0 %collective-permute-start.6 = (bf16[512,512]{1,0:T(8,128)(2,1)S(1)}, bf16[512,512]{1,0:T(8,128)(2,1)}, u32[]{:S(2)}, u32[]{:S(2)}) collective-permute-start(bf16[512,512]{1,0:T(8,128)(2,1)S(1)} %get-tuple-element.40.refs_0_), channel_id=1, source_target_pairs={{0,1},{1,0},{2,3},{3,2},{4,5},{5,4},{6,7},{7,6},{8,9},{9,8},{10,11... | collective-permute-start | bytes 1572872 | tf_op jit(solution)/shard_map/ppermute | solution.py:18
  17.4 1.2 collective-permute-start.2
  17.5 72.5 %copy-start.8 = (s32[2]{0:T(128)}, s32[2]{0:T(128)S(1)}, u32[]{:S(2)}) copy-start(s32[2]{0:T(128)S(1)} %pad_add_fusion.ids_ref) | copy-start | bytes 28
  18.6 8.9 %copy-start.23 = (bf16[512,512]{1,0:T(8,128)(2,1)}, bf16[512,512]{1,0:T(8,128)(2,1)S(1)}, u32[]{:S(2)}) copy-start(bf16[512,512]{1,0:T(8,128)(2,1)S(1)} %collective-permute-done.refs_1_) | copy-start | bytes 1572868
  18.6 2.2 %collective-permute-start.7 = (bf16[512,512]{1,0:T(8,128)(2,1)S(1)}, bf16[512,512]{1,0:T(8,128)(2,1)}, u32[]{:S(2)}, u32[]{:S(2)}) collective-permute-start(bf16[512,512]{1,0:T(8,128)(2,1)S(1)} %collective-permute-done.refs_1_), channel_id=1, source_target_pairs={{0,1},{1,0},{2,3},{3,2},{4,5},{5,4},{6,7},{7,6},{8,9},{9,8},{10,11... | collective-permute-start | bytes 1572872 | tf_op jit(solution)/shard_map/ppermute | solution.py:18
  18.8 14.3 %collective-permute-start.3 = (bf16[512,512]{1,0:T(8,128)(2,1)S(1)}, bf16[512,512]{1,0:T(8,128)(2,1)}, u32[]{:S(2)}, u32[]{:S(2)}) collective-permute-start(bf16[512,512]{1,0:T(8,128)(2,1)S(1)} %get-tuple-element.39.refs_0_), channel_id=1, source_target_pairs={{0,2},{1,3},{2,0},{3,1},{4,6},{5,7},{6,4},{7,5},{8,10},{9,11},{10,... | collective-permute-start | bytes 1572872 | tf_op jit(solution)/shard_map/ppermute | solution.py:18
  20.7 6.7 %copy-start.12 = (f32[1,512]{1,0:T(1,128)}, f32[1,512]{1,0:T(1,128)S(1)}, u32[]{:S(2)}) copy-start(f32[1,512]{1,0:T(1,128)S(1)} %get-tuple-element.45.refs_4_) | copy-start | bytes 6148
  20.8 1.2 copy-start.16
  22.0 1.2 copy-start.18
  27.4 19.8 %all-to-all-start.1 = ((bf16[4,128,512]{2,1,0:T(8,128)(2,1)}), bf16[4,128,512]{2,1,0:T(8,128)(2,1)S(1)}, u32[]{:S(2)}, u32[]{:S(2)}) async-start(bf16[4,128,512]{2,1,0:T(8,128)(2,1)} %get-tuple-element.30), calls=%async_computation.1 | async-start | bytes 1048576 | tf_op jit(solution)/shard_map/all_to_all | solution.py:68
  32.5 1.9 %collective-permute-start.4 = (bf16[512,512]{1,0:T(8,128)(2,1)S(1)}, bf16[512,512]{1,0:T(8,128)(2,1)S(1)}, u32[]{:S(2)}, u32[]{:S(2)}) collective-permute-start(bf16[512,512]{1,0:T(8,128)(2,1)S(1)} %get-tuple-element.39.refs_0_), channel_id=1, source_target_pairs={{0,1},{1,0},{2,3},{3,2},{4,5},{5,4},{6,7},{7,6},{8,9},{9,8},{10,11... | collective-permute-start | bytes 1572872 | tf_op jit(solution)/shard_map/ppermute | solution.py:18
  33.1 2.1 %collective-permute-start.5 = (bf16[512,512]{1,0:T(8,128)(2,1)}, bf16[512,512]{1,0:T(8,128)(2,1)S(1)}, u32[]{:S(2)}, u32[]{:S(2)}) collective-permute-start(bf16[512,512]{1,0:T(8,128)(2,1)} %collective-permute-done.3.refs_1_), channel_id=1, source_target_pairs={{0,1},{1,0},{2,3},{3,2},{4,5},{5,4},{6,7},{7,6},{8,9},{9,8},{10,11... | collective-permute-start | bytes 1572872 | tf_op jit(solution)/shard_map/ppermute | solution.py:18
  35.2 1.2 copy-start.15
  36.4 1.2 copy-start.17
  37.7 1.2 copy-start.19
  38.9 14.1 %copy-start = (bf16[256,2048]{1,0:T(8,128)(2,1)S(1)}, bf16[256,2048]{1,0:T(8,128)(2,1)}, u32[]{:S(2)}) copy-start(bf16[256,2048]{1,0:T(8,128)(2,1)} %refs_0_) | copy-start | bytes 3145732
  43.0 0.8 copy-start.6
  43.8 0.8 copy-start.25
  44.6 0.8 copy-start.27
  45.4 26.4 %copy-start.32 = (f32[1024,4]{0,1:T(4,128)S(1)}, f32[1024,4]{0,1:T(4,128)}, u32[]{:S(2)}) copy-start(f32[1024,4]{0,1:T(4,128)} %param.26) | copy-start | bytes 49156
  45.4 40.6 %copy-start.34 = (f32[3,256]{1,0:T(4,128)S(1)}, f32[3,256]{1,0:T(4,128)}, u32[]{:S(2)}) copy-start(f32[3,256]{1,0:T(4,128)} %param.27) | copy-start | bytes 9220
  45.4 40.8 %copy-start.37 = (f32[256]{0:T(256)S(1)}, f32[256]{0:T(256)}, u32[]{:S(2)}) copy-start(f32[256]{0:T(256)} %param.28) | copy-start | bytes 3076
  47.3 4.1 %copy-start.4 = (bf16[4,128,512]{2,1,0:T(8,128)(2,1)}, bf16[4,128,512]{2,1,0:T(8,128)(2,1)S(1)}, u32[]{:S(2)}) copy-start(bf16[4,128,512]{2,1,0:T(8,128)(2,1)S(1)} %all-to-all-done.1.refs_1_) | copy-start | bytes 1572868
  47.3 18.3 %all-to-all-start.2 = ((bf16[4,128,512]{2,1,0:T(8,128)(2,1)}), bf16[4,128,512]{2,1,0:T(8,128)(2,1)}, u32[]{:S(2)}, u32[]{:S(2)}) async-start(bf16[4,128,512]{2,1,0:T(8,128)(2,1)} %get-tuple-element.31), calls=%async_computation.2 | async-start | bytes 1048576 | tf_op jit(solution)/shard_map/all_to_all | solution.py:68
  51.4 61.6 %collective-permute-start.14 = (bf16[256,2048]{1,0:T(8,128)(2,1)}, bf16[256,2048]{1,0:T(8,128)(2,1)}, u32[]{:S(2)}, u32[]{:S(2)}) collective-permute-start(bf16[256,2048]{1,0:T(8,128)(2,1)} %refs_0_.1), channel_id=1, source_target_pairs={{0,2},{1,3},{2,0},{3,1},{4,6},{5,7},{6,4},{7,5},{8,10},{9,11},{10,... | collective-permute-start | bytes 3145736 | tf_op jit(solution)/shard_map/ppermute | solution.py:18
  53.0 64.3 %collective-permute-start.18 = (bf16[256,2048]{1,0:T(8,128)(2,1)S(1)}, bf16[256,2048]{1,0:T(8,128)(2,1)S(1)}, u32[]{:S(2)}, u32[]{:S(2)}) collective-permute-start(bf16[256,2048]{1,0:T(8,128)(2,1)S(1)} %copy-done), channel_id=1, source_target_pairs={{0,2},{1,3},{2,0},{3,1},{4,6},{5,7},{6,4},{7,5},{8,10},{9,11},{10,... | collective-permute-start | bytes 3145736 | tf_op jit(solution)/shard_map/ppermute | solution.py:18
  65.6 47.9 %all-to-all-start = ((bf16[4,64,1024]{2,1,0:T(8,128)(2,1)}), bf16[4,64,1024]{2,1,0:T(8,128)(2,1)}, u32[]{:S(2)}, u32[]{:S(2)}) async-start(bf16[4,64,1024]{2,1,0:T(8,128)(2,1)} %copy-done.6), calls=%async_computation | async-start | bytes 1048576 | tf_op jit(solution)/shard_map/all_to_all | solution.py:68
  69.8 47.8 %collective-permute-start.8 = (bf16[4,128,512]{2,1,0:T(8,128)(2,1)}, bf16[4,128,512]{2,1,0:T(8,128)(2,1)}, u32[]{:S(2)}, u32[]{:S(2)}) collective-permute-start(bf16[4,128,512]{2,1,0:T(8,128)(2,1)} %copy-done.4), channel_id=1, source_target_pairs={{0,4},{4,0},{8,12},{12,8},{16,20},{20,16},{24,28},{28,24},{1,5},{5... | collective-permute-start | bytes 1572872 | tf_op jit(solution)/shard_map/ppermute | solution.py:18
  71.4 46.5 %collective-permute-start.9 = (bf16[4,128,512]{2,1,0:T(8,128)(2,1)}, bf16[4,128,512]{2,1,0:T(8,128)(2,1)}, u32[]{:S(2)}, u32[]{:S(2)}) collective-permute-start(bf16[4,128,512]{2,1,0:T(8,128)(2,1)} %all-to-all-done.2.refs_2_), channel_id=1, source_target_pairs={{0,4},{4,0},{8,12},{12,8},{16,20},{20,16},{24,28},{28,24},{1,5},{5... | collective-permute-start | bytes 1572872 | tf_op jit(solution)/shard_map/ppermute | solution.py:18
  72.5 10.5 %collective-permute-start.12 = (f32[1,1024]{1,0:T(1,128)S(1)}, f32[1,1024]{1,0:T(1,128)S(1)}, u32[]{:S(2)}, u32[]{:S(2)}) collective-permute-start(f32[1,1024]{1,0:T(1,128)S(1)} %get-tuple-element.42), channel_id=1, source_target_pairs={{0,24},{4,28},{8,16},{12,20},{16,8},{20,12},{24,0},{28,4},{1,25},{... | collective-permute-start | bytes 12296 | tf_op jit(solution)/shard_map/ppermute | solution.py:18
  83.5 4.6 %collective-permute-start.11 = (f32[1,1024]{1,0:T(1,128)S(1)}, f32[1,1024]{1,0:T(1,128)}, u32[]{:S(2)}, u32[]{:S(2)}) collective-permute-start(f32[1,1024]{1,0:T(1,128)S(1)} %get-tuple-element.43), channel_id=1, source_target_pairs={{0,16},{4,20},{8,24},{12,28},{16,0},{20,4},{24,8},{28,12},{1,17},{... | collective-permute-start | bytes 12296 | tf_op jit(solution)/shard_map/ppermute | solution.py:18
  88.1 18.5 %copy-start.13 = (f32[1,512]{1,0:T(1,128)S(1)}, f32[1,512]{1,0:T(1,128)}, u32[]{:S(2)}) copy-start(f32[1,512]{1,0:T(1,128)} %copy-done.12) | copy-start | bytes 6148
  88.1 10.9 %collective-permute-start.10 = (f32[1,1024]{1,0:T(1,128)S(1)}, f32[1,1024]{1,0:T(1,128)S(1)}, u32[]{:S(2)}, u32[]{:S(2)}) collective-permute-start(f32[1,1024]{1,0:T(1,128)S(1)} %get-tuple-element.44), channel_id=1, source_target_pairs={{0,8},{4,12},{8,0},{12,4},{16,24},{20,28},{24,16},{28,20},{1,9},{5... | collective-permute-start | bytes 12296 | tf_op jit(solution)/shard_map/ppermute | solution.py:18
  90.0 1.2 copy-start.20
  91.2 1.2 copy-start.21
  92.4 1.2 copy-start.22
  93.7 1.0 copy-start.26
  94.7 1.0 copy-start.28
  95.7 6.5 %copy-start.33 = (f32[1,1024]{1,0:T(1,128)S(1)}, f32[1,1024]{1,0:T(1,128)}, u32[]{:S(2)}) copy-start(f32[1,1024]{1,0:T(1,128)} %get-tuple-element.41) | copy-start | bytes 12292
  95.7 6.5 %copy-start.36 = (f32[1,1024]{1,0:T(1,128)S(1)}, f32[1,1024]{1,0:T(1,128)}, u32[]{:S(2)}) copy-start(f32[1,1024]{1,0:T(1,128)} %copy-done.35) | copy-start | bytes 12292
  95.7 10.9 %copy-start.24 = (bf16[512,512]{1,0:T(8,128)(2,1)S(1)}, bf16[512,512]{1,0:T(8,128)(2,1)}, u32[]{:S(2)}) copy-start(bf16[512,512]{1,0:T(8,128)(2,1)} %copy-done.23) | copy-start | bytes 1572868
  99.1 5.1 %collective-permute-start.17 = (bf16[256,128]{1,0:T(8,128)(2,1)S(1)}, bf16[256,128]{1,0:T(8,128)(2,1)S(1)}, u32[]{:S(2)}, u32[]{:S(2)}) collective-permute-start(bf16[256,128]{1,0:T(8,128)(2,1)S(1)} %slice.21), channel_id=1, source_target_pairs={{0,4},{4,8},{8,12},{12,16},{16,20},{20,24},{24,28},{1,5},{5,9},{9,... | collective-permute-start | bytes 196616 | tf_op jit(solution)/shard_map/ppermute | solution.py:410
  104.1 8.2 %collective-permute-start.13 = (f32[4,1024]{1,0:T(4,128)S(1)}, f32[4,1024]{1,0:T(4,128)S(1)}, u32[]{:S(2)}, u32[]{:S(2)}) collective-permute-start(f32[4,1024]{1,0:T(4,128)S(1)} %pad_maximum_fusion.refs_5_), channel_id=1, source_target_pairs={{0,4},{4,0},{8,12},{12,8},{16,20},{20,16},{24,28},{28,24},{1,5},{5... | collective-permute-start | bytes 49160 | tf_op jit(solution)/shard_map/ppermute | solution.py:18
  106.6 0.6 copy-start.9
  110.6 7.3 %copy-start.5 = (bf16[4,128,512]{2,1,0:T(8,128)(2,1)S(1)}, bf16[4,128,512]{2,1,0:T(8,128)(2,1)}, u32[]{:S(2)}) copy-start(bf16[4,128,512]{2,1,0:T(8,128)(2,1)} %copy-done.4) | copy-start | bytes 1572868
  113.0 45.1 %collective-permute-start.15 = (bf16[256,2048]{1,0:T(8,128)(2,1)}, bf16[256,2048]{1,0:T(8,128)(2,1)}, u32[]{:S(2)}, u32[]{:S(2)}) collective-permute-start(bf16[256,2048]{1,0:T(8,128)(2,1)} %refs_0_.1), channel_id=1, source_target_pairs={{0,1},{1,0},{2,3},{3,2},{4,5},{5,4},{6,7},{7,6},{8,9},{9,8},{10,11... | collective-permute-start | bytes 3145736 | tf_op jit(solution)/shard_map/ppermute | solution.py:18
  113.0 39.7 %collective-permute-start.19 = (bf16[256,2048]{1,0:T(8,128)(2,1)S(1)}, bf16[256,2048]{1,0:T(8,128)(2,1)}, u32[]{:S(2)}, u32[]{:S(2)}) collective-permute-start(bf16[256,2048]{1,0:T(8,128)(2,1)S(1)} %copy-done), channel_id=1, source_target_pairs={{0,1},{1,0},{2,3},{3,2},{4,5},{5,4},{6,7},{7,6},{8,9},{9,8},{10,11... | collective-permute-start | bytes 3145736 | tf_op jit(solution)/shard_map/ppermute | solution.py:18
  113.5 39.3 %copy-start.11 = (s32[2]{0:T(128)S(1)}, s32[2]{0:T(128)}, u32[]{:S(2)}) copy-start(s32[2]{0:T(128)} %copy-done.8) | copy-start | bytes 28
  113.5 33.5 %all-to-all-start.4 = ((bf16[4,256,256]{2,1,0:T(8,128)(2,1)}), bf16[4,256,256]{2,1,0:T(8,128)(2,1)S(1)}, u32[]{:S(2)}, u32[]{:S(2)}) async-start(bf16[4,256,256]{2,1,0:T(8,128)(2,1)} %shard_map.159), calls=%async_computation.4 | async-start | bytes 1048576 | tf_op jit(solution)/shard_map/all_to_all | solution.py:431
  117.3 28.9 %copy-start.2 = (bf16[256,2048]{1,0:T(8,128)(2,1)}, bf16[256,2048]{1,0:T(8,128)(2,1)S(1)}, u32[]{:S(2)}) copy-start(bf16[256,2048]{1,0:T(8,128)(2,1)S(1)} %collective-permute-done.18.refs_1_) | copy-start | bytes 3145732
  117.3 40.7 %collective-permute-start.16 = (bf16[256,2048]{1,0:T(8,128)(2,1)}, bf16[256,2048]{1,0:T(8,128)(2,1)}, u32[]{:S(2)}, u32[]{:S(2)}) collective-permute-start(bf16[256,2048]{1,0:T(8,128)(2,1)} %collective-permute-done.14.refs_1_), channel_id=1, source_target_pairs={{0,1},{1,0},{2,3},{3,2},{4,5},{5,4},{6,7},{7,6},{8,9},{9,8},{10,11... | collective-permute-start | bytes 3145736 | tf_op jit(solution)/shard_map/ppermute | solution.py:18
  117.6 35.2 %collective-permute-start.20 = (bf16[256,2048]{1,0:T(8,128)(2,1)S(1)}, bf16[256,2048]{1,0:T(8,128)(2,1)}, u32[]{:S(2)}, u32[]{:S(2)}) collective-permute-start(bf16[256,2048]{1,0:T(8,128)(2,1)S(1)} %collective-permute-done.18.refs_1_), channel_id=1, source_target_pairs={{0,1},{1,0},{2,3},{3,2},{4,5},{5,4},{6,7},{7,6},{8,9},{9,8},{10,11... | collective-permute-start | bytes 3145736 | tf_op jit(solution)/shard_map/ppermute | solution.py:18
  117.9 0.6 copy-start.10
  118.5 0.7 copy-start.30
  146.2 0.8 copy-start.7
  147.0 20.9 %all-to-all-start.3 = ((bf16[16,64,256]{2,1,0:T(8,128)(2,1)}), bf16[16,64,256]{2,1,0:T(8,128)(2,1)S(1)}, u32[]{:S(2)}, u32[]{:S(2)}) async-start(bf16[16,64,256]{2,1,0:T(8,128)(2,1)} %copy-done.7), calls=%async_computation.3 | async-start | bytes 1048576 | tf_op jit(solution)/shard_map/all_to_all | solution.py:435
  152.8 1.2 copy-start.1
  154.0 1.2 copy-start.3
  (2 other events, 1.2 us)

commit v2 on v1

v2 whole, which is shorter than its diff:
```python
import jax
import jax.numpy as jnp
from jax import lax
from jax.experimental import pallas as pl
from jax.experimental.pallas import tpu as pltpu
from jax.sharding import PartitionSpec as P

NORM_EPSILON = 1e-06
LOG2_E = 1.4426950408889634
ROW_CHUNKS = 2
QUERY_TILE = 512
OUTPUT_PARTS = 4
F32 = jnp.float32
BF16 = jnp.bfloat16


def swapped(shard, axis, offset):
    devices = lax.axis_size(axis)
    return lax.ppermute(shard, axis, [(i, i ^ offset) for i in range(devices)])


def xor_offsets(count):
    offsets = [0]
    bit = count >> 1
    while bit:
        offsets = offsets + [o ^ bit for o in offsets]
        bit >>= 1
    return offsets


def in_hbm(x):
    return pltpu.with_memory_space_constraint(x, pltpu.HBM) if x.size >= 1 << 14 else x


def vmem_call(body, out_shape, operands, scalars=0, scratch=(), flops=0, limit=16, outside=(), resident=(), out_space=pltpu.VMEM):
    specs = [pl.BlockSpec(memory_space=pltpu.SMEM)] * scalars
    specs += [
        pl.BlockSpec(memory_space=pl.ANY if any(x is o for o in outside) else pltpu.VMEM) for x in operands[scalars:]
    ]
    many = isinstance(out_shape, (list, tuple))
    shapes = [pltpu.HBM(x.shape, x.dtype) for x in (out_shape if many else [out_shape])]
    out_specs = [pl.BlockSpec(memory_space=out_space)] * len(shapes)
    return pl.pallas_call(
        body,
        out_shape=shapes if many else shapes[0],
        in_specs=specs,
        out_specs=out_specs if many else out_specs[0],
        scratch_shapes=list(scratch),
        compiler_params=pltpu.CompilerParams(vmem_limit_bytes=limit * 1024 * 1024),
        cost_estimate=pl.CostEstimate(flops=flops, transcendentals=0, bytes_accessed=1 << 20),
    )(
        *[
            pltpu.with_memory_space_constraint(x, pltpu.VMEM) if any(x is r for r in resident) else in_hbm(x)
            for x in operands
        ]
    )


class Arrival:
    def __init__(self, sources, target, arrived):
        self.copies = [pltpu.make_async_copy(ref, target.at[i], arrived.at[i]) for i, ref in enumerate(sources)]
        for copy in self.copies:
            copy.start()

    def wait(self, index):
        self.copies[index].wait()


def dot_nn(left, right):
    return lax.dot_general(left, right, (((1,), (0,)), ((), ())), preferred_element_type=F32)


def column_norm(values):
    return values * lax.rsqrt(jnp.mean(values * values, axis=0, keepdims=True) + NORM_EPSILON)


def exchanged(shard, axis, groups):
    return lax.all_to_all(shard, axis, 0, 0, axis_index_groups=groups)


def staged(weights):
    def body(*refs):
        out, arrived = refs[-2:]
        arrival = Arrival(refs[:-2], out, arrived)
        for index in range(len(weights)):
            arrival.wait(index)

    return pl.pallas_call(
        body,
        out_shape=pltpu.VMEM((len(weights), *weights[0].shape), weights[0].dtype),
        in_specs=[pl.BlockSpec(memory_space=pl.ANY)] * len(weights),
        out_specs=pl.BlockSpec(memory_space=pltpu.VMEM),
        scratch_shapes=[pltpu.SemaphoreType.DMA((len(weights),))],
        compiler_params=pltpu.CompilerParams(vmem_limit_bytes=8 * 1024 * 1024),
        name="staged",
    )(*[in_hbm(w) for w in weights])


def project(ids, chunks, squares, weights, finish, out_shape, extra):
    rows, features = chunks[0][0].shape
    resident = not isinstance(weights, (list, tuple))
    weight_count = weights.shape[0] if resident else len(weights)
    width, channels = weights.shape[1:] if resident else weights[0].shape
    chunk_count, count = len(chunks), len(chunks[0])
    pieces = [piece for chunk in chunks for piece in chunk]
    weight_list = [weights] if resident else list(weights)

    def body(ids_ref, *refs):
        piece_refs, refs = refs[: len(pieces)], refs[len(pieces) :]
        squares_ref, refs = refs[0], refs[1:]
        weight_refs, refs = refs[: len(weight_list)], refs[len(weight_list) :]
        extra_refs, refs = refs[: len(extra)], refs[len(extra) :]
        outs, refs = refs[: len(out_shape)], refs[len(out_shape) :]
        held, product_store, joined = refs[:3]
        copies = []
        for chunk in range(chunk_count):
            for place, offset in enumerate(xor_offsets(count)):
                start = pl.multiple_of((ids_ref[1] ^ offset) * features, features)
                index = chunk * count + place
                copies.append(
                    pltpu.make_async_copy(
                        piece_refs[index], held.at[chunk, :, pl.ds(start, features)], joined.at[index]
                    )
                )
        for copy in copies[:count]:
            copy.start()
        if not resident:
            weight_store, arrived = refs[3:]
            arrival = Arrival(weight_refs, weight_store, arrived)
        for copy in copies[count:]:
            copy.start()
        for chunk in range(chunk_count):
            for copy in copies[chunk * count : (chunk + 1) * count]:
                copy.wait()
            span = slice(chunk * rows, (chunk + 1) * rows)
            row_scale = lax.rsqrt(squares_ref[:, span] / width + NORM_EPSILON)
            for index in range(weight_count):
                if not resident and chunk == 0:
                    arrival.wait(index)
                weight = weight_refs[0][index] if resident else weight_store[index]
                product_store[index] = dot_nn(held[chunk], weight).T * row_scale
                finish(ids_ref, chunk, index, product_store, extra_refs, outs)

    scratch = [
        pltpu.VMEM((chunk_count, rows, width), BF16),
        pltpu.VMEM((weight_count, channels, rows), F32),
        pltpu.SemaphoreType.DMA((len(pieces),)),
    ]
    if not resident:
        scratch += [pltpu.VMEM((weight_count, width, channels), BF16), pltpu.SemaphoreType.DMA((weight_count,))]
    return vmem_call(
        body,
        out_shape,
        [ids, *pieces, squares, *weight_list, *extra],
        scalars=1,
        scratch=scratch,
        flops=2 * weight_count * channels * rows * chunk_count * width,
        limit=24,
        outside=pieces if resident else (*weights, *pieces),
        resident=weight_list if resident else (),
    )


def project_heads(ids, pieces, squares, weights, gains, earlier, head_dim, slot_step, split):
    rows = pieces[0].shape[0]
    head_count = weights.shape[2] // head_dim
    before = 0 if earlier is None else earlier.shape[2]

    def finish(ids_ref, chunk, index, product, extra_refs, outs):
        query_out, pair_outs = outs[0], outs[1:]
        if index == 0 and before:
            query_out[:, :, :before] = extra_refs[2][...]
        own_slot = ids_ref[0] // slot_step
        for head in range(head_count):
            base = head * head_dim
            if split and index:
                base = pl.multiple_of((own_slot ^ head) * head_dim, head_dim)
            part = product[index, pl.ds(base, head_dim), :]
            if index == 0:
                query_out[head, :, before:] = (column_norm(part) * extra_refs[0][...]).astype(BF16)
                continue
            settled = (column_norm(part) * extra_refs[1][...] if index == 1 else part).astype(BF16)
            span = slice((index - 1) * head_dim, index * head_dim)
            if split:
                pair_outs[head][span, :] = settled
            else:
                pair_outs[0][head, span, :] = settled

    out_shape = [jax.ShapeDtypeStruct((head_count, head_dim, before + rows), BF16)]
    if split:
        out_shape += [jax.ShapeDtypeStruct((2 * head_dim, rows), BF16)] * head_count
    else:
        out_shape += [jax.ShapeDtypeStruct((head_count, 2 * head_dim, rows), BF16)]
    extra = [*gains] + ([earlier] if before else [])
    outs = project(ids, [pieces], squares, weights, finish, out_shape, extra)
    return outs[0], outs[1:]


def project_conv(ids, chunks, squares, weights):
    chunk_rows = chunks[0][0].shape[0]
    rows = chunk_rows * len(chunks)
    channels = weights[0].shape[1]
    tail = min(128, chunk_rows)

    def finish(ids_ref, chunk, index, product, extra_refs, outs):
        span = slice(chunk * chunk_rows, (chunk + 1) * chunk_rows)
        if index == 0:
            outs[0][:, span] = product[0]
        elif index == 2:
            gated = (product[1] * product[2]).astype(BF16)
            outs[1][:, span] = gated
            if chunk == len(chunks) - 1:
                outs[2][...] = gated[:, chunk_rows - tail :]

    out_shape = [
        jax.ShapeDtypeStruct((channels, rows), F32),
        jax.ShapeDtypeStruct((channels, rows), BF16),
        jax.ShapeDtypeStruct((channels, tail), BF16),
    ]
    return project(ids, chunks, squares, weights, finish, out_shape, [])


def finish_conv(outers, gateds, prior, taps, gain, group, tile_count):
    channels, chunk_rows = gateds[0].shape
    count = len(gateds)
    rows = chunk_rows * count
    tail = prior.shape[1]
    tap_count = taps.shape[1]
    tile_rows = rows // tile_count

    def body(*refs):
        outer_refs, gated_refs = refs[:count], refs[count : 2 * count]
        prior_ref, taps_ref, gain_ref, out = refs[2 * count :]
        lane = lax.broadcasted_iota(jnp.int32, (group, tail), 1)
        for index in range(channels // group):
            span = slice(index * group, (index + 1) * group)
            values = jnp.concatenate([ref[span, :].astype(F32) for ref in gated_refs], axis=1)
            outer = jnp.concatenate([ref[span, :] for ref in outer_refs], axis=1)
            before = prior_ref[span, :].astype(F32)
            weights = taps_ref[span, :]
            total = weights[:, tap_count - 1 : tap_count] * values
            for back in range(1, tap_count):
                moved = pltpu.roll(values, back, 1)
                head = jnp.where(lane < back, pltpu.roll(before, back, 1), moved[:, :tail])
                moved = jnp.concatenate([head, moved[:, tail:]], axis=1)
                total = total + weights[:, tap_count - 1 - back : tap_count - back] * moved
            mixed = (column_norm(outer * total) * gain_ref[span, :]).astype(BF16)
            for tile in range(tile_count):
                out[tile, span, :] = mixed[:, tile * tile_rows : (tile + 1) * tile_rows]

    return vmem_call(
        body,
        jax.ShapeDtypeStruct((tile_count, channels, tile_rows), BF16),
        [*outers, *gateds, prior, taps, gain],
        flops=1 << 20,
    )


def attend(ids, queries, pairs, gates, gain, lane_count, tile_count):
    chunk_count = len(pairs[0])
    slot_count, head_dim, rows = queries.shape
    counts = [len(chunk) for chunk in pairs[0]]
    flat_pairs = [kv for lane in pairs for chunk in lane for kv in chunk]
    chunk_rows = rows // chunk_count
    tile_rows = rows // tile_count
    q_tile = min(QUERY_TILE, chunk_rows)
    k_tile = q_tile
    q_tiles = rows // q_tile
    per_chunk = chunk_rows // k_tile
    block_count = slot_count * lane_count
    steps = slot_count * q_tiles
    wide = 2 * head_dim
    exponent_scale = LOG2_E * float(head_dim) ** -0.5
    subtiles = q_tile // tile_rows
    blocks = [slot * lane_count + (lane_count - 1 if slot % 2 else 0) for slot in range(slot_count)]
    full_tiles = sum(block * q_tiles + part for block in blocks for part in range(q_tiles))
    unroll = next(n for n in (4, 2, 1) if full_tiles % n == 0)

    def body(ids_ref, *refs):
        query_ref, refs = refs[0], refs[1:]
        flat_refs, refs = refs[: len(flat_pairs)], refs[len(flat_pairs) :]
        gate_refs, refs = refs[:lane_count], refs[lane_count:]
        gain_ref, out, key_store, value_store, query_store, score_store = refs[:6]
        top_store, total_store, arrived = refs[6:9]
        stages = refs[9:]
        copies = [pltpu.make_async_copy(ref, stage, arrived.at[i]) for i, (ref, stage) in enumerate(zip(flat_refs, stages))]
        for copy in copies:
            copy.start()
        own = ids_ref[0]
        own_slot = own // lane_count
        own_lane = own % lane_count
        query_lane = jnp.where(own_slot % 2 == 0, own_lane, lane_count - 1 - own_lane)

        ones = (lax.broadcasted_iota(jnp.int32, (head_dim, q_tile), 0) < 3).astype(F32).astype(BF16)
        for slot in range(slot_count):
            for part in range(q_tiles):
                index = slot * q_tiles + part
                query = query_ref[slot, :, part * q_tile : (part + 1) * q_tile].astype(F32) * exponent_scale
                coarse = query.astype(BF16)
                query_store[index, 0:head_dim, :] = coarse
                query_store[index, head_dim:wide, :] = ones
                query_store[index, wide : wide + head_dim, :] = (query - coarse.astype(F32)).astype(BF16)
                query_store[index, wide + head_dim : 2 * wide, :] = jnp.zeros_like(coarse)

        row8 = lax.broadcasted_iota(jnp.int32, (8, k_tile), 0)
        filler = jnp.zeros((head_dim - 8, k_tile), F32)

        def settle(ref, slot, lane, chunk):
            block = slot * lane_count + (own_lane ^ lane)
            for part in range(per_chunk):
                span = slice(part * k_tile, (part + 1) * k_tile)
                at = chunk * chunk_rows + part * k_tile
                index = block * q_tiles + chunk * per_chunk + part
                gate = gate_refs[lane][pl.ds(slot, 1), at : at + k_tile] * (-LOG2_E)
                first = gate.astype(BF16).astype(F32)
                rest = gate - first
                second = rest.astype(BF16).astype(F32)
                third = rest - second
                gate_rows = jnp.where(row8 == 0, first, jnp.where(row8 == 1, second, jnp.where(row8 == 2, third, 0.0)))
                stacked = jnp.concatenate([ref[0:head_dim, span].astype(F32), gate_rows, filler], axis=0)
                key_store[index] = stacked.T.astype(BF16)
                value_store[index] = ref[head_dim:wide, span]

        cursor = 0
        for lane in range(lane_count):
            for chunk in range(chunk_count):
                for member in range(counts[chunk]):
                    copies[cursor].wait()
                    if counts[chunk] > 1:
                        settle(stages[cursor], own_slot ^ member, lane, chunk)
                    else:
                        for slot in range(slot_count):
                            settle(stages[cursor].at[slot], slot, lane, chunk)
                    cursor += 1

        def tile_of(step):
            slot = step // q_tiles
            block = slot * lane_count + jnp.where(slot % 2 == 0, query_lane, lane_count - 1 - query_lane)
            return block * q_tiles + step % q_tiles

        def score(step, tile, place, masked):
            keys = key_store[tile]
            scores = dot_nn(jnp.concatenate([keys, keys], axis=1), query_store[step])
            if masked:
                key_at = lax.broadcasted_iota(jnp.int32, (k_tile, q_tile), 0)
                query_at = lax.broadcasted_iota(jnp.int32, (k_tile, q_tile), 1)
                scores = jnp.where(key_at <= query_at, scores, -1e30)
            score_store[place] = scores
            highest = jnp.max(scores, axis=0, keepdims=True)
            if masked:
                top_store[step] = highest
                return highest, None
            old = top_store[step]
            top = jnp.maximum(old, highest)
            top_store[step] = top
            return top, jnp.exp2(old - top)

        def absorb(step, tile, place, top, factor):
            weights = jnp.exp2(score_store[place] - top).astype(BF16)
            added = dot_nn(value_store[tile], weights)
            total_store[step] = added if factor is None else total_store[step] * factor + added

        top, _ = score(0, tile_of(0), 0, True)

        def on_diagonal(pair, top):
            step = 2 * pair
            middle, _ = score(step + 1, tile_of(step + 1), 1, True)
            absorb(step, tile_of(step), 0, top, None)
            following = jnp.minimum(step + 2, steps - 1)
            latest, _ = score(following, tile_of(following), 0, True)
            absorb(step + 1, tile_of(step + 1), 1, middle, None)
            return latest

        lax.fori_loop(0, steps // 2, on_diagonal, top)

        def following(step, tile):
            done = tile + 1 >= tile_of(step)
            return jnp.where(done, jnp.minimum(step + 1, steps - 1), step), jnp.where(done, 0, tile + 1)

        step = jnp.where(tile_of(0) == 0, 1, 0)
        top, factor = score(step, 0, 0, False)

        def below(turn, carry):
            step, tile, top, factor = carry
            for count in range(unroll):
                next_step, next_tile = following(step, tile)
                place = count % 2
                if unroll == 1:
                    absorb(step, tile, 0, top, factor)
                    next_top, next_factor = score(next_step, next_tile, 0, False)
                elif count < unroll - 1:
                    next_top, next_factor = score(next_step, next_tile, 1 - place, False)
                    absorb(step, tile, place, top, factor)
                else:
                    more = turn + 1 < full_tiles // unroll
                    next_step = jnp.where(more, next_step, step)
                    next_tile = jnp.where(more, next_tile, tile)
                    next_top, next_factor = score(next_step, next_tile, 0, False)
                    absorb(step, tile, 1, top, factor)
                step, tile, top, factor = next_step, next_tile, next_top, next_factor
            return step, tile, top, factor

        lax.fori_loop(0, full_tiles // unroll, below, (step, jnp.int32(0), top, factor))

        head_gain = gain_ref[own_slot]
        for step in range(steps):
            mixed = (column_norm(total_store[step]) * head_gain).astype(BF16)
            for sub in range(subtiles):
                out[step * subtiles + sub] = mixed[:, sub * tile_rows : (sub + 1) * tile_rows]

    return vmem_call(
        body,
        jax.ShapeDtypeStruct((slot_count * tile_count, head_dim, tile_rows), BF16),
        [ids, queries, *flat_pairs, *gates, gain],
        scalars=1,
        scratch=[
            pltpu.VMEM((block_count * q_tiles, k_tile, wide), BF16),
            pltpu.VMEM((block_count * q_tiles, head_dim, k_tile), BF16),
            pltpu.VMEM((steps, 2 * wide, q_tile), BF16),
            pltpu.VMEM((2, k_tile, q_tile), F32),
            pltpu.VMEM((steps, 1, q_tile), F32),
            pltpu.VMEM((steps, head_dim, q_tile), F32),
            pltpu.SemaphoreType.DMA((len(flat_pairs),)),
            *[pltpu.VMEM(kv.shape, BF16) for kv in flat_pairs],
        ],
        flops=4 * head_dim * slot_count * rows * block_count * rows,
        limit=28,
        outside=flat_pairs,
    )


def output_rows(ids, pieces, weights, base):
    source_count = len(weights)
    piece_count, piece_height, rows = pieces.shape
    slot_count = piece_count // source_count
    height = slot_count * piece_height
    width = weights[0].shape[1]
    offsets = xor_offsets(source_count)
    bases = [] if base is None else [base]
    parts = OUTPUT_PARTS
    part_width = width // parts

    def body(ids_ref, piece_ref, *refs):
        weight_refs, refs = refs[:source_count], refs[source_count:]
        base_refs, refs = refs[: len(bases)], refs[len(bases) :]
        out_ref, held, weight_store, result, joined, arrived, left = refs[:7]
        gathers = []
        for place, offset in enumerate(offsets):
            source = ids_ref[1] ^ offset
            for slot in range(slot_count):
                start = place * height + slot * piece_height
                gathers.append(
                    pltpu.make_async_copy(
                        piece_ref.at[slot * source_count + source],
                        held.at[start : start + piece_height, :],
                        joined.at[place * slot_count + slot],
                    )
                )
                gathers[-1].start()
        arrival = Arrival(weight_refs, weight_store, arrived)
        if bases:
            below = pltpu.make_async_copy(base_refs[0], refs[7], refs[8].at[0])
            below.start()
        for copy in gathers:
            copy.wait()
        turned = held[...].T
        for place in range(source_count):
            arrival.wait(place)
        if bases:
            below.wait()
        stores = []
        for part in range(parts):
            span = slice(part * part_width, (part + 1) * part_width)
            weight = jnp.concatenate([weight_store[place, :, span] for place in range(source_count)], axis=0)
            total = dot_nn(turned, weight)
            if bases:
                total = total + refs[7][:, span].astype(F32)
            result[:, span] = total.astype(BF16)
            stores.append(pltpu.make_async_copy(result.at[:, span], out_ref.at[:, span], left.at[part]))
            stores[-1].start()
        for copy in stores:
            copy.wait()

    scratch = [
        pltpu.VMEM((source_count * height, rows), BF16),
        pltpu.VMEM((source_count, height, width), BF16),
        pltpu.VMEM((rows, width), BF16),
        pltpu.SemaphoreType.DMA((piece_count,)),
        pltpu.SemaphoreType.DMA((source_count,)),
        pltpu.SemaphoreType.DMA((parts,)),
    ]
    if bases:
        scratch += [pltpu.VMEM((rows, width), BF16), pltpu.SemaphoreType.DMA((1,))]
    return vmem_call(
        body,
        jax.ShapeDtypeStruct((rows, width), BF16),
        [ids, pieces, *weights, *bases],
        scalars=1,
        scratch=scratch,
        flops=2 * source_count * height * rows * width,
        outside=(pieces, *weights, *bases),
        out_space=pl.ANY,
    )


def per_device(
    tokens,
    mix_gain,
    query_weight,
    key_weight,
    value_weight,
    outer_gate_weight,
    inner_gate_weight,
    conv_input_weight,
    query_gain,
    key_gain,
    gate_totals,
    conv_taps,
    attn_out_gain,
    conv_out_gain,
    attn_out_weight,
    conv_out_weight,
):
    rows, features = tokens.shape
    head_dim = query_gain.shape[0]
    head_count = query_weight.shape[1] // head_dim
    sp_count = lax.axis_size("sp")
    tp_count = lax.axis_size("tp")
    lane_count = sp_count // head_count
    sp_index = lax.axis_index("sp")
    tp_index = lax.axis_index("tp")
    ids = jnp.stack([sp_index, tp_index]).astype(jnp.int32)
    chunk_rows = rows // ROW_CHUNKS
    straight = [[slot * lane_count + lane for slot in range(head_count)] for lane in range(lane_count)]
    snaked = [
        [slot * lane_count + (lane_count - 1 - lane if slot % 2 else lane) for slot in range(head_count)]
        for lane in range(lane_count)
    ]
    snaked_wide = [[p * tp_count + t for p in group for t in range(tp_count)] for group in snaked]

    own_gain = lax.dynamic_slice_in_dim(mix_gain, tp_index * features, features, 0)
    scaled = [
        (tokens[c * chunk_rows : (c + 1) * chunk_rows].astype(F32) * own_gain).astype(BF16) for c in range(ROW_CHUNKS)
    ]
    far = []
    for c in range(ROW_CHUNKS):
        far.append(swapped(scaled[c], "tp", tp_count >> 1))
    tokens, gate_totals = lax.optimization_barrier((tokens, gate_totals, *scaled))[:2]
    widened = tokens.astype(F32)
    squares = jnp.sum(widened * widened, axis=1).reshape(1, rows)
    gains = (query_gain.reshape(-1, 1), key_gain.reshape(-1, 1))
    out_gains = (attn_out_gain.reshape(head_count, head_dim, 1), conv_out_gain.reshape(-1, 1), conv_taps.T)
    slot_gates = exchanged(gate_totals.T, "sp", straight)
    gates = [slot_gates] + [swapped(slot_gates, "sp", lane) for lane in range(1, lane_count)]
    attn_weight = staged((query_weight, key_weight, value_weight))
    conv_weight = (outer_gate_weight, inner_gate_weight, conv_input_weight)
    squares, ids, gains, out_gains, gates, attn_weight = lax.optimization_barrier(
        (squares, ids, gains, out_gains, gates, attn_weight)
    )
    bit = tp_count >> 1
    while bit:
        squares = squares + swapped(squares, "tp", bit)
        bit >>= 1
    chunks = []
    for c in range(ROW_CHUNKS):
        pieces = [scaled[c], far[c]]
        bit = tp_count >> 2
        while bit:
            pieces = pieces + [swapped(piece, "tp", bit) for piece in pieces]
            bit >>= 1
        chunks.append(pieces)

    queries, outers, gateds = None, [], []
    pairs = [[] for _ in range(lane_count)]
    for c in range(ROW_CHUNKS):
        chunk_squares = squares[:, c * chunk_rows : (c + 1) * chunk_rows]
        split = c > 0
        if split:
            chunk_squares, outers[-1] = lax.optimization_barrier((chunk_squares, outers[-1]))
        queries, own_pairs = project_heads(
            ids, chunks[c], chunk_squares, attn_weight, gains, queries, head_dim, lane_count, split
        )
        outer, gated, gated_tail = project_conv(ids, [chunks[c]], chunk_squares, conv_weight)
        outers.append(outer)
        gateds.append(gated)
        if split:
            moved = [swapped(p, "sp", i * lane_count) if i else p for i, p in enumerate(own_pairs)]
        else:
            moved = [exchanged(own_pairs[0], "sp", straight)]
        pairs[0].append(moved)
        for lane in range(1, lane_count):
            through = []
            for p in moved:
                through.append(swapped(p, "sp", lane))
            pairs[lane].append(through)
    prior = lax.ppermute(gated_tail, "sp", [(i, i + 1) for i in range(sp_count - 1)])
    queries = exchanged(queries, "sp", snaked)

    far_weights = lax.optimization_barrier((attn_out_weight, conv_out_weight, far[-1]))[:2]
    half = tp_count >> 1
    far_weights = [swapped(weight, "tp", half) for weight in far_weights]

    conv_mixed = finish_conv(
        outers, gateds, prior, out_gains[2], out_gains[1], head_dim, tp_count
    )
    conv_pieces = lax.all_to_all(conv_mixed, "tp", 0, 0)
    attended = attend(
        ids, queries, pairs, gates, out_gains[0], lane_count, tp_count
    )
    attn_pieces = lax.all_to_all(attended, ("sp", "tp"), 0, 0, axis_index_groups=snaked_wide)
    own_weights = lax.optimization_barrier((attn_out_weight, conv_out_weight, *far_weights, attended))[:4]
    gathered = []
    for own, distant in zip(own_weights[:2], own_weights[2:]):
        parts = [own, distant]
        bit = tp_count >> 2
        while bit:
            parts = parts + [swapped(part, "tp", bit) for part in parts]
            bit >>= 1
        gathered.append(parts)
    base = output_rows(ids, conv_pieces, gathered[1], None)
    return output_rows(ids, attn_pieces, gathered[0], base)


def solution(mesh):
    placed = (
        P("sp", "tp"),
        P(),
        P(None, "tp"),
        P(None, "tp"),
        P(None, "tp"),
        P(None, "tp"),
        P(None, "tp"),
        P(None, "tp"),
        P(),
        P(),
        P("sp", "tp"),
        P(None, "tp"),
        P("tp"),
        P("tp"),
        P("tp", None),
        P("tp", None),
    )
    return jax.shard_map(per_device, mesh=mesh, in_specs=placed, out_specs=P(("sp", "tp"), None), check_vma=False)
```

time: 174 us -> 175 us (level)
  local copies, waits for them, and re-layouts: 23.6 us -> 4.53 us
  Pallas kernels: 50.8 us -> 65.4 us
  starting transfers between devices: 47.9 us -> 51.2 us
  waiting for transfers between devices: 47.2 us -> 50.1 us
    unnamed x81 -> x44, local copies, waits for them, and re-layouts: 20.9 us -> 2.53 us
    pallas_call x8 -> x9, Pallas kernels: 50.8 us -> 65.4 us  [the longest x8 63.5 us: vmem_call(): pl.pallas_call(body, out_shape=shapes if many else shapes[0], in_specs=sp...]
    all_to_all x3, waiting for transfers between devices: 13.9 us -> 6.38 us  [exchanged(): return lax.all_to_all(shard, axis, 0, 0, axis_index_groups=groups)]
    ppermute x20 -> x23, waiting for transfers between devices: 22.2 us -> 28.4 us  [swapped(): return lax.ppermute(shard, axis, [(i, i ^ offset) for i in range(devices)])]
    all_to_all x1, starting transfers between devices: 5.74 us -> 8.47 us  [per_device(): lax.all_to_all(attended, ('sp', 'tp'), 0, 0, axis_index_groups=snaked_wide)]
    ppermute x1, waiting for transfers between devices: 1.22 us -> 3.48 us  [per_device(): lax.ppermute(gated_tail, 'sp', [(i, i + 1) for i in range(sp_count - 1)])]
    ppermute x20 -> x23, starting transfers between devices: 21.9 us -> 22.6 us  [swapped(): return lax.ppermute(shard, axis, [(i, i ^ offset) for i in range(devices)])]
  transfers between devices with their start and end apart: 26 -> 29, of which waited for: 11 -> 11; matrix products, arithmetic and copies ran while one was open for 2% -> 1% of each run, Pallas kernels for 27% -> 34%
where the time goes in v2:
time: 175 us; the launch traced here: 174 us
  Pallas kernels  65.4 us (37%)
  starting transfers between devices  51.2 us (29%)
  waiting for transfers between devices  50.1 us (29%)
  local copies, waits for them, and re-layouts  4.53 us (3%)
  other arithmetic  2.74 us (2%)
    pallas_call x8, Pallas kernels, vmem_call(): pl.pallas_call(body, out_shape=shapes if many else shapes[0], in_specs=sp...  63.5 us
    ppermute x23, waiting for transfers between devices, swapped(): return lax.ppermute(shard, axis, [(i, i ^ offset) for i in range(devices)])  28.4 us
    ppermute x23, starting transfers between devices, swapped(): return lax.ppermute(shard, axis, [(i, i ^ offset) for i in range(devices)])  22.6 us
    all_to_all x3, starting transfers between devices, exchanged(): return lax.all_to_all(shard, axis, 0, 0, axis_index_groups=groups)  13.9 us
    all_to_all x1, waiting for transfers between devices, per_device(): lax.all_to_all(attended, ('sp', 'tp'), 0, 0, axis_index_groups=snaked_wide)  10.2 us
    all_to_all x1, starting transfers between devices, per_device(): lax.all_to_all(attended, ('sp', 'tp'), 0, 0, axis_index_groups=snaked_wide)  8.47 us
    all_to_all x3, waiting for transfers between devices, exchanged(): return lax.all_to_all(shard, axis, 0, 0, axis_index_groups=groups)  6.38 us
    all_to_all x1, starting transfers between devices, per_device(): conv_pieces = lax.all_to_all(conv_mixed, 'tp', 0, 0)  3.65 us
  transfers between devices with their start and end apart: 29, of which 11 were waited for; matrix products, arithmetic and copies ran while one was open for 1% of the time, Pallas kernels for 34%

profile of v2, /device:TPU:0, one launch (start us, length us, event | category | flops | bytes accessed | tf_op | source)
XLA Modules:
  0.0 174.5 jit_solution(17645483984866070263)
XLA Ops:
  0.0 0.9 dynamic_slice.3
  0.9 2.4 %multiply_convert_fusion = (bf16[512,512]{1,0:T(8,128)(2,1)}, bf16[512,512]{1,0:T(8,128)(2,1)}) fusion(bf16[1024,512]{1,0:T(8,128)(2,1)} %param.16, f32[512]{0:T(512)S(1)} %dynamic_slice.3), kind=kLoop, calls=%fused_computation.1 | loop fusion | flops 1572864 | bytes 2099200 | tf_op jit(solution)/shard_map/convert_element_type | solution.py:543
  3.3 3.0 %collective-permute-start.6 = (bf16[512,512]{1,0:T(8,128)(2,1)}, bf16[512,512]{1,0:T(8,128)(2,1)}, u32[]{:S(2)}, u32[]{:S(2)}) collective-permute-start(bf16[512,512]{1,0:T(8,128)(2,1)} %get-tuple-element.70.refs_0_), channel_id=1, source_target_pairs={{0,2},{1,3},{2,0},{3,1},{4,6},{5,7},{6,4},{7,5},{8,10},{9,11},{10,... | collective-permute-start | bytes 1572872 | tf_op jit(solution)/shard_map/ppermute | solution.py:19
  6.2 12.2 %collective-permute-done.6.refs_1_ = bf16[512,512]{1,0:T(8,128)(2,1)} collective-permute-done((bf16[512,512]{1,0:T(8,128)(2,1)}, bf16[512,512]{1,0:T(8,128)(2,1)}, u32[]{:S(2)}, u32[]{:S(2)}) %collective-permute-start.6) | collective-permute-done | bytes 524320 | tf_op jit(solution)/shard_map/ppermute | solution.py:19
  18.5 1.7 collective-permute-start.1
  20.2 0.6 all_to_all.20
  20.8 4.9 %all-to-all-start = ((f32[4,1,1024]{2,1,0:T(1,128)}), f32[4,1,1024]{2,1,0:T(1,128)S(1)}, u32[]{:S(2)}, u32[]{:S(2)}) async-start(f32[4,1,1024]{2,1,0:T(1,128)} %all_to_all.20), calls=%async_computation | async-start | bytes 32768 | tf_op jit(solution)/shard_map/all_to_all | solution.py:78
  25.7 0.3 multiply_reduce_fusion
  26.0 5.3 %all-to-all-done = f32[4,1,1024]{2,1,0:T(1,128)S(1)} async-done(((f32[4,1,1024]{2,1,0:T(1,128)}), f32[4,1,1024]{2,1,0:T(1,128)S(1)}, u32[]{:S(2)}, u32[]{:S(2)}) %all-to-all-start) | async-done | bytes 16416 | tf_op jit(solution)/shard_map/all_to_all | solution.py:78
  31.3 1.5 collective-permute-start
  32.8 0.1 pad_add_fusion.ids_ref
  32.9 0.1 reshape.21
  33.0 0.1 copy.29
  33.1 0.0 copy-start.10
  33.2 0.0 copy-start.11
  33.2 1.9 %staged.1.refs_5_ = bf16[3,2048,256]{2,1,0:T(8,128)(2,1)S(1)} custom-call(bf16[2048,256]{1,0:T(8,128)(2,1)} %refs_0_.1, bf16[2048,256]{1,0:T(8,128)(2,1)} %refs_1_.1, bf16[2048,256]{1,0:T(8,128)(2,1)} %refs_2_.1), custom_call_target="tpu_custom_call" | custom-call | tf_op jit(solution)/shard_map/staged/pallas_call | solution.py:88
  35.1 0.0 collective-permute-done.refs_12_
  35.1 0.6 collective-permute-start.4
  35.7 3.1 %collective-permute-done.4 = f32[1,1024]{1,0:T(1,128)S(1)} collective-permute-done((f32[1,1024]{1,0:T(1,128)S(1)}, f32[1,1024]{1,0:T(1,128)S(1)}, u32[]{:S(2)}, u32[]{:S(2)}) %collective-permute-start.4) | collective-permute-done | bytes 4128 | tf_op jit(solution)/shard_map/ppermute | solution.py:19
  38.8 0.0 collective-permute-start.5
  38.8 0.1 copy.32.refs_6_
  38.9 0.1 copy.33.refs_7_
  39.0 1.0 collective-permute-done.5
  40.0 4.9 %shard_map.155 = (bf16[4,64,512]{2,1,0:T(8,128)(2,1)}, bf16[4,128,512]{2,1,0:T(8,128)(2,1)}) custom-call(s32[2]{0:T(128)S(1)} %pad_add_fusion.ids_ref, bf16[512,512]{1,0:T(8,128)(2,1)} %get-tuple-element.70.refs_0_, bf16[512,512]{1,0:T(8,128)(2,1)} %collective-permute-done.6.refs_1_, bf16[512,512]{1,0:T(8,128)(2,1)} %collective-permute-done.7.refs_2_, ...), custom_call_target="tpu_custom_call" | custom-call | flops 1610612736 | bytes 1048576 | tf_op jit(solution)/shard_map/pallas_call | solution.py:43
  44.9 4.2 %all-to-all-start.2 = ((bf16[4,128,512]{2,1,0:T(8,128)(2,1)}), bf16[4,128,512]{2,1,0:T(8,128)(2,1)}, u32[]{:S(2)}, u32[]{:S(2)}) async-start(bf16[4,128,512]{2,1,0:T(8,128)(2,1)} %get-tuple-element.48), calls=%async_computation.2 | async-start | bytes 1048576 | tf_op jit(solution)/shard_map/all_to_all | solution.py:78
  49.0 0.2 collective-permute-start.2
  49.3 0.3 collective-permute-start.3
  49.6 6.9 %shard_map.154 = (f32[256,512]{1,0:T(8,128)}, bf16[256,512]{1,0:T(8,128)(2,1)}, bf16[256,128]{1,0:T(8,128)(2,1)}) custom-call(s32[2]{0:T(128)S(1)} %pad_add_fusion.ids_ref, bf16[512,512]{1,0:T(8,128)(2,1)} %get-tuple-element.70.refs_0_, bf16[512,512]{1,0:T(8,128)(2,1)} %collective-permute-done.6.refs_1_, bf16[512,512]{1,0:T(8,128)(2,1)} %collective-permute-done.7.refs_2_, ...), custom_call_target="tpu_custom_call" | custom-call | flops 1610612736 | bytes 1048576 | tf_op jit(solution)/shard_map/pallas_call | solution.py:43
  56.6 0.8 copy-done.12
  57.3 0.2 copy-done.13
  57.5 5.6 %shard_map.156 = (bf16[4,64,1024]{2,1,0:T(8,128)(2,1)}, bf16[128,512]{1,0:T(8,128)(2,1)}, bf16[128,512]{1,0:T(8,128)(2,1)}, bf16[128,512]{1,0:T(8,128)(2,1)}, bf16[128,512]{1,0:T(8,128)(2,1)}) custom-call(s32[2]{0:T(128)S(1)} %pad_add_fusion.ids_ref, bf16[512,512]{1,0:T(8,128)(2,1)} %get-tuple-element.69.refs_0_, ...), custom_call_target="tpu_custom_call" | custom-call | flops 1610612736 | bytes 1048576 | tf_op jit(solution)/shard_map/pallas_call | solution.py:43
  63.2 1.0 all-to-all-done.2.refs_1_
  64.2 4.8 %all-to-all-start.1 = ((bf16[4,64,1024]{2,1,0:T(8,128)(2,1)}), bf16[4,64,1024]{2,1,0:T(8,128)(2,1)}, u32[]{:S(2)}, u32[]{:S(2)}) async-start(bf16[4,64,1024]{2,1,0:T(8,128)(2,1)} %get-tuple-element.47), calls=%async_computation.1 | async-start | bytes 1048576 | tf_op jit(solution)/shard_map/all_to_all | solution.py:78
  69.0 0.8 collective-permute-start.12
  69.9 2.7 %collective-permute-start.9 = (bf16[128,512]{1,0:T(8,128)(2,1)}, bf16[128,512]{1,0:T(8,128)(2,1)S(1)}, u32[]{:S(2)}, u32[]{:S(2)}) collective-permute-start(bf16[128,512]{1,0:T(8,128)(2,1)} %get-tuple-element.50), channel_id=1, source_target_pairs={{0,8},{4,12},{8,0},{12,4},{16,24},{20,28},{24,16},{28,20},{1,9},{5... | collective-permute-start | bytes 393224 | tf_op jit(solution)/shard_map/ppermute | solution.py:19
  72.5 2.4 %collective-permute-start.10 = (bf16[128,512]{1,0:T(8,128)(2,1)}, bf16[128,512]{1,0:T(8,128)(2,1)S(1)}, u32[]{:S(2)}, u32[]{:S(2)}) collective-permute-start(bf16[128,512]{1,0:T(8,128)(2,1)} %get-tuple-element.51), channel_id=1, source_target_pairs={{0,16},{4,20},{8,24},{12,28},{16,0},{20,4},{24,8},{28,12},{1,17},{... | collective-permute-start | bytes 393224 | tf_op jit(solution)/shard_map/ppermute | solution.py:19
  74.9 0.1 collective-permute-start.11
  75.0 6.9 %shard_map.158 = (f32[256,512]{1,0:T(8,128)}, bf16[256,512]{1,0:T(8,128)(2,1)}, bf16[256,128]{1,0:T(8,128)(2,1)}) custom-call(s32[2]{0:T(128)S(1)} %pad_add_fusion.ids_ref, bf16[512,512]{1,0:T(8,128)(2,1)} %get-tuple-element.69.refs_0_, bf16[512,512]{1,0:T(8,128)(2,1)} %collective-permute-done.1.refs_1_, bf16[512,512]{1,0:T(8,128)(2,1)} %copy-done.12, ...), custom_call_target="tpu_custom_call" | custom-call | flops 1610612736 | bytes 1048576 | tf_op jit(solution)/shard_map/pallas_call | solution.py:43
  81.9 2.6 %collective-permute-start.21 = (bf16[256,128]{1,0:T(8,128)(2,1)}, bf16[256,128]{1,0:T(8,128)(2,1)S(1)}, u32[]{:S(2)}, u32[]{:S(2)}) collective-permute-start(bf16[256,128]{1,0:T(8,128)(2,1)} %get-tuple-element.64), channel_id=1, source_target_pairs={{0,4},{4,8},{8,12},{12,16},{16,20},{20,24},{24,28},{1,5},{5,9},{9,... | collective-permute-start | bytes 196616 | tf_op jit(solution)/shard_map/ppermute | solution.py:596
  84.6 3.5 %collective-permute-done.21.refs_4_ = bf16[256,128]{1,0:T(8,128)(2,1)S(1)} collective-permute-done((bf16[256,128]{1,0:T(8,128)(2,1)}, bf16[256,128]{1,0:T(8,128)(2,1)S(1)}, u32[]{:S(2)}, u32[]{:S(2)}) %collective-permute-start.21) | collective-permute-done | bytes 65568 | tf_op jit(solution)/shard_map/ppermute | solution.py:596
  88.0 2.4 %collective-permute-start.13 = (bf16[128,512]{1,0:T(8,128)(2,1)S(1)}, bf16[128,512]{1,0:T(8,128)(2,1)S(1)}, u32[]{:S(2)}, u32[]{:S(2)}) collective-permute-start(bf16[128,512]{1,0:T(8,128)(2,1)S(1)} %copy-done.14), channel_id=1, source_target_pairs={{0,4},{4,0},{8,12},{12,8},{16,20},{20,16},{24,28},{28,24},{1,5},{5... | collective-permute-start | bytes 393224 | tf_op jit(solution)/shard_map/ppermute | solution.py:19
  90.4 0.1 collective-permute-start.14
  90.5 2.6 %collective-permute-done.10.refs_4_ = bf16[128,512]{1,0:T(8,128)(2,1)S(1)} collective-permute-done((bf16[128,512]{1,0:T(8,128)(2,1)}, bf16[128,512]{1,0:T(8,128)(2,1)S(1)}, u32[]{:S(2)}, u32[]{:S(2)}) %collective-permute-start.10) | collective-permute-done | bytes 131104 | tf_op jit(solution)/shard_map/ppermute | solution.py:19
  93.2 0.5 collective-permute-start.17
  93.7 1.6 collective-permute-start.18
  95.3 1.3 collective-permute-start.15
  96.5 0.5 collective-permute-done.14.refs_8_
  97.0 2.4 %collective-permute-start.16 = (bf16[128,512]{1,0:T(8,128)(2,1)S(1)}, bf16[128,512]{1,0:T(8,128)(2,1)}, u32[]{:S(2)}, u32[]{:S(2)}) collective-permute-start(bf16[128,512]{1,0:T(8,128)(2,1)S(1)} %collective-permute-done.11.refs_5_), channel_id=1, source_target_pairs={{0,4},{4,0},{8,12},{12,8},{16,20},{20,16},{24,28},{28,24},{1,5},{5... | collective-permute-start | bytes 393224 | tf_op jit(solution)/shard_map/ppermute | solution.py:19
  99.4 0.1 copy.34.refs_13_
  99.5 0.1 copy.35.refs_6_
  99.6 3.0 %shard_map.159 = bf16[4,256,256]{2,1,0:T(8,128)(2,1)} custom-call(f32[256,512]{1,0:T(8,128)} %get-tuple-element.60.refs_0_, f32[256,512]{1,0:T(8,128)} %get-tuple-element.61.refs_1_, bf16[256,512]{1,0:T(8,128)(2,1)} %get-tuple-element.62.refs_2_, bf16[256,512]{1,0:T(8,128)(2,1)} %get-tuple-element.63.refs_3_, bf16[256,128]{1,0:T(8,128)(2,1)} %copy-done.5, ...), custom_call_target="tpu_custom_call" | custom-call | flops 1048576 | bytes 1048576 | tf_op jit(solution)/shard_map/pallas_call | solution.py:43
  102.7 3.7 %all-to-all-start.4 = ((bf16[4,256,256]{2,1,0:T(8,128)(2,1)}), bf16[4,256,256]{2,1,0:T(8,128)(2,1)S(1)}, u32[]{:S(2)}, u32[]{:S(2)}) async-start(bf16[4,256,256]{2,1,0:T(8,128)(2,1)} %shard_map.159), calls=%async_computation.4 | async-start | bytes 1048576 | tf_op jit(solution)/shard_map/all_to_all | solution.py:606
  106.4 0.6 copy-done.20
  107.0 25.6 %shard_map.157 = bf16[16,64,256]{2,1,0:T(8,128)(2,1)} custom-call(s32[2]{0:T(128)S(1)} %pad_add_fusion.ids_ref, bf16[4,64,1024]{2,1,0:T(8,128)(2,1)} %all-to-all-done.1.refs_0_, bf16[4,128,512]{2,1,0:T(8,128)(2,1)} %all-to-all-done.2.refs_1_, bf16[128,512]{1,0:T(8,128)(2,1)} %get-tuple-element.49.refs_2_, bf16[128,512]{1,0:T(8,128)(2,1)} %copy-done.15, ...), custom_call_target="tpu_custom_call" | custom-call | flops 8589934592 | bytes 1048576 | tf_op jit(solution)/shard_map/pallas_call | solution.py:43
  132.6 9.0 %collective-permute-done.18.refs_1_ = bf16[256,2048]{1,0:T(8,128)(2,1)} collective-permute-done((bf16[256,2048]{1,0:T(8,128)(2,1)S(1)}, bf16[256,2048]{1,0:T(8,128)(2,1)}, u32[]{:S(2)}, u32[]{:S(2)}) %collective-permute-start.18) | collective-permute-done | bytes 1048608 | tf_op jit(solution)/shard_map/ppermute | solution.py:19
  141.7 0.5 collective-permute-start.23
  142.2 0.0 collective-permute-start.19
  142.2 0.5 collective-permute-start.20
  142.7 1.7 all-to-all-done.4.piece_ref
  144.4 8.5 %all-to-all-start.3 = ((bf16[16,64,256]{2,1,0:T(8,128)(2,1)}), bf16[16,64,256]{2,1,0:T(8,128)(2,1)S(1)}, u32[]{:S(2)}, u32[]{:S(2)}) async-start(bf16[16,64,256]{2,1,0:T(8,128)(2,1)} %shard_map.157), calls=%async_computation.3 | async-start | bytes 1048576 | tf_op jit(solution)/shard_map/all_to_all | solution.py:610
  152.9 5.0 %shard_map.160.refs_4_ = bf16[256,2048]{1,0:T(8,128)(2,1)} custom-call(s32[2]{0:T(128)S(1)} %pad_add_fusion.ids_ref, bf16[4,256,256]{2,1,0:T(8,128)(2,1)} %copy-done.1, bf16[256,2048]{1,0:T(8,128)(2,1)} %refs_0_.2, bf16[256,2048]{1,0:T(8,128)(2,1)} %collective-permute-done.18.refs_1_, bf16[256,2048]{1,0:T(8,128)(2,1)} %collective-permute-done.22.refs_2_, ...), custom_call_target="tpu_custom_call" | custom-call | flops 1073741824 | bytes 1048576 | tf_op jit(solution)/shard_map/pallas_call | solution.py:43
  157.8 10.2 %all-to-all-done.3.piece_ref = bf16[16,64,256]{2,1,0:T(8,128)(2,1)S(1)} async-done(((bf16[16,64,256]{2,1,0:T(8,128)(2,1)}), bf16[16,64,256]{2,1,0:T(8,128)(2,1)S(1)}, u32[]{:S(2)}, u32[]{:S(2)}) %all-to-all-start.3) | async-done | bytes 524320 | tf_op jit(solution)/shard_map/all_to_all | solution.py:610
  168.0 0.8 copy-done.2
  168.8 5.5 %shard_map.161 = bf16[256,2048]{1,0:T(8,128)(2,1)} custom-call(s32[2]{0:T(128)S(1)} %pad_add_fusion.ids_ref, bf16[16,64,256]{2,1,0:T(8,128)(2,1)} %copy-done.2, bf16[256,2048]{1,0:T(8,128)(2,1)} %refs_0_.3, bf16[256,2048]{1,0:T(8,128)(2,1)} %collective-permute-done.17.refs_1_, bf16[256,2048]{1,0:T(8,128)(2,1)} %collective-permute-done.19.refs_2_, ...), custom_call_target="tpu_custom_call" | custom-call | flops 1073741824 | bytes 1048576 | tf_op jit(solution)/shard_map/pallas_call | solution.py:43
  (60 shorter events, 0.1 us)
Async XLA Ops:
  0.0 25.7 %copy-start = (bf16[1024,512]{1,0:T(8,128)(2,1)S(1)}, bf16[1024,512]{1,0:T(8,128)(2,1)}, u32[]{:S(2)}) copy-start(bf16[1024,512]{1,0:T(8,128)(2,1)} %param.16) | copy-start | bytes 3145732
  0.0 20.2 %copy-start.6 = (f32[1024,4]{0,1:T(4,128)S(1)}, f32[1024,4]{0,1:T(4,128)}, u32[]{:S(2)}) copy-start(f32[1024,4]{0,1:T(4,128)} %param.26) | copy-start | bytes 49156
  0.0 32.9 %copy-start.9 = (f32[256]{0:T(256)S(1)}, f32[256]{0:T(256)}, u32[]{:S(2)}) copy-start(f32[256]{0:T(256)} %param.28) | copy-start | bytes 3076
  0.0 33.0 %copy-start.7 = (f32[3,256]{1,0:T(4,128)S(1)}, f32[3,256]{1,0:T(4,128)}, u32[]{:S(2)}) copy-start(f32[3,256]{1,0:T(4,128)} %param.27) | copy-start | bytes 9220
  3.3 15.2 %collective-permute-start.6 = (bf16[512,512]{1,0:T(8,128)(2,1)}, bf16[512,512]{1,0:T(8,128)(2,1)}, u32[]{:S(2)}, u32[]{:S(2)}) collective-permute-start(bf16[512,512]{1,0:T(8,128)(2,1)} %get-tuple-element.70.refs_0_), channel_id=1, source_target_pairs={{0,2},{1,3},{2,0},{3,1},{4,6},{5,7},{6,4},{7,5},{8,10},{9,11},{10,... | collective-permute-start | bytes 1572872 | tf_op jit(solution)/shard_map/ppermute | solution.py:19
  6.2 33.7 %collective-permute-start.7 = (bf16[512,512]{1,0:T(8,128)(2,1)}, bf16[512,512]{1,0:T(8,128)(2,1)}, u32[]{:S(2)}, u32[]{:S(2)}) collective-permute-start(bf16[512,512]{1,0:T(8,128)(2,1)} %get-tuple-element.70.refs_0_), channel_id=1, source_target_pairs={{0,1},{1,0},{2,3},{3,2},{4,5},{5,4},{6,7},{7,6},{8,9},{9,8},{10,11... | collective-permute-start | bytes 1572872 | tf_op jit(solution)/shard_map/ppermute | solution.py:19
  18.5 21.5 %collective-permute-start.8 = (bf16[512,512]{1,0:T(8,128)(2,1)}, bf16[512,512]{1,0:T(8,128)(2,1)}, u32[]{:S(2)}, u32[]{:S(2)}) collective-permute-start(bf16[512,512]{1,0:T(8,128)(2,1)} %collective-permute-done.6.refs_1_), channel_id=1, source_target_pairs={{0,1},{1,0},{2,3},{3,2},{4,5},{5,4},{6,7},{7,6},{8,9},{9,8},{10,11... | collective-permute-start | bytes 1572872 | tf_op jit(solution)/shard_map/ppermute | solution.py:19
  18.5 30.8 %collective-permute-start.1 = (bf16[512,512]{1,0:T(8,128)(2,1)}, bf16[512,512]{1,0:T(8,128)(2,1)}, u32[]{:S(2)}, u32[]{:S(2)}) collective-permute-start(bf16[512,512]{1,0:T(8,128)(2,1)} %get-tuple-element.69.refs_0_), channel_id=1, source_target_pairs={{0,2},{1,3},{2,0},{3,1},{4,6},{5,7},{6,4},{7,5},{8,10},{9,11},{10,... | collective-permute-start | bytes 1572872 | tf_op jit(solution)/shard_map/ppermute | solution.py:19
  20.8 10.5 %all-to-all-start = ((f32[4,1,1024]{2,1,0:T(1,128)}), f32[4,1,1024]{2,1,0:T(1,128)S(1)}, u32[]{:S(2)}, u32[]{:S(2)}) async-start(f32[4,1,1024]{2,1,0:T(1,128)} %all_to_all.20), calls=%async_computation | async-start | bytes 32768 | tf_op jit(solution)/shard_map/all_to_all | solution.py:78
  31.3 3.8 %collective-permute-start = (f32[4,1024]{1,0:T(4,128)S(1)}, f32[4,1024]{1,0:T(4,128)S(1)}, u32[]{:S(2)}, u32[]{:S(2)}) collective-permute-start(f32[4,1024]{1,0:T(4,128)S(1)} %bitcast.12), channel_id=1, source_target_pairs={{0,4},{4,0},{8,12},{12,8},{16,20},{20,16},{24,28},{28,24},{1,5},{5... | collective-permute-start | bytes 49160 | tf_op jit(solution)/shard_map/ppermute | solution.py:19
  33.1 5.6 %copy-start.10 = (f32[64]{0:T(128)S(1)}, f32[64]{0:T(128)}, u32[]{:S(2)}) copy-start(f32[64]{0:T(128)} %param.24) | copy-start | bytes 772
  33.2 5.7 %copy-start.11 = (f32[64]{0:T(128)S(1)}, f32[64]{0:T(128)}, u32[]{:S(2)}) copy-start(f32[64]{0:T(128)} %param.25) | copy-start | bytes 772
  35.1 3.7 %collective-permute-start.4 = (f32[1,1024]{1,0:T(1,128)S(1)}, f32[1,1024]{1,0:T(1,128)S(1)}, u32[]{:S(2)}, u32[]{:S(2)}) collective-permute-start(f32[1,1024]{1,0:T(1,128)S(1)} %bitcast.14), channel_id=1, source_target_pairs={{0,2},{1,3},{2,0},{3,1},{4,6},{5,7},{6,4},{7,5},{8,10},{9,11},{10,... | collective-permute-start | bytes 12296 | tf_op jit(solution)/shard_map/ppermute | solution.py:19
  38.8 1.2 collective-permute-start.5
  44.9 19.3 %all-to-all-start.2 = ((bf16[4,128,512]{2,1,0:T(8,128)(2,1)}), bf16[4,128,512]{2,1,0:T(8,128)(2,1)}, u32[]{:S(2)}, u32[]{:S(2)}) async-start(bf16[4,128,512]{2,1,0:T(8,128)(2,1)} %get-tuple-element.48), calls=%async_computation.2 | async-start | bytes 1048576 | tf_op jit(solution)/shard_map/all_to_all | solution.py:78
  49.0 7.5 %collective-permute-start.2 = (bf16[512,512]{1,0:T(8,128)(2,1)}, bf16[512,512]{1,0:T(8,128)(2,1)S(1)}, u32[]{:S(2)}, u32[]{:S(2)}) collective-permute-start(bf16[512,512]{1,0:T(8,128)(2,1)} %get-tuple-element.69.refs_0_), channel_id=1, source_target_pairs={{0,1},{1,0},{2,3},{3,2},{4,5},{5,4},{6,7},{7,6},{8,9},{9,8},{10,11... | collective-permute-start | bytes 1572872 | tf_op jit(solution)/shard_map/ppermute | solution.py:19
  49.3 7.3 %collective-permute-start.3 = (bf16[512,512]{1,0:T(8,128)(2,1)}, bf16[512,512]{1,0:T(8,128)(2,1)S(1)}, u32[]{:S(2)}, u32[]{:S(2)}) collective-permute-start(bf16[512,512]{1,0:T(8,128)(2,1)} %collective-permute-done.1.refs_1_), channel_id=1, source_target_pairs={{0,1},{1,0},{2,3},{3,2},{4,5},{5,4},{6,7},{7,6},{8,9},{9,8},{10,11... | collective-permute-start | bytes 1572872 | tf_op jit(solution)/shard_map/ppermute | solution.py:19
  56.5 0.8 copy-start.12
  56.6 1.0 copy-start.13
  64.2 38.5 %all-to-all-start.1 = ((bf16[4,64,1024]{2,1,0:T(8,128)(2,1)}), bf16[4,64,1024]{2,1,0:T(8,128)(2,1)}, u32[]{:S(2)}, u32[]{:S(2)}) async-start(bf16[4,64,1024]{2,1,0:T(8,128)(2,1)} %get-tuple-element.47), calls=%async_computation.1 | async-start | bytes 1048576 | tf_op jit(solution)/shard_map/all_to_all | solution.py:78
  69.0 37.3 %collective-permute-start.12 = (bf16[4,128,512]{2,1,0:T(8,128)(2,1)}, bf16[4,128,512]{2,1,0:T(8,128)(2,1)}, u32[]{:S(2)}, u32[]{:S(2)}) collective-permute-start(bf16[4,128,512]{2,1,0:T(8,128)(2,1)} %all-to-all-done.2.refs_1_), channel_id=1, source_target_pairs={{0,4},{4,0},{8,12},{12,8},{16,20},{20,16},{24,28},{28,24},{1,5},{5... | collective-permute-start | bytes 1572872 | tf_op jit(solution)/shard_map/ppermute | solution.py:19
  69.9 20.6 %collective-permute-start.9 = (bf16[128,512]{1,0:T(8,128)(2,1)}, bf16[128,512]{1,0:T(8,128)(2,1)S(1)}, u32[]{:S(2)}, u32[]{:S(2)}) collective-permute-start(bf16[128,512]{1,0:T(8,128)(2,1)} %get-tuple-element.50), channel_id=1, source_target_pairs={{0,8},{4,12},{8,0},{12,4},{16,24},{20,28},{24,16},{28,20},{1,9},{5... | collective-permute-start | bytes 393224 | tf_op jit(solution)/shard_map/ppermute | solution.py:19
  72.5 20.6 %collective-permute-start.10 = (bf16[128,512]{1,0:T(8,128)(2,1)}, bf16[128,512]{1,0:T(8,128)(2,1)S(1)}, u32[]{:S(2)}, u32[]{:S(2)}) collective-permute-start(bf16[128,512]{1,0:T(8,128)(2,1)} %get-tuple-element.51), channel_id=1, source_target_pairs={{0,16},{4,20},{8,24},{12,28},{16,0},{20,4},{24,8},{28,12},{1,17},{... | collective-permute-start | bytes 393224 | tf_op jit(solution)/shard_map/ppermute | solution.py:19
  74.9 13.2 %copy-start.14 = (bf16[128,512]{1,0:T(8,128)(2,1)S(1)}, bf16[128,512]{1,0:T(8,128)(2,1)}, u32[]{:S(2)}) copy-start(bf16[128,512]{1,0:T(8,128)(2,1)} %get-tuple-element.49.refs_2_) | copy-start | bytes 393220
  74.9 18.3 %copy-start.4 = (bf16[256,2048]{1,0:T(8,128)(2,1)S(1)}, bf16[256,2048]{1,0:T(8,128)(2,1)}, u32[]{:S(2)}) copy-start(bf16[256,2048]{1,0:T(8,128)(2,1)} %refs_0_.3) | copy-start | bytes 3145732
  74.9 18.8 %copy-start.3 = (bf16[256,2048]{1,0:T(8,128)(2,1)S(1)}, bf16[256,2048]{1,0:T(8,128)(2,1)}, u32[]{:S(2)}) copy-start(bf16[256,2048]{1,0:T(8,128)(2,1)} %refs_0_.2) | copy-start | bytes 3145732
  74.9 24.6 %copy-start.8 = (f32[256]{0:T(256)S(1)}, f32[256]{0:T(256)}, u32[]{:S(2)}) copy-start(f32[256]{0:T(256)} %param.29) | copy-start | bytes 3076
  74.9 18.8 %collective-permute-start.11 = (bf16[128,512]{1,0:T(8,128)(2,1)}, bf16[128,512]{1,0:T(8,128)(2,1)S(1)}, u32[]{:S(2)}, u32[]{:S(2)}) collective-permute-start(bf16[128,512]{1,0:T(8,128)(2,1)} %get-tuple-element.52), channel_id=1, source_target_pairs={{0,24},{4,28},{8,16},{12,20},{16,8},{20,12},{24,0},{28,4},{1,25},{... | collective-permute-start | bytes 393224 | tf_op jit(solution)/shard_map/ppermute | solution.py:19
  81.9 6.1 %collective-permute-start.21 = (bf16[256,128]{1,0:T(8,128)(2,1)}, bf16[256,128]{1,0:T(8,128)(2,1)S(1)}, u32[]{:S(2)}, u32[]{:S(2)}) collective-permute-start(bf16[256,128]{1,0:T(8,128)(2,1)} %get-tuple-element.64), channel_id=1, source_target_pairs={{0,4},{4,8},{8,12},{12,16},{16,20},{20,24},{24,28},{1,5},{5,9},{9,... | collective-permute-start | bytes 196616 | tf_op jit(solution)/shard_map/ppermute | solution.py:596
  88.0 11.6 %copy-start.5 = (bf16[256,128]{1,0:T(8,128)(2,1)}, bf16[256,128]{1,0:T(8,128)(2,1)S(1)}, u32[]{:S(2)}) copy-start(bf16[256,128]{1,0:T(8,128)(2,1)S(1)} %collective-permute-done.21.refs_4_) | copy-start | bytes 196612
  88.0 7.2 %collective-permute-start.13 = (bf16[128,512]{1,0:T(8,128)(2,1)S(1)}, bf16[128,512]{1,0:T(8,128)(2,1)S(1)}, u32[]{:S(2)}, u32[]{:S(2)}) collective-permute-start(bf16[128,512]{1,0:T(8,128)(2,1)S(1)} %copy-done.14), channel_id=1, source_target_pairs={{0,4},{4,0},{8,12},{12,8},{16,20},{20,16},{24,28},{28,24},{1,5},{5... | collective-permute-start | bytes 393224 | tf_op jit(solution)/shard_map/ppermute | solution.py:19
  90.4 15.9 %copy-start.15 = (bf16[128,512]{1,0:T(8,128)(2,1)}, bf16[128,512]{1,0:T(8,128)(2,1)S(1)}, u32[]{:S(2)}) copy-start(bf16[128,512]{1,0:T(8,128)(2,1)S(1)} %collective-permute-done.9.refs_3_) | copy-start | bytes 393220
  90.4 6.6 %collective-permute-start.14 = (bf16[128,512]{1,0:T(8,128)(2,1)S(1)}, bf16[128,512]{1,0:T(8,128)(2,1)S(1)}, u32[]{:S(2)}, u32[]{:S(2)}) collective-permute-start(bf16[128,512]{1,0:T(8,128)(2,1)S(1)} %collective-permute-done.9.refs_3_), channel_id=1, source_target_pairs={{0,4},{4,0},{8,12},{12,8},{16,20},{20,16},{24,28},{28,24},{1,5},{5... | collective-permute-start | bytes 393224 | tf_op jit(solution)/shard_map/ppermute | solution.py:19
  93.2 13.2 %copy-start.16 = (bf16[128,512]{1,0:T(8,128)(2,1)}, bf16[128,512]{1,0:T(8,128)(2,1)S(1)}, u32[]{:S(2)}) copy-start(bf16[128,512]{1,0:T(8,128)(2,1)S(1)} %collective-permute-done.10.refs_4_) | copy-start | bytes 393220
  93.2 39.5 %collective-permute-start.17 = (bf16[256,2048]{1,0:T(8,128)(2,1)S(1)}, bf16[256,2048]{1,0:T(8,128)(2,1)}, u32[]{:S(2)}, u32[]{:S(2)}) collective-permute-start(bf16[256,2048]{1,0:T(8,128)(2,1)S(1)} %copy-done.4), channel_id=1, source_target_pairs={{0,2},{1,3},{2,0},{3,1},{4,6},{5,7},{6,4},{7,5},{8,10},{9,11},{10,... | collective-permute-start | bytes 3145736 | tf_op jit(solution)/shard_map/ppermute | solution.py:19
  93.7 12.7 %copy-start.17 = (bf16[128,512]{1,0:T(8,128)(2,1)}, bf16[128,512]{1,0:T(8,128)(2,1)S(1)}, u32[]{:S(2)}) copy-start(bf16[128,512]{1,0:T(8,128)(2,1)S(1)} %collective-permute-done.11.refs_5_) | copy-start | bytes 393220
  93.7 48.0 %collective-permute-start.18 = (bf16[256,2048]{1,0:T(8,128)(2,1)S(1)}, bf16[256,2048]{1,0:T(8,128)(2,1)}, u32[]{:S(2)}, u32[]{:S(2)}) collective-permute-start(bf16[256,2048]{1,0:T(8,128)(2,1)S(1)} %copy-done.3), channel_id=1, source_target_pairs={{0,2},{1,3},{2,0},{3,1},{4,6},{5,7},{6,4},{7,5},{8,10},{9,11},{10,... | collective-permute-start | bytes 3145736 | tf_op jit(solution)/shard_map/ppermute | solution.py:19
  95.3 4.1 %copy-start.18 = (bf16[128,512]{1,0:T(8,128)(2,1)}, bf16[128,512]{1,0:T(8,128)(2,1)S(1)}, u32[]{:S(2)}) copy-start(bf16[128,512]{1,0:T(8,128)(2,1)S(1)} %collective-permute-done.13.refs_7_) | copy-start | bytes 393220
  95.3 11.1 %collective-permute-start.15 = (bf16[128,512]{1,0:T(8,128)(2,1)S(1)}, bf16[128,512]{1,0:T(8,128)(2,1)S(1)}, u32[]{:S(2)}, u32[]{:S(2)}) collective-permute-start(bf16[128,512]{1,0:T(8,128)(2,1)S(1)} %collective-permute-done.10.refs_4_), channel_id=1, source_target_pairs={{0,4},{4,0},{8,12},{12,8},{16,20},{20,16},{24,28},{28,24},{1,5},{5... | collective-permute-start | bytes 393224 | tf_op jit(solution)/shard_map/ppermute | solution.py:19
  97.0 5.7 %copy-start.19 = (bf16[128,512]{1,0:T(8,128)(2,1)}, bf16[128,512]{1,0:T(8,128)(2,1)S(1)}, u32[]{:S(2)}) copy-start(bf16[128,512]{1,0:T(8,128)(2,1)S(1)} %collective-permute-done.14.refs_8_) | copy-start | bytes 393220
  97.0 9.3 %collective-permute-start.16 = (bf16[128,512]{1,0:T(8,128)(2,1)S(1)}, bf16[128,512]{1,0:T(8,128)(2,1)}, u32[]{:S(2)}, u32[]{:S(2)}) collective-permute-start(bf16[128,512]{1,0:T(8,128)(2,1)S(1)} %collective-permute-done.11.refs_5_), channel_id=1, source_target_pairs={{0,4},{4,0},{8,12},{12,8},{16,20},{20,16},{24,28},{28,24},{1,5},{5... | collective-permute-start | bytes 393224 | tf_op jit(solution)/shard_map/ppermute | solution.py:19
  102.7 41.7 %all-to-all-start.4 = ((bf16[4,256,256]{2,1,0:T(8,128)(2,1)}), bf16[4,256,256]{2,1,0:T(8,128)(2,1)S(1)}, u32[]{:S(2)}, u32[]{:S(2)}) async-start(bf16[4,256,256]{2,1,0:T(8,128)(2,1)} %shard_map.159), calls=%async_computation.4 | async-start | bytes 1048576 | tf_op jit(solution)/shard_map/all_to_all | solution.py:606
  106.3 0.7 copy-start.20
  141.7 11.2 %collective-permute-start.22 = (bf16[256,2048]{1,0:T(8,128)(2,1)S(1)}, bf16[256,2048]{1,0:T(8,128)(2,1)}, u32[]{:S(2)}, u32[]{:S(2)}) collective-permute-start(bf16[256,2048]{1,0:T(8,128)(2,1)S(1)} %copy-done.3), channel_id=1, source_target_pairs={{0,1},{1,0},{2,3},{3,2},{4,5},{5,4},{6,7},{7,6},{8,9},{9,8},{10,11... | collective-permute-start | bytes 3145736 | tf_op jit(solution)/shard_map/ppermute | solution.py:19
  141.7 11.2 %collective-permute-start.23 = (bf16[256,2048]{1,0:T(8,128)(2,1)}, bf16[256,2048]{1,0:T(8,128)(2,1)}, u32[]{:S(2)}, u32[]{:S(2)}) collective-permute-start(bf16[256,2048]{1,0:T(8,128)(2,1)} %collective-permute-done.18.refs_1_), channel_id=1, source_target_pairs={{0,1},{1,0},{2,3},{3,2},{4,5},{5,4},{6,7},{7,6},{8,9},{9,8},{10,11... | collective-permute-start | bytes 3145736 | tf_op jit(solution)/shard_map/ppermute | solution.py:19
  142.2 25.8 %collective-permute-start.19 = (bf16[256,2048]{1,0:T(8,128)(2,1)S(1)}, bf16[256,2048]{1,0:T(8,128)(2,1)}, u32[]{:S(2)}, u32[]{:S(2)}) collective-permute-start(bf16[256,2048]{1,0:T(8,128)(2,1)S(1)} %copy-done.4), channel_id=1, source_target_pairs={{0,1},{1,0},{2,3},{3,2},{4,5},{5,4},{6,7},{7,6},{8,9},{9,8},{10,11... | collective-permute-start | bytes 3145736 | tf_op jit(solution)/shard_map/ppermute | solution.py:19
  142.2 25.8 %collective-permute-start.20 = (bf16[256,2048]{1,0:T(8,128)(2,1)}, bf16[256,2048]{1,0:T(8,128)(2,1)}, u32[]{:S(2)}, u32[]{:S(2)}) collective-permute-start(bf16[256,2048]{1,0:T(8,128)(2,1)} %collective-permute-done.17.refs_1_), channel_id=1, source_target_pairs={{0,1},{1,0},{2,3},{3,2},{4,5},{5,4},{6,7},{7,6},{8,9},{9,8},{10,11... | collective-permute-start | bytes 3145736 | tf_op jit(solution)/shard_map/ppermute | solution.py:19
  144.4 8.5 %copy-start.1 = (bf16[4,256,256]{2,1,0:T(8,128)(2,1)}, bf16[4,256,256]{2,1,0:T(8,128)(2,1)S(1)}, u32[]{:S(2)}) copy-start(bf16[4,256,256]{2,1,0:T(8,128)(2,1)S(1)} %all-to-all-done.4.piece_ref) | copy-start | bytes 1572868
  144.4 23.6 %all-to-all-start.3 = ((bf16[16,64,256]{2,1,0:T(8,128)(2,1)}), bf16[16,64,256]{2,1,0:T(8,128)(2,1)S(1)}, u32[]{:S(2)}, u32[]{:S(2)}) async-start(bf16[16,64,256]{2,1,0:T(8,128)(2,1)} %shard_map.157), calls=%async_computation.3 | async-start | bytes 1048576 | tf_op jit(solution)/shard_map/all_to_all | solution.py:610
  168.0 0.8 copy-start.2

commit v3 on v2

--- a/solution.py
+++ b/solution.py
@@ -96,131 +96,99 @@
     )(*[in_hbm(w) for w in weights])
 
 
-def project(ids, chunks, squares, weights, finish, out_shape, extra):
-    rows, features = chunks[0][0].shape
-    resident = not isinstance(weights, (list, tuple))
-    weight_count = weights.shape[0] if resident else len(weights)
-    width, channels = weights.shape[1:] if resident else weights[0].shape
-    chunk_count, count = len(chunks), len(chunks[0])
-    pieces = [piece for chunk in chunks for piece in chunk]
-    weight_list = [weights] if resident else list(weights)
+def project(ids, pieces, squares, head_weights, conv_weights, gains, earlier, head_dim, slot_step, split, heads, conv):
+    rows, features = pieces[0].shape
+    _, width, attn_width = head_weights.shape
+    channels = conv_weights[0].shape[1]
+    head_count = attn_width // head_dim
+    count = len(pieces)
+    tail = min(128, rows)
+    before = 0 if earlier is None else earlier.shape[2]
+    earlier_list = [] if earlier is None else [earlier]
+    pair_count = head_count if split else 1
 
     def body(ids_ref, *refs):
-        piece_refs, refs = refs[: len(pieces)], refs[len(pieces) :]
-        squares_ref, refs = refs[0], refs[1:]
-        weight_refs, refs = refs[: len(weight_list)], refs[len(weight_list) :]
-        extra_refs, refs = refs[: len(extra)], refs[len(extra) :]
-        outs, refs = refs[: len(out_shape)], refs[len(out_shape) :]
-        held, product_store, joined = refs[:3]
+        piece_refs, refs = refs[:count], refs[count:]
+        squares_ref, head_ref, refs = refs[0], refs[1], refs[2:]
+        conv_refs, refs = refs[:3], refs[3:]
+        query_gain_ref, key_gain_ref, refs = refs[0], refs[1], refs[2:]
+        earlier_refs, refs = refs[: len(earlier_list)], refs[len(earlier_list) :]
+        if heads:
+            query_out, pair_outs, refs = refs[0], refs[1 : 1 + pair_count], refs[1 + pair_count :]
+        if conv:
+            outer_out, gated_out, tail_out = refs[:3]
+            refs = refs[3:]
+        held, product, weight_store, joined, arrived = refs
         copies = []
-        for chunk in range(chunk_count):
-            for place, offset in enumerate(xor_offsets(count)):
-                start = pl.multiple_of((ids_ref[1] ^ offset) * features, features)
-                index = chunk * count + place
-                copies.append(
-                    pltpu.make_async_copy(
-                        piece_refs[index], held.at[chunk, :, pl.ds(start, features)], joined.at[index]
-                    )
-                )
-        for copy in copies[:count]:
-            copy.start()
-        if not resident:
-            weight_store, arrived = refs[3:]
-            arrival = Arrival(weight_refs, weight_store, arrived)
-        for copy in copies[count:]:
-            copy.start()
-        for chunk in range(chunk_count):
-            for copy in copies[chunk * count : (chunk + 1) * count]:
-                copy.wait()
-            span = slice(chunk * rows, (chunk + 1) * rows)
-            row_scale = lax.rsqrt(squares_ref[:, span] / width + NORM_EPSILON)
-            for index in range(weight_count):
-                if not resident and chunk == 0:
-                    arrival.wait(index)
-                weight = weight_refs[0][index] if resident else weight_store[index]
-                product_store[index] = dot_nn(held[chunk], weight).T * row_scale
-                finish(ids_ref, chunk, index, product_store, extra_refs, outs)
-
-    scratch = [
-        pltpu.VMEM((chunk_count, rows, width), BF16),
-        pltpu.VMEM((weight_count, channels, rows), F32),
-        pltpu.SemaphoreType.DMA((len(pieces),)),
-    ]
-    if not resident:
-        scratch += [pltpu.VMEM((weight_count, width, channels), BF16), pltpu.SemaphoreType.DMA((weight_count,))]
-    return vmem_call(
-        body,
-        out_shape,
-        [ids, *pieces, squares, *weight_list, *extra],
-        scalars=1,
-        scratch=scratch,
-        flops=2 * weight_count * channels * rows * chunk_count * width,
-        limit=24,
-        outside=pieces if resident else (*weights, *pieces),
-        resident=weight_list if resident else (),
-    )
-
-
-def project_heads(ids, pieces, squares, weights, gains, earlier, head_dim, slot_step, split):
-    rows = pieces[0].shape[0]
-    head_count = weights.shape[2] // head_dim
-    before = 0 if earlier is None else earlier.shape[2]
-
-    def finish(ids_ref, chunk, index, product, extra_refs, outs):
-        query_out, pair_outs = outs[0], outs[1:]
-        if index == 0 and before:
-            query_out[:, :, :before] = extra_refs[2][...]
+        for place, (offset, piece_ref) in enumerate(zip(xor_offsets(count), piece_refs)):
+            start = pl.multiple_of((ids_ref[1] ^ offset) * features, features)
+            copies.append(pltpu.make_async_copy(piece_ref, held.at[:, pl.ds(start, features)], joined.at[place]))
+            copies[-1].start()
+        if conv:
+            arrival = Arrival(conv_refs, weight_store, arrived)
+        row_scale = lax.rsqrt(squares_ref[...] / width + NORM_EPSILON)
+        if heads and before:
+            query_out[:, :, :before] = earlier_refs[0][...]
         own_slot = ids_ref[0] // slot_step
-        for head in range(head_count):
-            base = head * head_dim
-            if split and index:
-                base = pl.multiple_of((own_slot ^ head) * head_dim, head_dim)
-            part = product[index, pl.ds(base, head_dim), :]
-            if index == 0:
-                query_out[head, :, before:] = (column_norm(part) * extra_refs[0][...]).astype(BF16)
-                continue
-            settled = (column_norm(part) * extra_refs[1][...] if index == 1 else part).astype(BF16)
-            span = slice((index - 1) * head_dim, index * head_dim)
-            if split:
-                pair_outs[head][span, :] = settled
-            else:
-                pair_outs[0][head, span, :] = settled
-
-    out_shape = [jax.ShapeDtypeStruct((head_count, head_dim, before + rows), BF16)]
+        for copy in copies:
+            copy.wait()
+        for index in range(3 if heads else 0):
+            product[index] = dot_nn(held[...], head_ref[index]).T * row_scale
+            for head in range(head_count):
+                base = head * head_dim
+                if split and index:
+                    base = pl.multiple_of((own_slot ^ head) * head_dim, head_dim)
+                part = product[index, pl.ds(base, head_dim), :]
+                if index == 0:
+                    query_out[head, :, before:] = (column_norm(part) * query_gain_ref[...]).astype(BF16)
+                    continue
+                settled = (column_norm(part) * key_gain_ref[...] if index == 1 else part).astype(BF16)
+                span = slice((index - 1) * head_dim, index * head_dim)
+                if split:
+                    pair_outs[head][span, :] = settled
+                else:
+                    pair_outs[0][head, span, :] = settled
+        if not conv:
+            return
+        for index in range(3):
+            arrival.wait(index)
+        outer_out[...] = dot_nn(held[...], weight_store[0]).T * row_scale
+        inner = dot_nn(held[...], weight_store[1]).T * row_scale
+        gated = (inner * (dot_nn(held[...], weight_store[2]).T * row_scale)).astype(BF16)
+        gated_out[...] = gated
+        tail_out[...] = gated[:, rows - tail :]
+
+    head_shape = [jax.ShapeDtypeStruct((head_count, head_dim, before + rows), BF16)]
     if split:
-        out_shape += [jax.ShapeDtypeStruct((2 * head_dim, rows), BF16)] * head_count
+        head_shape += [jax.ShapeDtypeStruct((2 * head_dim, rows), BF16)] * head_count
     else:
-        out_shape += [jax.ShapeDtypeStruct((head_count, 2 * head_dim, rows), BF16)]
-    extra = [*gains] + ([earlier] if before else [])
-    outs = project(ids, [pieces], squares, weights, finish, out_shape, extra)
-    return outs[0], outs[1:]
-
-
-def project_conv(ids, chunks, squares, weights):
-    chunk_rows = chunks[0][0].shape[0]
-    rows = chunk_rows * len(chunks)
-    channels = weights[0].shape[1]
-    tail = min(128, chunk_rows)
-
-    def finish(ids_ref, chunk, index, product, extra_refs, outs):
-        span = slice(chunk * chunk_rows, (chunk + 1) * chunk_rows)
-        if index == 0:
-            outs[0][:, span] = product[0]
-        elif index == 2:
-            gated = (product[1] * product[2]).astype(BF16)
-            outs[1][:, span] = gated
-            if chunk == len(chunks) - 1:
-                outs[2][...] = gated[:, chunk_rows - tail :]
-
-    out_shape = [
+        head_shape += [jax.ShapeDtypeStruct((head_count, 2 * head_dim, rows), BF16)]
+    conv_shape = [
         jax.ShapeDtypeStruct((channels, rows), F32),
         jax.ShapeDtypeStruct((channels, rows), BF16),
         jax.ShapeDtypeStruct((channels, tail), BF16),
     ]
-    return project(ids, chunks, squares, weights, finish, out_shape, [])
-
-
-def finish_conv(outers, gateds, prior, taps, gain, group, tile_count):
+    outs = vmem_call(
+        body,
+        (head_shape if heads else []) + (conv_shape if conv else []),
+        [ids, *pieces, squares, head_weights, *conv_weights, *gains, *earlier_list],
+        scalars=1,
+        scratch=[
+            pltpu.VMEM((rows, width), BF16),
+            pltpu.VMEM((3, attn_width, rows), F32),
+            pltpu.VMEM((3, width, channels), BF16),
+            pltpu.SemaphoreType.DMA((count,)),
+            pltpu.SemaphoreType.DMA((3,)),
+        ],
+        flops=2 * 3 * (attn_width + channels) * rows * width,
+        limit=28,
+        outside=(*conv_weights, *pieces) if heads else (*conv_weights, *pieces, head_weights),
+        resident=(head_weights,) if heads else (),
+    )
+    return outs
+
+
+def finish_conv(ids, outers, gateds, prior, taps, gain, group, tile_count):
     channels, chunk_rows = gateds[0].shape
     count = len(gateds)
     rows = chunk_rows * count
@@ -228,9 +196,10 @@
     tap_count = taps.shape[1]
     tile_rows = rows // tile_count
 
-    def body(*refs):
+    def body(ids_ref, *refs):
         outer_refs, gated_refs = refs[:count], refs[count : 2 * count]
-        prior_ref, taps_ref, gain_ref, out = refs[2 * count :]
+        prior_ref, taps_ref, gain_ref = refs[2 * count : 2 * count + 3]
+        outs, out = refs[2 * count + 3 : -1], refs[-1]
         lane = lax.broadcasted_iota(jnp.int32, (group, tail), 1)
         for index in range(channels // group):
             span = slice(index * group, (index + 1) * group)
@@ -247,11 +216,15 @@
             mixed = (column_norm(outer * total) * gain_ref[span, :]).astype(BF16)
             for tile in range(tile_count):
                 out[tile, span, :] = mixed[:, tile * tile_rows : (tile + 1) * tile_rows]
+        for ref, offset in zip(outs, xor_offsets(tile_count)):
+            ref[...] = out[ids_ref[1] ^ offset]
 
     return vmem_call(
         body,
-        jax.ShapeDtypeStruct((tile_count, channels, tile_rows), BF16),
-        [*outers, *gateds, prior, taps, gain],
+        [jax.ShapeDtypeStruct((channels, tile_rows), BF16)] * tile_count,
+        [ids, *outers, *gateds, prior, taps, gain],
+        scalars=1,
+        scratch=[pltpu.VMEM((tile_count, channels, tile_rows), BF16)],
         flops=1 << 20,
     )
 
@@ -429,9 +402,14 @@
     )
 
 
-def output_rows(ids, pieces, weights, base):
+def output_rows(ids, pieces, weights, base, early=None):
     source_count = len(weights)
-    piece_count, piece_height, rows = pieces.shape
+    early_count = 0 if early is None else early.shape[0]
+    early_list = [early] if early_count else []
+    weights = weights[early_count:]
+    listed = isinstance(pieces, (list, tuple))
+    piece_list = list(pieces) if listed else [pieces]
+    piece_count, piece_height, rows = (len(pieces), *pieces[0].shape) if listed else pieces.shape
     slot_count = piece_count // source_count
     height = slot_count * piece_height
     width = weights[0].shape[1]
@@ -440,8 +418,10 @@
     parts = OUTPUT_PARTS
     part_width = width // parts
 
-    def body(ids_ref, piece_ref, *refs):
-        weight_refs, refs = refs[:source_count], refs[source_count:]
+    def body(ids_ref, *refs):
+        piece_refs, refs = refs[: len(piece_list)], refs[len(piece_list) :]
+        early_refs, refs = refs[: len(early_list)], refs[len(early_list) :]
+        weight_refs, refs = refs[: len(weights)], refs[len(weights) :]
         base_refs, refs = refs[: len(bases)], refs[len(bases) :]
         out_ref, held, weight_store, result, joined, arrived, left = refs[:7]
         gathers = []
@@ -451,7 +431,7 @@
                 start = place * height + slot * piece_height
                 gathers.append(
                     pltpu.make_async_copy(
-                        piece_ref.at[slot * source_count + source],
+                        piece_refs[place] if listed else piece_refs[0].at[slot * source_count + source],
                         held.at[start : start + piece_height, :],
                         joined.at[place * slot_count + slot],
                     )
@@ -464,14 +444,16 @@
         for copy in gathers:
             copy.wait()
         turned = held[...].T
-        for place in range(source_count):
+        for place in range(len(weights)):
             arrival.wait(place)
         if bases:
             below.wait()
         stores = []
         for part in range(parts):
             span = slice(part * part_width, (part + 1) * part_width)
-            weight = jnp.concatenate([weight_store[place, :, span] for place in range(source_count)], axis=0)
+            slices = [early_refs[0][place, :, span] for place in range(early_count)]
+            slices += [weight_store[place, :, span] for place in range(len(weights))]
+            weight = jnp.concatenate(slices, axis=0)
             total = dot_nn(turned, weight)
             if bases:
                 total = total + refs[7][:, span].astype(F32)
@@ -483,10 +465,10 @@
 
     scratch = [
         pltpu.VMEM((source_count * height, rows), BF16),
-        pltpu.VMEM((source_count, height, width), BF16),
+        pltpu.VMEM((len(weights), height, width), BF16),
         pltpu.VMEM((rows, width), BF16),
         pltpu.SemaphoreType.DMA((piece_count,)),
-        pltpu.SemaphoreType.DMA((source_count,)),
+        pltpu.SemaphoreType.DMA((len(weights),)),
         pltpu.SemaphoreType.DMA((parts,)),
     ]
     if bases:
@@ -494,11 +476,12 @@
     return vmem_call(
         body,
         jax.ShapeDtypeStruct((rows, width), BF16),
-        [ids, pieces, *weights, *bases],
+        [ids, *piece_list, *early_list, *weights, *bases],
         scalars=1,
         scratch=scratch,
         flops=2 * source_count * height * rows * width,
-        outside=(pieces, *weights, *bases),
+        outside=(*piece_list, *weights, *bases),
+        resident=early_list,
         out_space=pl.ANY,
     )
 
@@ -570,19 +553,16 @@
             bit >>= 1
         chunks.append(pieces)
 
-    queries, outers, gateds = None, [], []
+    queries, conv_outs = None, [None] * ROW_CHUNKS
     pairs = [[] for _ in range(lane_count)]
     for c in range(ROW_CHUNKS):
         chunk_squares = squares[:, c * chunk_rows : (c + 1) * chunk_rows]
         split = c > 0
+        shared = (ids, chunks[c], chunk_squares, attn_weight, conv_weight, gains, queries, head_dim, lane_count, split)
+        outs = project(*shared, True, split)
+        queries, own_pairs = outs[0], outs[1 : 1 + (head_count if split else 1)]
         if split:
-            chunk_squares, outers[-1] = lax.optimization_barrier((chunk_squares, outers[-1]))
-        queries, own_pairs = project_heads(
-            ids, chunks[c], chunk_squares, attn_weight, gains, queries, head_dim, lane_count, split
-        )
-        outer, gated, gated_tail = project_conv(ids, [chunks[c]], chunk_squares, conv_weight)
-        outers.append(outer)
-        gateds.append(gated)
+            conv_outs[c] = outs[-3:]
         if split:
             moved = [swapped(p, "sp", i * lane_count) if i else p for i, p in enumerate(own_pairs)]
         else:
@@ -593,7 +573,11 @@
             for p in moved:
                 through.append(swapped(p, "sp", lane))
             pairs[lane].append(through)
-    prior = lax.ppermute(gated_tail, "sp", [(i, i + 1) for i in range(sp_count - 1)])
+    conv_outs[0] = project(
+        ids, chunks[0], squares[:, :chunk_rows], attn_weight, conv_weight, gains, None, head_dim, lane_count, False, False, True
+    )
+    outers, gateds = [o[0] for o in conv_outs], [o[1] for o in conv_outs]
+    prior = lax.ppermute(conv_outs[-1][2], "sp", [(i, i + 1) for i in range(sp_count - 1)])
     queries = exchanged(queries, "sp", snaked)
 
     far_weights = lax.optimization_barrier((attn_out_weight, conv_out_weight, far[-1]))[:2]
@@ -601,9 +585,12 @@
     far_weights = [swapped(weight, "tp", half) for weight in far_weights]
 
     conv_mixed = finish_conv(
-        outers, gateds, prior, out_gains[2], out_gains[1], head_dim, tp_count
-    )
-    conv_pieces = lax.all_to_all(conv_mixed, "tp", 0, 0)
+        ids, outers, gateds, prior, out_gains[2], out_gains[1], head_dim, tp_count
+    )
+    conv_pieces = [
+        swapped(piece, "tp", offset) if offset else piece
+        for piece, offset in zip(conv_mixed, xor_offsets(tp_count))
+    ]
     attended = attend(
         ids, queries, pairs, gates, out_gains[0], lane_count, tp_count
     )
@@ -618,7 +605,8 @@
             bit >>= 1
         gathered.append(parts)
     base = output_rows(ids, conv_pieces, gathered[1], None)
-    return output_rows(ids, attn_pieces, gathered[0], base)
+    early = staged(gathered[0][: tp_count // 2])
+    return output_rows(ids, attn_pieces, gathered[0], base, early)
 
 
 def solution(mesh):

time: 175 us -> 186 us (1.063)
  the two profiles are of different devices: /device:TPU:0 before, /device:TPU:17 now
where the time goes in v3:
time: 186 us; the launch traced here: 185 us
  Pallas kernels  62.3 us (33%)
  starting transfers between devices  61.7 us (33%)
  waiting for transfers between devices  52 us (28%)
  local copies, waits for them, and re-layouts  5.8 us (3%)
  other arithmetic  2.75 us (1%)
    pallas_call x7, Pallas kernels, vmem_call(): pl.pallas_call(body, out_shape=shapes if many else shapes[0], in_specs=sp...  58.8 us
    ppermute x26, waiting for transfers between devices, swapped(): return lax.ppermute(shard, axis, [(i, i ^ offset) for i in range(devices)])  42.2 us
    ppermute x26, starting transfers between devices, swapped(): return lax.ppermute(shard, axis, [(i, i ^ offset) for i in range(devices)])  28.7 us
    all_to_all x3, starting transfers between devices, exchanged(): return lax.all_to_all(shard, axis, 0, 0, axis_index_groups=groups)  17.3 us
    all_to_all x1, starting transfers between devices, per_device(): lax.all_to_all(attended, ('sp', 'tp'), 0, 0, axis_index_groups=snaked_wide)  11.9 us
    ppermute x1, waiting for transfers between devices, per_device(): lax.ppermute(conv_outs[-1][2], 'sp', [(i, i + 1) for i in range(sp_count...  4.96 us
    all_to_all x3, waiting for transfers between devices, exchanged(): return lax.all_to_all(shard, axis, 0, 0, axis_index_groups=groups)  4.83 us
    unnamed x48, local copies, waits for them, and re-layouts  3.81 us
  transfers between devices with their start and end apart: 31, of which 14 were waited for; matrix products, arithmetic and copies ran while one was open for 1% of the time, Pallas kernels for 31%

profile of v3, /device:TPU:17, one launch (start us, length us, event | category | flops | bytes accessed | tf_op | source)
XLA Modules:
  0.0 185.1 jit_solution(8904020291926562947)
XLA Ops:
  0.0 0.8 dynamic_slice.3
  0.9 2.4 %multiply_convert_fusion = (bf16[512,512]{1,0:T(8,128)(2,1)}, bf16[512,512]{1,0:T(8,128)(2,1)}) fusion(bf16[1024,512]{1,0:T(8,128)(2,1)} %param.16, f32[512]{0:T(512)S(1)} %dynamic_slice.3), kind=kLoop, calls=%fused_computation.1 | loop fusion | flops 1572864 | bytes 2099200 | tf_op jit(solution)/shard_map/convert_element_type | solution.py:526
  3.3 1.2 collective-permute-start.6
  4.5 0.3 collective-permute-start.1
  4.7 1.2 collective-permute-start.7
  6.0 10.4 %collective-permute-done.6.refs_1_ = bf16[512,512]{1,0:T(8,128)(2,1)} collective-permute-done((bf16[512,512]{1,0:T(8,128)(2,1)}, bf16[512,512]{1,0:T(8,128)(2,1)}, u32[]{:S(2)}, u32[]{:S(2)}) %collective-permute-start.6) | collective-permute-done | bytes 524320 | tf_op jit(solution)/shard_map/ppermute | solution.py:19
  16.4 2.7 %collective-permute-start.8 = (bf16[512,512]{1,0:T(8,128)(2,1)}, bf16[512,512]{1,0:T(8,128)(2,1)}, u32[]{:S(2)}, u32[]{:S(2)}) collective-permute-start(bf16[512,512]{1,0:T(8,128)(2,1)} %collective-permute-done.6.refs_1_), channel_id=1, source_target_pairs={{0,1},{1,0},{2,3},{3,2},{4,5},{5,4},{6,7},{7,6},{8,9},{9,8},{10,11... | collective-permute-start | bytes 1572872 | tf_op jit(solution)/shard_map/ppermute | solution.py:19
  19.1 0.6 all_to_all.17
  19.7 4.6 %all-to-all-start = ((f32[4,1,1024]{2,1,0:T(1,128)}), f32[4,1,1024]{2,1,0:T(1,128)S(1)}, u32[]{:S(2)}, u32[]{:S(2)}) async-start(f32[4,1,1024]{2,1,0:T(1,128)} %all_to_all.17), calls=%async_computation | async-start | bytes 32768 | tf_op jit(solution)/shard_map/all_to_all | solution.py:78
  24.3 0.3 multiply_reduce_fusion
  24.6 2.5 %all-to-all-done = f32[4,1,1024]{2,1,0:T(1,128)S(1)} async-done(((f32[4,1,1024]{2,1,0:T(1,128)}), f32[4,1,1024]{2,1,0:T(1,128)S(1)}, u32[]{:S(2)}, u32[]{:S(2)}) %all-to-all-start) | async-done | bytes 16416 | tf_op jit(solution)/shard_map/all_to_all | solution.py:78
  27.1 1.2 collective-permute-start
  28.5 0.1 copy.33
  28.7 1.9 %staged.2.refs_5_ = bf16[3,2048,256]{2,1,0:T(8,128)(2,1)S(1)} custom-call(bf16[2048,256]{1,0:T(8,128)(2,1)} %refs_0_.1, bf16[2048,256]{1,0:T(8,128)(2,1)} %refs_1_.1, bf16[2048,256]{1,0:T(8,128)(2,1)} %refs_2_.1), custom_call_target="tpu_custom_call" | custom-call | tf_op jit(solution)/shard_map/staged/pallas_call | solution.py:88
  30.6 1.3 collective-permute-start.4
  31.9 1.2 collective-permute-done.4
  33.2 2.5 %collective-permute-start.5 = (f32[1,1024]{1,0:T(1,128)S(1)}, f32[1,1024]{1,0:T(1,128)S(1)}, u32[]{:S(2)}, u32[]{:S(2)}) collective-permute-start(f32[1,1024]{1,0:T(1,128)S(1)} %add.10), channel_id=1, source_target_pairs={{0,1},{1,0},{2,3},{3,2},{4,5},{5,4},{6,7},{7,6},{8,9},{9,8},{10,11... | collective-permute-start | bytes 12296 | tf_op jit(solution)/shard_map/ppermute | solution.py:19
  35.7 0.1 copy.36.refs_9_
  35.9 0.6 collective-permute-done.5
  36.5 0.4 collective-permute-start.3
  36.9 5.0 %shard_map.154 = (bf16[4,64,512]{2,1,0:T(8,128)(2,1)}, bf16[4,128,512]{2,1,0:T(8,128)(2,1)}) custom-call(s32[2]{0:T(128)S(1)} %pad_add_fusion.ids_ref, bf16[512,512]{1,0:T(8,128)(2,1)} %get-tuple-element.74.refs_0_, bf16[512,512]{1,0:T(8,128)(2,1)} %collective-permute-done.6.refs_1_, bf16[512,512]{1,0:T(8,128)(2,1)} %collective-permute-done.7.refs_2_, ...), custom_call_target="tpu_custom_call" | custom-call | flops 3221225472 | bytes 1048576 | tf_op jit(solution)/shard_map/pallas_call | solution.py:43
  41.9 6.1 %all-to-all-start.2 = ((bf16[4,128,512]{2,1,0:T(8,128)(2,1)}), bf16[4,128,512]{2,1,0:T(8,128)(2,1)}, u32[]{:S(2)}, u32[]{:S(2)}) async-start(bf16[4,128,512]{2,1,0:T(8,128)(2,1)} %get-tuple-element.48), calls=%async_computation.2 | async-start | bytes 1048576 | tf_op jit(solution)/shard_map/all_to_all | solution.py:78
  48.0 9.1 %shard_map.155 = (bf16[4,64,1024]{2,1,0:T(8,128)(2,1)}, bf16[128,512]{1,0:T(8,128)(2,1)}, bf16[128,512]{1,0:T(8,128)(2,1)}, bf16[128,512]{1,0:T(8,128)(2,1)}, bf...) custom-call(s32[2]{0:T(128)S(1)} %pad_add_fusion.ids_ref, ...), custom_call_target="tpu_custom_call" | custom-call | flops 3221225472 | bytes 1048576 | tf_op jit(solution)/shard_map/pallas_call | solution.py:43
  57.2 2.3 %all-to-all-done.2.refs_1_ = bf16[4,128,512]{2,1,0:T(8,128)(2,1)} async-done(((bf16[4,128,512]{2,1,0:T(8,128)(2,1)}), bf16[4,128,512]{2,1,0:T(8,128)(2,1)}, u32[]{:S(2)}, u32[]{:S(2)}) %all-to-all-start.2) | async-done | bytes 524320 | tf_op jit(solution)/shard_map/all_to_all | solution.py:78
  59.5 6.5 %all-to-all-start.1 = ((bf16[4,64,1024]{2,1,0:T(8,128)(2,1)}), bf16[4,64,1024]{2,1,0:T(8,128)(2,1)S(1)}, u32[]{:S(2)}, u32[]{:S(2)}) async-start(bf16[4,64,1024]{2,1,0:T(8,128)(2,1)} %get-tuple-element.47), calls=%async_computation.1 | async-start | bytes 1048576 | tf_op jit(solution)/shard_map/all_to_all | solution.py:78
  66.0 1.1 collective-permute-start.12
  67.1 1.2 collective-permute-start.9
  68.4 0.3 collective-permute-start.10
  68.6 1.1 collective-permute-start.11
  69.8 0.9 collective-permute-start.13
  70.7 8.6 %collective-permute-done.9.refs_3_ = bf16[128,512]{1,0:T(8,128)(2,1)S(1)} collective-permute-done((bf16[128,512]{1,0:T(8,128)(2,1)}, bf16[128,512]{1,0:T(8,128)(2,1)S(1)}, u32[]{:S(2)}, u32[]{:S(2)}) %collective-permute-start.9) | collective-permute-done | bytes 131104 | tf_op jit(solution)/shard_map/ppermute | solution.py:19
  79.3 0.2 collective-permute-start.14
  79.5 1.6 collective-permute-done.10.refs_4_
  81.1 1.2 collective-permute-start.17
  82.3 7.8 %collective-permute-done.11.refs_5_ = bf16[128,512]{1,0:T(8,128)(2,1)S(1)} collective-permute-done((bf16[128,512]{1,0:T(8,128)(2,1)}, bf16[128,512]{1,0:T(8,128)(2,1)S(1)}, u32[]{:S(2)}, u32[]{:S(2)}) %collective-permute-start.11) | collective-permute-done | bytes 131104 | tf_op jit(solution)/shard_map/ppermute | solution.py:19
  90.1 1.2 collective-permute-start.18
  91.4 1.4 collective-permute-start.16
  92.8 0.1 copy.38.refs_13_
  93.0 2.6 %collective-permute-done.15.refs_9_ = bf16[128,512]{1,0:T(8,128)(2,1)S(1)} collective-permute-done((bf16[128,512]{1,0:T(8,128)(2,1)S(1)}, bf16[128,512]{1,0:T(8,128)(2,1)S(1)}, u32[]{:S(2)}, u32[]{:S(2)}) %collective-permute-start.15) | collective-permute-done | bytes 131104 | tf_op jit(solution)/shard_map/ppermute | solution.py:19
  95.6 2.2 %collective-permute-done.16.refs_10_ = bf16[128,512]{1,0:T(8,128)(2,1)S(1)} collective-permute-done((bf16[128,512]{1,0:T(8,128)(2,1)S(1)}, bf16[128,512]{1,0:T(8,128)(2,1)S(1)}, u32[]{:S(2)}, u32[]{:S(2)}) %collective-permute-start.16) | collective-permute-done | bytes 131104 | tf_op jit(solution)/shard_map/ppermute | solution.py:19
  97.8 0.6 copy-done.21
  98.4 0.2 copy-done.3
  98.6 0.8 copy-done.14
  99.4 26.0 %shard_map.156 = bf16[16,64,256]{2,1,0:T(8,128)(2,1)} custom-call(s32[2]{0:T(128)S(1)} %pad_add_fusion.ids_ref, bf16[4,64,1024]{2,1,0:T(8,128)(2,1)} %copy-done.3, bf16[4,128,512]{2,1,0:T(8,128)(2,1)} %all-to-all-done.2.refs_1_, bf16[128,512]{1,0:T(8,128)(2,1)} %get-tuple-element.49.refs_2_, bf16[128,512]{1,0:T(8,128)(2,1)} %copy-done.15, ...), custom_call_target="tpu_custom_call" | custom-call | flops 8589934592 | bytes 1048576 | tf_op jit(solution)/shard_map/pallas_call | solution.py:43
  125.4 4.0 %collective-permute-start.25 = (bf16[256,2048]{1,0:T(8,128)(2,1)}, bf16[256,2048]{1,0:T(8,128)(2,1)}, u32[]{:S(2)}, u32[]{:S(2)}) collective-permute-start(bf16[256,2048]{1,0:T(8,128)(2,1)} %refs_4_), channel_id=1, source_target_pairs={{0,1},{1,0},{2,3},{3,2},{4,5},{5,4},{6,7},{7,6},{8,9},{9,8},{10,11... | collective-permute-start | bytes 3145736 | tf_op jit(solution)/shard_map/ppermute | solution.py:19
  129.5 0.5 collective-permute-start.19
  130.0 11.9 %all-to-all-start.3 = ((bf16[16,64,256]{2,1,0:T(8,128)(2,1)}), bf16[16,64,256]{2,1,0:T(8,128)(2,1)S(1)}, u32[]{:S(2)}, u32[]{:S(2)}) async-start(bf16[16,64,256]{2,1,0:T(8,128)(2,1)} %shard_map.156), calls=%async_computation.3 | async-start | bytes 1048576 | tf_op jit(solution)/shard_map/all_to_all | solution.py:597
  141.8 0.1 copy.41.refs_6_
  142.0 3.8 %collective-permute-start.21 = (bf16[256,128]{1,0:T(8,128)(2,1)S(1)}, bf16[256,128]{1,0:T(8,128)(2,1)S(1)}, u32[]{:S(2)}, u32[]{:S(2)}) collective-permute-start(bf16[256,128]{1,0:T(8,128)(2,1)S(1)} %copy-done.22), channel_id=1, source_target_pairs={{0,4},{4,8},{8,12},{12,16},{16,20},{20,24},{24,28},{1,5},{5,9},{9,... | collective-permute-start | bytes 196616 | tf_op jit(solution)/shard_map/ppermute | solution.py:580
  145.8 5.8 %shard_map.157 = (f32[256,512]{1,0:T(8,128)}, bf16[256,512]{1,0:T(8,128)(2,1)}, bf16[256,128]{1,0:T(8,128)(2,1)}) custom-call(s32[2]{0:T(128)S(1)} %pad_add_fusion.ids_ref, bf16[512,512]{1,0:T(8,128)(2,1)} %get-tuple-element.74.refs_0_, bf16[512,512]{1,0:T(8,128)(2,1)} %collective-permute-done.6.refs_1_, bf16[512,512]{1,0:T(8,128)(2,1)} %collective-permute-done.7.refs_2_, ...), custom_call_target="tpu_custom_call" | custom-call | flops 3221225472 | bytes 1048576 | tf_op jit(solution)/shard_map/pallas_call | solution.py:43
  151.6 5.0 %collective-permute-done.21.refs_4_ = bf16[256,128]{1,0:T(8,128)(2,1)S(1)} collective-permute-done((bf16[256,128]{1,0:T(8,128)(2,1)S(1)}, bf16[256,128]{1,0:T(8,128)(2,1)S(1)}, u32[]{:S(2)}, u32[]{:S(2)}) %collective-permute-start.21) | collective-permute-done | bytes 65568 | tf_op jit(solution)/shard_map/ppermute | solution.py:580
  156.6 0.6 copy-done.7
  157.2 3.0 %shard_map.158 = (bf16[256,256]{1,0:T(8,128)(2,1)}, bf16[256,256]{1,0:T(8,128)(2,1)}, bf16[256,256]{1,0:T(8,128)(2,1)}, bf16[256,256]{1,0:T(8,128)(2,1)}) custom-call(s32[2]{0:T(128)S(1)} %pad_add_fusion.ids_ref, f32[256,512]{1,0:T(8,128)} %get-tuple-element.60.refs_0_, f32[256,512]{1,0:T(8,128)} %get-tuple-element.61.refs_1_, ...), custom_call_target="tpu_custom_call" | custom-call | flops 1048576 | bytes 1048576 | tf_op jit(solution)/shard_map/pallas_call | solution.py:43
  160.2 1.1 collective-permute-start.22
  161.4 2.9 %collective-permute-done.22.refs_1_ = bf16[256,256]{1,0:T(8,128)(2,1)S(1)} collective-permute-done((bf16[256,256]{1,0:T(8,128)(2,1)}, bf16[256,256]{1,0:T(8,128)(2,1)S(1)}, u32[]{:S(2)}, u32[]{:S(2)}) %collective-permute-start.22) | collective-permute-done | bytes 131104 | tf_op jit(solution)/shard_map/ppermute | solution.py:19
  164.2 2.5 %collective-permute-start.23 = (bf16[256,256]{1,0:T(8,128)(2,1)}, bf16[256,256]{1,0:T(8,128)(2,1)S(1)}, u32[]{:S(2)}, u32[]{:S(2)}) collective-permute-start(bf16[256,256]{1,0:T(8,128)(2,1)} %get-tuple-element.69), channel_id=1, source_target_pairs={{0,1},{1,0},{2,3},{3,2},{4,5},{5,4},{6,7},{7,6},{8,9},{9,8},{10,11... | collective-permute-start | bytes 393224 | tf_op jit(solution)/shard_map/ppermute | solution.py:19
  166.7 1.2 collective-permute-done.23.refs_2_
  167.9 1.1 collective-permute-start.24
  168.9 1.6 staged.3.refs_1_
  170.5 3.0 %collective-permute-done.24.refs_3_ = bf16[256,256]{1,0:T(8,128)(2,1)S(1)} collective-permute-done((bf16[256,256]{1,0:T(8,128)(2,1)}, bf16[256,256]{1,0:T(8,128)(2,1)S(1)}, u32[]{:S(2)}, u32[]{:S(2)}) %collective-permute-start.24) | collective-permute-done | bytes 131104 | tf_op jit(solution)/shard_map/ppermute | solution.py:19
  173.6 0.6 copy-done.6
  174.2 5.0 %shard_map.159.refs_4_ = bf16[256,2048]{1,0:T(8,128)(2,1)} custom-call(s32[2]{0:T(128)S(1)} %pad_add_fusion.ids_ref, bf16[256,256]{1,0:T(8,128)(2,1)} %get-tuple-element.67.refs_0_, bf16[256,256]{1,0:T(8,128)(2,1)} %copy-done.4, bf16[256,256]{1,0:T(8,128)(2,1)} %copy-done.5, bf16[256,256]{1,0:T(8,128)(2,1)} %copy-done.6, bf16[256,2048]{1,0:T(8,128)(2,1)} %refs_4_, ...), custom_call_target="tpu_custom_call" | custom-call | flops 1073741824 | bytes 1048576 | tf_op jit(solution)/shard_map/pallas_call | solution.py:43
  179.3 0.8 copy-done.2
  180.1 4.8 %shard_map.160 = bf16[256,2048]{1,0:T(8,128)(2,1)} custom-call(s32[2]{0:T(128)S(1)} %pad_add_fusion.ids_ref, bf16[16,64,256]{2,1,0:T(8,128)(2,1)} %copy-done.2, bf16[2,256,2048]{2,1,0:T(8,128)(2,1)S(1)} %staged.3.refs_1_, bf16[256,2048]{1,0:T(8,128)(2,1)} %collective-permute-done.19.refs_2_, bf16[256,2048]{1,0:T(8,128)(2,1)} %collective-permute-done.20.refs_3_, ...), custom_call_target="tpu_custom_call" | custom-call | flops 1073741824 | bytes 1048576 | tf_op jit(solution)/shard_map/pallas_call | solution.py:43
  (68 shorter events, 0.5 us)
Async XLA Ops:
  0.0 24.3 %copy-start.1 = (bf16[1024,512]{1,0:T(8,128)(2,1)S(1)}, bf16[1024,512]{1,0:T(8,128)(2,1)}, u32[]{:S(2)}) copy-start(bf16[1024,512]{1,0:T(8,128)(2,1)} %param.16) | copy-start | bytes 3145732
  0.0 19.0 %copy-start.8 = (f32[1024,4]{0,1:T(4,128)S(1)}, f32[1024,4]{0,1:T(4,128)}, u32[]{:S(2)}) copy-start(f32[1024,4]{0,1:T(4,128)} %param.26) | copy-start | bytes 49156
  0.0 28.5 %copy-start.9 = (f32[3,256]{1,0:T(4,128)S(1)}, f32[3,256]{1,0:T(4,128)}, u32[]{:S(2)}) copy-start(f32[3,256]{1,0:T(4,128)} %param.27) | copy-start | bytes 9220
  0.0 28.6 %copy-start.11 = (f32[256]{0:T(256)S(1)}, f32[256]{0:T(256)}, u32[]{:S(2)}) copy-start(f32[256]{0:T(256)} %param.28) | copy-start | bytes 3076
  3.3 13.1 %collective-permute-start.6 = (bf16[512,512]{1,0:T(8,128)(2,1)}, bf16[512,512]{1,0:T(8,128)(2,1)}, u32[]{:S(2)}, u32[]{:S(2)}) collective-permute-start(bf16[512,512]{1,0:T(8,128)(2,1)} %get-tuple-element.74.refs_0_), channel_id=1, source_target_pairs={{0,2},{1,3},{2,0},{3,1},{4,6},{5,7},{6,4},{7,5},{8,10},{9,11},{10,... | collective-permute-start | bytes 1572872 | tf_op jit(solution)/shard_map/ppermute | solution.py:19
  4.5 32.0 %collective-permute-start.1 = (bf16[512,512]{1,0:T(8,128)(2,1)}, bf16[512,512]{1,0:T(8,128)(2,1)}, u32[]{:S(2)}, u32[]{:S(2)}) collective-permute-start(bf16[512,512]{1,0:T(8,128)(2,1)} %get-tuple-element.73.refs_0_), channel_id=1, source_target_pairs={{0,2},{1,3},{2,0},{3,1},{4,6},{5,7},{6,4},{7,5},{8,10},{9,11},{10,... | collective-permute-start | bytes 1572872 | tf_op jit(solution)/shard_map/ppermute | solution.py:19
  4.7 32.2 %collective-permute-start.7 = (bf16[512,512]{1,0:T(8,128)(2,1)}, bf16[512,512]{1,0:T(8,128)(2,1)}, u32[]{:S(2)}, u32[]{:S(2)}) collective-permute-start(bf16[512,512]{1,0:T(8,128)(2,1)} %get-tuple-element.74.refs_0_), channel_id=1, source_target_pairs={{0,1},{1,0},{2,3},{3,2},{4,5},{5,4},{6,7},{7,6},{8,9},{9,8},{10,11... | collective-permute-start | bytes 1572872 | tf_op jit(solution)/shard_map/ppermute | solution.py:19
  16.4 20.5 %collective-permute-start.8 = (bf16[512,512]{1,0:T(8,128)(2,1)}, bf16[512,512]{1,0:T(8,128)(2,1)}, u32[]{:S(2)}, u32[]{:S(2)}) collective-permute-start(bf16[512,512]{1,0:T(8,128)(2,1)} %collective-permute-done.6.refs_1_), channel_id=1, source_target_pairs={{0,1},{1,0},{2,3},{3,2},{4,5},{5,4},{6,7},{7,6},{8,9},{9,8},{10,11... | collective-permute-start | bytes 1572872 | tf_op jit(solution)/shard_map/ppermute | solution.py:19
  19.7 7.5 %all-to-all-start = ((f32[4,1,1024]{2,1,0:T(1,128)}), f32[4,1,1024]{2,1,0:T(1,128)S(1)}, u32[]{:S(2)}, u32[]{:S(2)}) async-start(f32[4,1,1024]{2,1,0:T(1,128)} %all_to_all.17), calls=%async_computation | async-start | bytes 32768 | tf_op jit(solution)/shard_map/all_to_all | solution.py:78
  27.1 3.5 %collective-permute-start = (f32[4,1024]{1,0:T(4,128)S(1)}, f32[4,1024]{1,0:T(4,128)S(1)}, u32[]{:S(2)}, u32[]{:S(2)}) collective-permute-start(f32[4,1024]{1,0:T(4,128)S(1)} %bitcast.12), channel_id=1, source_target_pairs={{0,4},{4,0},{8,12},{12,8},{16,20},{20,16},{24,28},{28,24},{1,5},{5... | collective-permute-start | bytes 49160 | tf_op jit(solution)/shard_map/ppermute | solution.py:19
  28.7 7.0 %copy-start.12 = (f32[64]{0:T(128)S(1)}, f32[64]{0:T(128)}, u32[]{:S(2)}) copy-start(f32[64]{0:T(128)} %param.24) | copy-start | bytes 772
  28.7 7.1 %copy-start.13 = (f32[64]{0:T(128)S(1)}, f32[64]{0:T(128)}, u32[]{:S(2)}) copy-start(f32[64]{0:T(128)} %param.25) | copy-start | bytes 772
  30.6 17.4 %copy-start = (bf16[3,2048,256]{2,1,0:T(8,128)(2,1)}, bf16[3,2048,256]{2,1,0:T(8,128)(2,1)S(1)}, u32[]{:S(2)}) copy-start(bf16[3,2048,256]{2,1,0:T(8,128)(2,1)S(1)} %staged.2.refs_5_) | copy-start | bytes 9437188
  30.6 2.5 %collective-permute-start.4 = (f32[1,1024]{1,0:T(1,128)S(1)}, f32[1,1024]{1,0:T(1,128)S(1)}, u32[]{:S(2)}, u32[]{:S(2)}) collective-permute-start(f32[1,1024]{1,0:T(1,128)S(1)} %bitcast.14), channel_id=1, source_target_pairs={{0,2},{1,3},{2,0},{3,1},{4,6},{5,7},{6,4},{7,5},{8,10},{9,11},{10,... | collective-permute-start | bytes 12296 | tf_op jit(solution)/shard_map/ppermute | solution.py:19
  33.2 3.3 %collective-permute-start.5 = (f32[1,1024]{1,0:T(1,128)S(1)}, f32[1,1024]{1,0:T(1,128)S(1)}, u32[]{:S(2)}, u32[]{:S(2)}) collective-permute-start(f32[1,1024]{1,0:T(1,128)S(1)} %add.10), channel_id=1, source_target_pairs={{0,1},{1,0},{2,3},{3,2},{4,5},{5,4},{6,7},{7,6},{8,9},{9,8},{10,11... | collective-permute-start | bytes 12296 | tf_op jit(solution)/shard_map/ppermute | solution.py:19
  35.6 12.4 %collective-permute-start.2 = (bf16[512,512]{1,0:T(8,128)(2,1)}, bf16[512,512]{1,0:T(8,128)(2,1)}, u32[]{:S(2)}, u32[]{:S(2)}) collective-permute-start(bf16[512,512]{1,0:T(8,128)(2,1)} %get-tuple-element.73.refs_0_), channel_id=1, source_target_pairs={{0,1},{1,0},{2,3},{3,2},{4,5},{5,4},{6,7},{7,6},{8,9},{9,8},{10,11... | collective-permute-start | bytes 1572872 | tf_op jit(solution)/shard_map/ppermute | solution.py:19
  36.5 11.6 %collective-permute-start.3 = (bf16[512,512]{1,0:T(8,128)(2,1)}, bf16[512,512]{1,0:T(8,128)(2,1)}, u32[]{:S(2)}, u32[]{:S(2)}) collective-permute-start(bf16[512,512]{1,0:T(8,128)(2,1)} %collective-permute-done.1.refs_1_), channel_id=1, source_target_pairs={{0,1},{1,0},{2,3},{3,2},{4,5},{5,4},{6,7},{7,6},{8,9},{9,8},{10,11... | collective-permute-start | bytes 1572872 | tf_op jit(solution)/shard_map/ppermute | solution.py:19
  41.9 17.6 %all-to-all-start.2 = ((bf16[4,128,512]{2,1,0:T(8,128)(2,1)}), bf16[4,128,512]{2,1,0:T(8,128)(2,1)}, u32[]{:S(2)}, u32[]{:S(2)}) async-start(bf16[4,128,512]{2,1,0:T(8,128)(2,1)} %get-tuple-element.48), calls=%async_computation.2 | async-start | bytes 1048576 | tf_op jit(solution)/shard_map/all_to_all | solution.py:78
  59.5 38.3 %all-to-all-start.1 = ((bf16[4,64,1024]{2,1,0:T(8,128)(2,1)}), bf16[4,64,1024]{2,1,0:T(8,128)(2,1)S(1)}, u32[]{:S(2)}, u32[]{:S(2)}) async-start(bf16[4,64,1024]{2,1,0:T(8,128)(2,1)} %get-tuple-element.47), calls=%async_computation.1 | async-start | bytes 1048576 | tf_op jit(solution)/shard_map/all_to_all | solution.py:78
  66.0 31.8 %collective-permute-start.12 = (bf16[4,128,512]{2,1,0:T(8,128)(2,1)}, bf16[4,128,512]{2,1,0:T(8,128)(2,1)S(1)}, u32[]{:S(2)}, u32[]{:S(2)}) collective-permute-start(bf16[4,128,512]{2,1,0:T(8,128)(2,1)} %all-to-all-done.2.refs_1_), channel_id=1, source_target_pairs={{0,4},{4,0},{8,12},{12,8},{16,20},{20,16},{24,28},{28,24},{1,5},{5... | collective-permute-start | bytes 1572872 | tf_op jit(solution)/shard_map/ppermute | solution.py:19
  67.1 12.2 %collective-permute-start.9 = (bf16[128,512]{1,0:T(8,128)(2,1)}, bf16[128,512]{1,0:T(8,128)(2,1)S(1)}, u32[]{:S(2)}, u32[]{:S(2)}) collective-permute-start(bf16[128,512]{1,0:T(8,128)(2,1)} %get-tuple-element.50), channel_id=1, source_target_pairs={{0,8},{4,12},{8,0},{12,4},{16,24},{20,28},{24,16},{28,20},{1,9},{5... | collective-permute-start | bytes 393224 | tf_op jit(solution)/shard_map/ppermute | solution.py:19
  68.4 12.7 %collective-permute-start.10 = (bf16[128,512]{1,0:T(8,128)(2,1)}, bf16[128,512]{1,0:T(8,128)(2,1)S(1)}, u32[]{:S(2)}, u32[]{:S(2)}) collective-permute-start(bf16[128,512]{1,0:T(8,128)(2,1)} %get-tuple-element.51), channel_id=1, source_target_pairs={{0,16},{4,20},{8,24},{12,28},{16,0},{20,4},{24,8},{28,12},{1,17},{... | collective-permute-start | bytes 393224 | tf_op jit(solution)/shard_map/ppermute | solution.py:19
  68.6 21.5 %collective-permute-start.11 = (bf16[128,512]{1,0:T(8,128)(2,1)}, bf16[128,512]{1,0:T(8,128)(2,1)S(1)}, u32[]{:S(2)}, u32[]{:S(2)}) collective-permute-start(bf16[128,512]{1,0:T(8,128)(2,1)} %get-tuple-element.52), channel_id=1, source_target_pairs={{0,24},{4,28},{8,16},{12,20},{16,8},{20,12},{24,0},{28,4},{1,25},{... | collective-permute-start | bytes 393224 | tf_op jit(solution)/shard_map/ppermute | solution.py:19
  69.8 21.6 %collective-permute-start.13 = (bf16[128,512]{1,0:T(8,128)(2,1)}, bf16[128,512]{1,0:T(8,128)(2,1)S(1)}, u32[]{:S(2)}, u32[]{:S(2)}) collective-permute-start(bf16[128,512]{1,0:T(8,128)(2,1)} %get-tuple-element.49.refs_2_), channel_id=1, source_target_pairs={{0,4},{4,0},{8,12},{12,8},{16,20},{20,16},{24,28},{28,24},{1,5},{5... | collective-permute-start | bytes 393224 | tf_op jit(solution)/shard_map/ppermute | solution.py:19
  79.3 18.4 %copy-start.15 = (bf16[128,512]{1,0:T(8,128)(2,1)}, bf16[128,512]{1,0:T(8,128)(2,1)S(1)}, u32[]{:S(2)}) copy-start(bf16[128,512]{1,0:T(8,128)(2,1)S(1)} %collective-permute-done.9.refs_3_) | copy-start | bytes 393220
  79.3 12.0 %collective-permute-start.14 = (bf16[128,512]{1,0:T(8,128)(2,1)S(1)}, bf16[128,512]{1,0:T(8,128)(2,1)S(1)}, u32[]{:S(2)}, u32[]{:S(2)}) collective-permute-start(bf16[128,512]{1,0:T(8,128)(2,1)S(1)} %collective-permute-done.9.refs_3_), channel_id=1, source_target_pairs={{0,4},{4,0},{8,12},{12,8},{16,20},{20,16},{24,28},{28,24},{1,5},{5... | collective-permute-start | bytes 393224 | tf_op jit(solution)/shard_map/ppermute | solution.py:19
  81.1 16.7 %copy-start.16 = (bf16[128,512]{1,0:T(8,128)(2,1)}, bf16[128,512]{1,0:T(8,128)(2,1)S(1)}, u32[]{:S(2)}) copy-start(bf16[128,512]{1,0:T(8,128)(2,1)S(1)} %collective-permute-done.10.refs_4_) | copy-start | bytes 393220
  81.1 44.3 %collective-permute-start.17 = (bf16[256,2048]{1,0:T(8,128)(2,1)}, bf16[256,2048]{1,0:T(8,128)(2,1)}, u32[]{:S(2)}, u32[]{:S(2)}) collective-permute-start(bf16[256,2048]{1,0:T(8,128)(2,1)} %refs_0_.2), channel_id=1, source_target_pairs={{0,2},{1,3},{2,0},{3,1},{4,6},{5,7},{6,4},{7,5},{8,10},{9,11},{10,... | collective-permute-start | bytes 3145736 | tf_op jit(solution)/shard_map/ppermute | solution.py:19
  90.1 7.6 %copy-start.17 = (bf16[128,512]{1,0:T(8,128)(2,1)}, bf16[128,512]{1,0:T(8,128)(2,1)S(1)}, u32[]{:S(2)}) copy-start(bf16[128,512]{1,0:T(8,128)(2,1)S(1)} %collective-permute-done.11.refs_5_) | copy-start | bytes 393220
  90.1 35.3 %collective-permute-start.18 = (bf16[256,2048]{1,0:T(8,128)(2,1)}, bf16[256,2048]{1,0:T(8,128)(2,1)}, u32[]{:S(2)}, u32[]{:S(2)}) collective-permute-start(bf16[256,2048]{1,0:T(8,128)(2,1)} %refs_4_), channel_id=1, source_target_pairs={{0,2},{1,3},{2,0},{3,1},{4,6},{5,7},{6,4},{7,5},{8,10},{9,11},{10,... | collective-permute-start | bytes 3145736 | tf_op jit(solution)/shard_map/ppermute | solution.py:19
  91.4 6.4 %copy-start.18 = (bf16[128,512]{1,0:T(8,128)(2,1)}, bf16[128,512]{1,0:T(8,128)(2,1)S(1)}, u32[]{:S(2)}) copy-start(bf16[128,512]{1,0:T(8,128)(2,1)S(1)} %collective-permute-done.13.refs_7_) | copy-start | bytes 393220
  91.4 4.2 %collective-permute-start.15 = (bf16[128,512]{1,0:T(8,128)(2,1)S(1)}, bf16[128,512]{1,0:T(8,128)(2,1)S(1)}, u32[]{:S(2)}, u32[]{:S(2)}) collective-permute-start(bf16[128,512]{1,0:T(8,128)(2,1)S(1)} %collective-permute-done.10.refs_4_), channel_id=1, source_target_pairs={{0,4},{4,0},{8,12},{12,8},{16,20},{20,16},{24,28},{28,24},{1,5},{5... | collective-permute-start | bytes 393224 | tf_op jit(solution)/shard_map/ppermute | solution.py:19
  91.4 6.4 %copy-start.19 = (bf16[128,512]{1,0:T(8,128)(2,1)}, bf16[128,512]{1,0:T(8,128)(2,1)S(1)}, u32[]{:S(2)}) copy-start(bf16[128,512]{1,0:T(8,128)(2,1)S(1)} %collective-permute-done.14.refs_8_) | copy-start | bytes 393220
  91.4 6.4 %collective-permute-start.16 = (bf16[128,512]{1,0:T(8,128)(2,1)S(1)}, bf16[128,512]{1,0:T(8,128)(2,1)S(1)}, u32[]{:S(2)}, u32[]{:S(2)}) collective-permute-start(bf16[128,512]{1,0:T(8,128)(2,1)S(1)} %collective-permute-done.11.refs_5_), channel_id=1, source_target_pairs={{0,4},{4,0},{8,12},{12,8},{16,20},{20,16},{24,28},{28,24},{1,5},{5... | collective-permute-start | bytes 393224 | tf_op jit(solution)/shard_map/ppermute | solution.py:19
  92.9 48.9 %copy-start.10 = (f32[256]{0:T(256)S(1)}, f32[256]{0:T(256)}, u32[]{:S(2)}) copy-start(f32[256]{0:T(256)} %param.29) | copy-start | bytes 3076
  93.0 49.0 %copy-start.22 = (bf16[256,128]{1,0:T(8,128)(2,1)S(1)}, bf16[256,128]{1,0:T(8,128)(2,1)}, u32[]{:S(2)}) copy-start(bf16[256,128]{1,0:T(8,128)(2,1)} %get-tuple-element.64) | copy-start | bytes 196612
  95.6 2.2 %copy-start.20 = (bf16[128,512]{1,0:T(8,128)(2,1)}, bf16[128,512]{1,0:T(8,128)(2,1)S(1)}, u32[]{:S(2)}) copy-start(bf16[128,512]{1,0:T(8,128)(2,1)S(1)} %collective-permute-done.15.refs_9_) | copy-start | bytes 393220
  97.7 0.7 copy-start.21
  97.7 0.8 copy-start.3
  98.6 0.8 copy-start.14
  125.4 48.1 %collective-permute-start.25 = (bf16[256,2048]{1,0:T(8,128)(2,1)}, bf16[256,2048]{1,0:T(8,128)(2,1)}, u32[]{:S(2)}, u32[]{:S(2)}) collective-permute-start(bf16[256,2048]{1,0:T(8,128)(2,1)} %refs_4_), channel_id=1, source_target_pairs={{0,1},{1,0},{2,3},{3,2},{4,5},{5,4},{6,7},{7,6},{8,9},{9,8},{10,11... | collective-permute-start | bytes 3145736 | tf_op jit(solution)/shard_map/ppermute | solution.py:19
  129.5 44.1 %collective-permute-start.26 = (bf16[256,2048]{1,0:T(8,128)(2,1)}, bf16[256,2048]{1,0:T(8,128)(2,1)}, u32[]{:S(2)}, u32[]{:S(2)}) collective-permute-start(bf16[256,2048]{1,0:T(8,128)(2,1)} %collective-permute-done.18.refs_5_), channel_id=1, source_target_pairs={{0,1},{1,0},{2,3},{3,2},{4,5},{5,4},{6,7},{7,6},{8,9},{9,8},{10,11... | collective-permute-start | bytes 3145736 | tf_op jit(solution)/shard_map/ppermute | solution.py:19
  129.5 49.8 %collective-permute-start.19 = (bf16[256,2048]{1,0:T(8,128)(2,1)}, bf16[256,2048]{1,0:T(8,128)(2,1)}, u32[]{:S(2)}, u32[]{:S(2)}) collective-permute-start(bf16[256,2048]{1,0:T(8,128)(2,1)} %refs_0_.2), channel_id=1, source_target_pairs={{0,1},{1,0},{2,3},{3,2},{4,5},{5,4},{6,7},{7,6},{8,9},{9,8},{10,11... | collective-permute-start | bytes 3145736 | tf_op jit(solution)/shard_map/ppermute | solution.py:19
  130.0 49.3 %collective-permute-start.20 = (bf16[256,2048]{1,0:T(8,128)(2,1)}, bf16[256,2048]{1,0:T(8,128)(2,1)}, u32[]{:S(2)}, u32[]{:S(2)}) collective-permute-start(bf16[256,2048]{1,0:T(8,128)(2,1)} %collective-permute-done.17.refs_1_), channel_id=1, source_target_pairs={{0,1},{1,0},{2,3},{3,2},{4,5},{5,4},{6,7},{7,6},{8,9},{9,8},{10,11... | collective-permute-start | bytes 3145736 | tf_op jit(solution)/shard_map/ppermute | solution.py:19
  130.0 49.3 %all-to-all-start.3 = ((bf16[16,64,256]{2,1,0:T(8,128)(2,1)}), bf16[16,64,256]{2,1,0:T(8,128)(2,1)S(1)}, u32[]{:S(2)}, u32[]{:S(2)}) async-start(bf16[16,64,256]{2,1,0:T(8,128)(2,1)} %shard_map.156), calls=%async_computation.3 | async-start | bytes 1048576 | tf_op jit(solution)/shard_map/all_to_all | solution.py:597
  142.0 14.6 %collective-permute-start.21 = (bf16[256,128]{1,0:T(8,128)(2,1)S(1)}, bf16[256,128]{1,0:T(8,128)(2,1)S(1)}, u32[]{:S(2)}, u32[]{:S(2)}) collective-permute-start(bf16[256,128]{1,0:T(8,128)(2,1)S(1)} %copy-done.22), channel_id=1, source_target_pairs={{0,4},{4,8},{8,12},{12,16},{16,20},{20,24},{24,28},{1,5},{5,9},{9,... | collective-permute-start | bytes 196616 | tf_op jit(solution)/shard_map/ppermute | solution.py:580
  156.6 0.6 copy-start.7
  160.2 4.0 %collective-permute-start.22 = (bf16[256,256]{1,0:T(8,128)(2,1)}, bf16[256,256]{1,0:T(8,128)(2,1)S(1)}, u32[]{:S(2)}, u32[]{:S(2)}) collective-permute-start(bf16[256,256]{1,0:T(8,128)(2,1)} %get-tuple-element.68), channel_id=1, source_target_pairs={{0,2},{1,3},{2,0},{3,1},{4,6},{5,7},{6,4},{7,5},{8,10},{9,11},{10,... | collective-permute-start | bytes 393224 | tf_op jit(solution)/shard_map/ppermute | solution.py:19
  164.2 6.3 %copy-start.4 = (bf16[256,256]{1,0:T(8,128)(2,1)}, bf16[256,256]{1,0:T(8,128)(2,1)S(1)}, u32[]{:S(2)}) copy-start(bf16[256,256]{1,0:T(8,128)(2,1)S(1)} %collective-permute-done.22.refs_1_) | copy-start | bytes 393220
  164.2 3.7 %collective-permute-start.23 = (bf16[256,256]{1,0:T(8,128)(2,1)}, bf16[256,256]{1,0:T(8,128)(2,1)S(1)}, u32[]{:S(2)}, u32[]{:S(2)}) collective-permute-start(bf16[256,256]{1,0:T(8,128)(2,1)} %get-tuple-element.69), channel_id=1, source_target_pairs={{0,1},{1,0},{2,3},{3,2},{4,5},{5,4},{6,7},{7,6},{8,9},{9,8},{10,11... | collective-permute-start | bytes 393224 | tf_op jit(solution)/shard_map/ppermute | solution.py:19
  167.9 2.6 %copy-start.5 = (bf16[256,256]{1,0:T(8,128)(2,1)}, bf16[256,256]{1,0:T(8,128)(2,1)S(1)}, u32[]{:S(2)}) copy-start(bf16[256,256]{1,0:T(8,128)(2,1)S(1)} %collective-permute-done.23.refs_2_) | copy-start | bytes 393220
  167.9 5.7 %collective-permute-start.24 = (bf16[256,256]{1,0:T(8,128)(2,1)}, bf16[256,256]{1,0:T(8,128)(2,1)S(1)}, u32[]{:S(2)}, u32[]{:S(2)}) collective-permute-start(bf16[256,256]{1,0:T(8,128)(2,1)} %get-tuple-element.70), channel_id=1, source_target_pairs={{0,3},{1,2},{2,1},{3,0},{4,7},{5,6},{6,5},{7,4},{8,11},{9,10},{10,... | collective-permute-start | bytes 393224 | tf_op jit(solution)/shard_map/ppermute | solution.py:19
  173.6 0.6 copy-start.6
  179.2 0.8 copy-start.2
